TPU v7x, 32 devices: a whole 2x2x4 slice. The times are simulated.
32 devices in a mesh: dp: 4 (over y, x), kv: 4 (over z), tp: 2 (over core).
Axes of the slice: x: 2, y: 2, z: 4, core: 2. Of those that a mesh axis runs over, the one named last changes fastest.
Arguments:
- tokens: bfloat16 [64, 2048], P('dp', ('kv', 'tp')), may hold values from -30 to 30
- state: float32 [64, 4, 256, 512], P(('dp', 'kv'), 'tp'), may hold values from -6 to 6
- mix_gain: float32 [2048], P('kv'), may hold values from 0.1 to 1.9
- w_query: bfloat16 [2048, 1024], P('kv', 'tp'), may hold values from -0.125 to 0.125
- w_key: bfloat16 [2048, 1024], P('kv', 'tp'), may hold values from -0.125 to 0.125
- w_decay: bfloat16 [2048, 1024], P('kv', 'tp'), may hold values from -0.125 to 0.125
- w_value: bfloat16 [2048, 2048], P('kv', 'tp'), may hold values from -0.125 to 0.125
- w_gate: bfloat16 [2048, 2048], P('kv', 'tp'), may hold values from -0.125 to 0.125
- decay_offset: float32 [1024], P('tp'), may hold values from -1 to 4
- head_gain: float32 [512], replicated, may hold values from 0.1 to 1.9
- w_out: bfloat16 [2048, 2048], P('tp', 'kv'), may hold values from -0.125 to 0.125
- mlp_gain: float32 [2048], replicated, may hold values from 0.1 to 1.9
- w_up: bfloat16 [2048, 8192], P(None, ('kv', 'tp')), may hold values from -0.125 to 0.125
- w_down: bfloat16 [8192, 2048], P(('kv', 'tp')), may hold values from -0.09375 to 0.09375
Outputs:
- mixed: bfloat16 [64, 2048], P('dp', ('kv', 'tp'))
- new_state: float32 [64, 4, 256, 512], P(('dp', 'kv'), 'tp')
All inputs are finite; a program needn't handle non-finite values.
Results may differ from a plain program's by a relative error of at most 0.013.
Values may be sent and summed in bfloat16 or wider, within the bound.
No kernel may reach another device: no remote copies, remote signals or barrier semaphores. Data moves between devices by JAX's collectives and lax.ppermute only.
A program may use at most 64 MiB of HBM per device.

v0:
```python
import jax
import jax.numpy as jnp
from jax import lax
from jax.sharding import PartitionSpec as P

D = 2048


epsilon = 1e-06


def shards(
    tokens,
    state,
    mix_gain,
    w_query,
    w_key,
    w_decay,
    w_value,
    w_gate,
    decay_offset,
    head_gain,
    w_out,
    mlp_gain,
    w_up,
    w_down,
):
    seq_dev = state.shape[0]
    heads_here = state.shape[1]
    key_dim = state.shape[2]
    val_dim = state.shape[3]
    weights = (w_query, w_key, w_decay, w_value, w_gate)
    tok_cols = lax.all_gather(tokens, "tp", axis=1, tiled=True)
    tok_float = tok_cols.astype(jnp.float32)
    squares = jnp.sum(tok_float * tok_float, axis=1)
    scaled = (tok_float * mix_gain).astype(jnp.bfloat16)
    kv_index = lax.axis_index("kv")
    projected = lax.psum_scatter(
        jnp.concatenate(
            [jnp.dot(scaled, weight, preferred_element_type=jnp.float32) for weight in weights],
            axis=1,
        ),
        "kv",
        scatter_dimension=0,
        tiled=True,
    )
    all_sums = lax.psum(squares, "kv")
    row_sums = lax.dynamic_slice_in_dim(all_sums, kv_index * seq_dev, seq_dev, 0)
    row_scale = lax.rsqrt(row_sums / D + epsilon)[:, None]
    projected = projected * row_scale
    key_width = heads_here * key_dim
    val_width = heads_here * val_dim
    queries = (projected[:, :key_width] * key_dim ** (-0.5)).reshape(seq_dev, heads_here, key_dim)
    new_keys = projected[:, key_width : 2 * key_width].reshape(seq_dev, heads_here, key_dim)
    retain = jax.nn.sigmoid(projected[:, 2 * key_width : 3 * key_width] + decay_offset).reshape(
        seq_dev, heads_here, key_dim
    )
    values = projected[:, 3 * key_width : 3 * key_width + val_width].reshape(
        seq_dev, heads_here, val_dim
    )
    gates = projected[:, 3 * key_width + val_width :]
    new_state = retain[..., None] * state + new_keys[..., None] * values[:, :, None, :]
    readout = jnp.einsum("bhk,bhkv->bhv", queries, new_state, precision=lax.Precision.HIGHEST)
    readout = (
        readout
        * lax.rsqrt(jnp.mean(readout * readout, axis=2, keepdims=True) + epsilon)
        * head_gain
    )
    gated = (readout.reshape(seq_dev, val_width) * jax.nn.silu(gates)).astype(jnp.bfloat16)
    branch = jnp.dot(
        lax.all_gather(gated, "kv", axis=0, tiled=True), w_out, preferred_element_type=jnp.float32
    )
    own_width = tokens.shape[1]
    branch_total = lax.psum(branch.astype(jnp.bfloat16), "tp").astype(jnp.float32)
    stream_cols = (tok_float + branch_total).astype(jnp.bfloat16)
    stream = lax.all_gather(stream_cols, "kv", axis=1, tiled=True)
    stream_own = lax.dynamic_slice_in_dim(
        stream_cols, lax.axis_index("tp") * own_width, own_width, 1
    )
    stream_float = stream.astype(jnp.float32)
    mlp_scale = lax.rsqrt(jnp.mean(stream_float * stream_float, axis=1, keepdims=True) + epsilon)
    normed = (stream_float * mlp_gain).astype(jnp.bfloat16)
    hidden = jnp.dot(normed, w_up, preferred_element_type=jnp.float32) * mlp_scale
    squared = jnp.square(jax.nn.relu(hidden)).astype(jnp.bfloat16)
    down_own = lax.psum_scatter(
        lax.dot_general(
            w_down, squared, (((0,), (1,)), ((), ())), preferred_element_type=jnp.float32
        ),
        ("kv", "tp"),
        scatter_dimension=0,
        tiled=True,
    )
    mixed = (stream_own.astype(jnp.float32) + down_own.T).astype(jnp.bfloat16)
    return (mixed, new_state)


def solution(mesh):
    in_specs = (
        P("dp", ("kv", "tp")),
        P(("dp", "kv"), "tp", None, None),
        P("kv"),
        P("kv", "tp"),
        P("kv", "tp"),
        P("kv", "tp"),
        P("kv", "tp"),
        P("kv", "tp"),
        P("tp"),
        P(),
        P("tp", "kv"),
        P(),
        P(None, ("kv", "tp")),
        P(("kv", "tp"), None),
    )
    out_specs = (P("dp", ("kv", "tp")), P(("dp", "kv"), "tp", None, None))
    return jax.shard_map(shards, mesh=mesh, in_specs=in_specs, out_specs=out_specs, check_vma=False)
```

profile of v0, /device:TPU:0, one launch (start us, length us, event | category | flops | bytes accessed | tf_op | source)
XLA Modules:
  0.0 136.5 jit_solution(3327729443919918969)
XLA Ops:
  7.2 2.3 %all_gather.9 = bf16[16,512]{1,0:T(8,128)(2,1)S(1)} all-gather(bf16[16,256]{1,0:T(8,128)(2,1)} %param.14), channel_id=1, replica_groups=mesh['dp'=4,'kv'=4,'tp'=2] {'tp'}, dimensions={1}, use_global_device_ids=true | all-gather | bytes 24576 | tf_op jit(solution)/shard_map/all_gather | solution.py:33
  9.6 1.2 convolution_dynamic-update-slice_fusion.4
  10.8 1.2 convolution_dynamic-update-slice_fusion.3
  12.0 1.2 convolution_dynamic-update-slice_fusion.2
  13.3 0.9 convolution_dynamic-update-slice_fusion.1
  14.2 1.5 %convolution_dynamic-update-slice_fusion = f32[16,3584]{1,0:T(8,128)S(1)} fusion(f32[16,3584]{1,0:T(8,128)S(1)} %convolution_dynamic-update-slice_fusion.1, bf16[512,1024]{1,0:T(8,128)(2,1)} %param.21, bf16[16,512]{1,0:T(8,128)(2,1)S(1)} %all_gather.9, f32[512]{0:T(512)} %param.16), kind=kOutput, calls=%fused_computation.2 | convolution fusion | flops 16801792 | bytes 1132544 | tf_op jit(solution)/shard_map/dot_general | solution.py:40
  15.7 0.7 copy-done.3
  16.5 0.6 dynamic-slice
  17.7 0.1 fusion.10
  17.8 13.3 %psum.14 = f32[16]{0:T(128)S(1)} all-reduce(f32[16]{0:T(128)S(1)} %fusion.10), channel_id=1, replica_groups=mesh['dp'=4,'kv'=4,'tp'=2] {'kv'}, use_global_device_ids=true, to_apply=%region_2.0 | all-reduce | flops 16 | bytes 128 | tf_op jit(solution)/shard_map/psum | solution.py:47
  31.3 23.2 %all-reduce.3.cloned.1.call-done = f32[16,3584]{1,0:T(8,128)} async-done(((f32[16,3584]{1,0:T(8,128)}), f32[16,3584]{1,0:T(8,128)}) %all-reduce.3.cloned.1.call-update) | async-done | bytes 229392
  54.4 1.0 dynamic-slice_multiply_fusion
  55.5 2.6 %multiply_add_fusion = f32[4,2,256,512]{3,2,1,0:T(8,128)S(1)} fusion(f32[4,2,256,512]{3,2,1,0:T(8,128)} %param.15, f32[4,2,512]{2,1,0:T(2,128)S(1)} %mul.116, f32[4,2,256]{2,1,0:T(2,128)S(1)} %mul.114, f32[4,2,256]{2,1,0:T(2,128)S(1)} %mul.111), kind=kLoop, calls=%fused_computation | loop fusion | flops 3145728 | bytes 8421376 | tf_op jit(solution)/shard_map/add | solution.py:62
  58.2 2.0 %copy-done.1 = f32[4,2,256,512]{3,2,1,0:T(8,128)} copy-done((f32[4,2,256,512]{3,2,1,0:T(8,128)}, f32[4,2,256,512]{3,2,1,0:T(8,128)S(1)}, u32[]{:S(2)}) %copy-start.1) | copy-done | bytes 4194328
  60.2 2.1 %fusion.31 = f32[4,2,1,512]{3,2,1,0:T(1,128)S(1)} fusion(f32[4,2,256,1]{2,3,1,0:T(1,128)S(1)} %reshape.41, f32[4,2,256,512]{3,2,1,0:T(8,128)S(1)} %multiply_add_fusion), kind=kOutput, calls=%fused_computation.47 | convolution fusion | flops 12582912 | bytes 4218880 | tf_op jit(solution)/shard_map/bhk,bhkv->bhv/dot_general | solution.py:63
  62.2 0.1 fusion.16
  62.5 13.1 %all-gather = bf16[4,4,1024]{2,1,0:T(4,128)(2,1)S(1)} all-gather(bf16[1,4,1024]{2,1,0:T(4,128)(2,1)S(1)} %fusion.24), channel_id=1, replica_groups=mesh['dp'=4,'kv'=4,'tp'=2] {'kv'}, dimensions={0}, use_global_device_ids=true | all-gather | bytes 40960 | tf_op jit(solution)/shard_map/all_gather | solution.py:71
  75.6 0.2 convolution_convert_fusion
  75.9 3.4 %psum.15 = bf16[16,512]{1,0:T(8,128)(2,1)S(1)} all-reduce(bf16[16,512]{1,0:T(8,128)(2,1)S(1)} %convolution_convert_fusion), channel_id=1, replica_groups=mesh['dp'=4,'kv'=4,'tp'=2] {'tp'}, use_global_device_ids=true, to_apply=%region_4.5 | all-reduce | flops 8192 | bytes 32768 | tf_op jit(solution)/shard_map/psum | solution.py:74
  79.3 13.1 %all_gather.11 = bf16[16,2048]{1,0:T(8,128)(2,1)S(1)} all-gather(bf16[16,512]{1,0:T(8,128)(2,1)S(1)} %fusion.11), channel_id=1, replica_groups=mesh['dp'=4,'kv'=4,'tp'=2] {'kv'}, dimensions={1}, use_global_device_ids=true | all-gather | bytes 81920 | tf_op jit(solution)/shard_map/all_gather | solution.py:76
  92.4 0.1 fusion.4
  92.5 5.3 %convolution_bitcast_fusion = f32[2048,16]{0,1:T(8,128)} fusion(bf16[1024,2048]{1,0:T(8,128)(2,1)} %param.27, bf16[2048,1024]{1,0:T(8,128)(2,1)} %param.26, bf16[16,2048]{1,0:T(8,128)(2,1)S(1)} %all_gather.11, f32[2048]{0:T(1024)S(1)} %copy-done.4, f32[16]{0:T(128)S(1)} %add_rsqrt_fusion.1), kind=kOutput, calls=%fused_computation.1 | convolution fusion | flops 134381568 | bytes 8593472 | tf_op jit(solution)/shard_map/dot_general | solution.py:86
  97.9 30.5 %reduce-scatter.2.cloned.1.call-done = f32[256,16]{0,1:T(8,128)} async-done(((f32[2048,16]{0,1:T(8,128)}), f32[256,16]{0,1:T(8,128)}) %reduce-scatter.2.cloned.1.call-update) | async-done | bytes 16400 | tf_op jit(solution)/shard_map/reduce_scatter | solution.py:85
  128.4 1.3 fusion.15
  (32 shorter events, 0.5 us)
Async XLA Ops:
  7.2 6.1 %copy-start = (bf16[512,1024]{1,0:T(8,128)(2,1)S(1)}, bf16[512,1024]{1,0:T(8,128)(2,1)}, u32[]{:S(2)}) copy-start(bf16[512,1024]{1,0:T(8,128)(2,1)} %param.20) | copy-start | bytes 3145732
  7.2 9.3 %copy-start.7 = (u32[32]{0:T(128)S(1)}, u32[32]{0:T(128)}, u32[]{:S(2)}) copy-start(u32[32]{0:T(128)} %constant.43) | copy-start | bytes 388
  7.2 48.3 %copy-start.5 = (f32[512]{0:T(512)S(1)}, f32[512]{0:T(512)}, u32[]{:S(2)}) copy-start(f32[512]{0:T(512)} %param.22) | copy-start | bytes 6148
  7.2 47.2 %all-reduce.3.cloned.1.call-start = ((), (), s32[]{:S(2)}) async-start(), calls=%async_computation.2 | async-start | bytes 458752
  15.7 0.7 copy-start.3
  16.4 111.9 %reduce-scatter.2.cloned.1.call-start = ((), (), s32[]{:S(2)}) async-start(), calls=%async_computation.1 | async-start | bytes 147456 | tf_op jit(solution)/shard_map/reduce_scatter | solution.py:85
  58.1 2.0 %copy-start.1 = (f32[4,2,256,512]{3,2,1,0:T(8,128)}, f32[4,2,256,512]{3,2,1,0:T(8,128)S(1)}, u32[]{:S(2)}) copy-start(f32[4,2,256,512]{3,2,1,0:T(8,128)S(1)} %multiply_add_fusion) | copy-start | bytes 12582916
  60.2 2.2 %copy-start.6 = (f32[512]{0:T(512)S(1)}, f32[512]{0:T(512)}, u32[]{:S(2)}) copy-start(f32[512]{0:T(512)} %param.23) | copy-start | bytes 6148
  60.2 15.5 %copy-start.2 = (bf16[1024,512]{1,0:T(8,128)(2,1)S(1)}, bf16[1024,512]{1,0:T(8,128)(2,1)}, u32[]{:S(2)}) copy-start(bf16[1024,512]{1,0:T(8,128)(2,1)} %param.24) | copy-start | bytes 3145732
  60.2 32.4 %copy-start.4 = (f32[2048]{0:T(1024)S(1)}, f32[2048]{0:T(1024)}, u32[]{:S(2)}) copy-start(f32[2048]{0:T(1024)} %param.25) | copy-start | bytes 24580
Sparse Core Ops, SparseCore 0:
  16.5 37.8 all-reduce.2
  98.0 30.3 reduce-scatter.1
where the time goes:
time: 137 us
  waiting for transfers between devices  53.7 us (39%)
  blocking collectives  45.3 us (33%)
  between operations  14.8 us (11%)
  matrix products  13.8 us (10%)
  other arithmetic  5.45 us (4%)
  local copies, waits for them, and re-layouts  3.42 us (2%)
    reduce_scatter x1, waiting for transfers between devices, shards(): lax.psum_scatter(lax.dot_general(w_down, squared, (((0,), (1,)), ((), ())...  30.5 us
    unnamed x3, waiting for transfers between devices  23.2 us
    psum x1, blocking collectives, shards(): all_sums = lax.psum(squares, 'kv')  13.3 us
    all_gather x1, blocking collectives, shards(): lax.all_gather(gated, 'kv', axis=0, tiled=True)  13.1 us
    all_gather x1, blocking collectives, shards(): stream = lax.all_gather(stream_cols, 'kv', axis=1, tiled=True)  13.1 us
    dot_general x5, matrix products, shards(): jnp.dot(scaled, weight, preferred_element_type=jnp.float32)  6.15 us
    dot_general x1, matrix products, shards(): lax.dot_general(w_down, squared, (((0,), (1,)), ((), ())), preferred_elem...  5.33 us
    psum x1, blocking collectives, shards(): lax.psum(branch.astype(jnp.bfloat16), 'tp').astype(jnp.float32)  3.37 us
  transfers between devices with their start and end apart: 2, of which 2 were waited for; matrix products, arithmetic and copies ran while one was open for 1% of the time, Pallas kernels for 0%

commit v1 on v0

v1 whole, which is shorter than its diff:
```python
import jax
import jax.numpy as jnp
from jax import lax
from jax.sharding import PartitionSpec as P

epsilon = 1e-06


def swap_cores(value):
    return lax.ppermute(value, "tp", [(0, 1), (1, 0)])


def spread(pieces, kv_size, me):
    if kv_size <= 8:
        return [pieces[0]] + [
            lax.ppermute(pieces[k], "kv", [(i, i ^ k) for i in range(kv_size)])
            for k in range(1, kv_size)
        ]
    order = jnp.arange(kv_size) ^ me
    sent = jnp.take(jnp.stack(pieces), order, axis=0)
    came = jnp.take(lax.all_to_all(sent, "kv", 0, 0, tiled=True), order, axis=0)
    return [came[k] for k in range(kv_size)]


def shards(kv_size, tokens, state, mix_gain, w_query, w_key, w_decay, w_value, w_gate, decay_offset, head_gain,
           w_out, mlp_gain, w_up, w_down):
    seq_dev, heads_here, key_dim, val_dim = state.shape
    own_width = tokens.shape[1]
    me = lax.axis_index("kv")
    core = lax.axis_index("tp")
    depth = 2 * own_width * kv_size
    bf16, f32 = jnp.bfloat16, jnp.float32

    other = swap_cores(tokens)
    tok_cols = jnp.where(core == 0, jnp.concatenate([tokens, other], 1), jnp.concatenate([other, tokens], 1))
    tok_float = tok_cols.astype(f32)
    squares = jnp.sum(tok_float * tok_float, axis=1, keepdims=True)
    scaled = (tok_float * mix_gain).astype(bf16)
    weights = (w_query, w_key, w_decay, w_value, w_gate)
    partial = jnp.concatenate(
        [jnp.dot(scaled, w, preferred_element_type=f32) for w in weights]
        + [jnp.broadcast_to(squares, (squares.shape[0], 128))], axis=1).astype(bf16)
    blocks = [lax.dynamic_slice_in_dim(partial, (me ^ k) * seq_dev, seq_dev, 0) for k in range(kv_size)]
    projected = sum(b.astype(f32) for b in spread(blocks, kv_size, me))
    row_sums = projected[:, -1:]
    projected = projected * lax.rsqrt(row_sums / depth + epsilon)
    kw, vw = heads_here * key_dim, heads_here * val_dim
    queries = (projected[:, :kw] * key_dim ** (-0.5)).reshape(seq_dev, heads_here, key_dim)
    new_keys = projected[:, kw: 2 * kw].reshape(seq_dev, heads_here, key_dim)
    retain = jax.nn.sigmoid(projected[:, 2 * kw: 3 * kw] + decay_offset).reshape(seq_dev, heads_here, key_dim)
    values = projected[:, 3 * kw: 3 * kw + vw].reshape(seq_dev, heads_here, val_dim)
    gates = projected[:, 3 * kw + vw: 3 * kw + 2 * vw]
    new_state = retain[..., None] * state + new_keys[..., None] * values[:, :, None, :]
    readout = jnp.einsum("bhk,bhkv->bhv", queries, new_state, precision=lax.Precision.HIGHEST)
    readout = readout * lax.rsqrt(jnp.mean(readout * readout, axis=2, keepdims=True) + epsilon) * head_gain
    gated = (readout.reshape(seq_dev, vw) * jax.nn.silu(gates)).astype(bf16)

    arrived = spread([gated] * kv_size, kv_size, me)
    order = jnp.arange(kv_size) ^ me
    gated_all = jnp.take(jnp.stack(arrived), order, axis=0).reshape(kv_size * seq_dev, vw)
    branch = jnp.dot(gated_all, w_out, preferred_element_type=f32)
    branch_sent = branch.astype(bf16)
    branch_total = branch + swap_cores(branch_sent).astype(f32)
    stream_cols = (tok_float + branch_total).astype(bf16)
    stream_parts = spread([stream_cols] * kv_size, kv_size, me)
    stream = jnp.take(jnp.stack(stream_parts), order, axis=0)
    stream = stream.transpose(1, 0, 2).reshape(stream_cols.shape[0], depth)
    stream_float = stream.astype(f32)
    mlp_scale = lax.rsqrt(jnp.mean(stream_float * stream_float, axis=1, keepdims=True) + epsilon)
    normed = (stream_float * mlp_gain).astype(bf16)
    hidden = jnp.dot(normed, w_up, preferred_element_type=f32) * mlp_scale
    squared = jnp.square(jax.nn.relu(hidden)).astype(bf16)
    down = jnp.dot(squared, w_down, preferred_element_type=f32)
    rows = down.shape[0]
    down = down.reshape(rows, kv_size, 2, own_width)
    keep = jnp.where(core == 0, down[:, :, 0], down[:, :, 1])
    give = jnp.where(core == 0, down[:, :, 1], down[:, :, 0]).astype(bf16)
    pair = (keep + swap_cores(give).astype(f32)).astype(bf16)
    pieces = [lax.dynamic_index_in_dim(pair, me ^ k, 1, keepdims=False) for k in range(kv_size)]
    down_own = sum(p.astype(f32) for p in spread(pieces, kv_size, me))
    stream_own = lax.dynamic_slice_in_dim(stream_cols, core * own_width, own_width, 1)
    mixed = (stream_own.astype(f32) + down_own).astype(bf16)
    return (mixed, new_state)


def solution(mesh):
    kv_size = mesh.shape["kv"]
    in_specs = (
        P("dp", ("kv", "tp")),
        P(("dp", "kv"), "tp", None, None),
        P("kv"),
        P("kv", "tp"),
        P("kv", "tp"),
        P("kv", "tp"),
        P("kv", "tp"),
        P("kv", "tp"),
        P("tp"),
        P(),
        P("tp", "kv"),
        P(),
        P(None, ("kv", "tp")),
        P(("kv", "tp"), None),
    )
    out_specs = (P("dp", ("kv", "tp")), P(("dp", "kv"), "tp", None, None))

    def body(*args):
        return shards(kv_size, *args)

    return jax.shard_map(body, mesh=mesh, in_specs=in_specs, out_specs=out_specs, check_vma=False)
```

time: 137 us -> 59.2 us (0.43)
  blocking collectives: 45.3 us -> 0 us
  waiting for transfers between devices: 53.7 us -> 17 us
  starting transfers between devices: 0.08 us -> 18.7 us
  between operations: 14.8 us -> 0.88 us
    reduce_scatter x1 -> x0, waiting for transfers between devices: 30.5 us -> none  [shards(): lax.psum_scatter(lax.dot_general(w_down, squared, (((0,), (1,)), ((), ())...]
    all_gather x3 -> x0, blocking collectives: 28.6 us -> none  [the longest x1 13.1 us: shards(): lax.all_gather(gated, 'kv', axis=0, tiled=True)]
    unnamed x3 -> x0, waiting for transfers between devices: 23.2 us -> none
    ppermute x0 -> x15, starting transfers between devices: none -> 18.7 us  [the longest x12 18 us: spread(): lax.ppermute(pieces[k], 'kv', [(i, i ^ k) for i in range(kv_size)])]
    ppermute x0 -> x15, waiting for transfers between devices: none -> 17 us  [the longest x12 13.6 us: spread(): lax.ppermute(pieces[k], 'kv', [(i, i ^ k) for i in range(kv_size)])]
    psum x2 -> x0, blocking collectives: 16.7 us -> none  [the longest x1 13.3 us: shards(): all_sums = lax.psum(squares, 'kv')]
    unnamed x19 -> x15, local copies, waits for them, and re-layouts: 3.34 us -> 2.04 us
  transfers between devices with their start and end apart: 2 -> 15, of which waited for: 2 -> 14; matrix products, arithmetic and copies ran while one was open for 1% -> 0% of each run, Pallas kernels for 0% -> 0%
where the time goes in v1:
time: 59.2 us; the launch traced here: 58.8 us
  starting transfers between devices  18.7 us (32%)
  waiting for transfers between devices  17 us (29%)
  matrix products  13.4 us (23%)
  other arithmetic  5.03 us (8%)
  local copies, waits for them, and re-layouts  3.83 us (6%)
  between operations  0.88 us (1%)
    ppermute x12, starting transfers between devices, spread(): lax.ppermute(pieces[k], 'kv', [(i, i ^ k) for i in range(kv_size)])  18 us
    ppermute x12, waiting for transfers between devices, spread(): lax.ppermute(pieces[k], 'kv', [(i, i ^ k) for i in range(kv_size)])  13.6 us
    dot_general x5, matrix products, shards(): jnp.dot(scaled, w, preferred_element_type=f32)  6.39 us
    dot_general x1, matrix products, shards(): down = jnp.dot(squared, w_down, preferred_element_type=f32)  4.69 us
    ppermute x3, waiting for transfers between devices, swap_cores(): return lax.ppermute(value, 'tp', [(0, 1), (1, 0)])  3.39 us
    add x1, other arithmetic, shards(): retain[..., None] * state + new_keys[..., None] * values[:, :, None, :]  2.6 us
    dot_general x1, matrix products, shards(): jnp.einsum('bhk,bhkv->bhv', queries, new_state, precision=lax.Precision.H...  2.08 us
    unnamed x15, local copies, waits for them, and re-layouts  2.04 us
  transfers between devices with their start and end apart: 15, of which 14 were waited for; matrix products, arithmetic and copies ran while one was open for 0% of the time, Pallas kernels for 0%

profile of v1, /device:TPU:0, one launch (start us, length us, event | category | flops | bytes accessed | tf_op | source)
XLA Modules:
  0.0 58.8 jit_solution(7717542093487509713)
XLA Ops:
  3.1 1.3 %fusion.8 = bf16[16,3712]{1,0:T(8,128)(2,1)S(1)} fusion(bf16[512,512]{1,0:T(8,128)(2,1)} %param.17, f32[512]{0:T(512)} %param.16, bf16[16,256]{1,0:T(8,128)(2,1)S(1)} %collective-permute-done, bf16[16,256]{1,0:T(8,128)(2,1)} %param.14, pred[]{:T(512)S(6)} %eq.2), kind=kOutput, calls=%fused_computation.17 | convolution fusion | flops 8495103 | bytes 559105 | tf_op jit(solution)/shard_map/dot_general | solution.py:41
  4.4 1.3 %fusion.7 = bf16[16,3712]{1,0:T(8,128)(2,1)S(1)} fusion(bf16[16,3712]{1,0:T(8,128)(2,1)S(1)} %fusion.8, bf16[512,512]{1,0:T(8,128)(2,1)} %param.18, f32[512]{0:T(512)} %param.16, bf16[16,256]{1,0:T(8,128)(2,1)S(1)} %collective-permute-done, bf16[16,256]{1,0:T(8,128)(2,1)} %param.14, pred[]{:T(512)S(6)} %eq.2), kind=kOutput, calls=%fused_computation.15 | convolution fusion | flops 8495104 | bytes 559105 | tf_op jit(solution)/shard_map/dot_general | solution.py:41
  5.7 1.3 %fusion.6 = bf16[16,3712]{1,0:T(8,128)(2,1)S(1)} fusion(bf16[16,3712]{1,0:T(8,128)(2,1)S(1)} %fusion.7, bf16[512,512]{1,0:T(8,128)(2,1)} %param.19, f32[512]{0:T(512)} %param.16, bf16[16,256]{1,0:T(8,128)(2,1)S(1)} %collective-permute-done, bf16[16,256]{1,0:T(8,128)(2,1)} %param.14, pred[]{:T(512)S(6)} %eq.2), kind=kOutput, calls=%fused_computation.13 | convolution fusion | flops 8495104 | bytes 559105 | tf_op jit(solution)/shard_map/dot_general | solution.py:41
  7.0 1.0 %fusion.3 = bf16[16,3712]{1,0:T(8,128)(2,1)S(1)} fusion(bf16[16,3712]{1,0:T(8,128)(2,1)S(1)} %fusion.6, bf16[512,1024]{1,0:T(8,128)(2,1)S(1)} %copy-done, f32[512]{0:T(512)} %param.16, bf16[16,256]{1,0:T(8,128)(2,1)S(1)} %collective-permute-done, bf16[16,256]{1,0:T(8,128)(2,1)} %param.14, pred[]{:T(512)S(6)} %eq.2), kind=kOutput, calls=%fused_computation.9 | convolution fusion | flops 16891904 | bytes 1099777 | tf_op jit(solution)/shard_map/dot_general | solution.py:41
  8.0 1.5 %fusion.2 = bf16[16,3712]{1,0:T(8,128)(2,1)S(1)} fusion(bf16[16,3712]{1,0:T(8,128)(2,1)S(1)} %fusion.3, bf16[512,1024]{1,0:T(8,128)(2,1)} %param.21, f32[512]{0:T(512)} %param.16, bf16[16,256]{1,0:T(8,128)(2,1)S(1)} %collective-permute-done, bf16[16,256]{1,0:T(8,128)(2,1)} %param.14, pred[]{:T(512)S(6)} %eq.2), kind=kOutput, calls=%fused_computation.7 | convolution fusion | flops 16891904 | bytes 1099777 | tf_op jit(solution)/shard_map/dot_general | solution.py:41
  9.7 3.0 %collective-permute-start.1 = (bf16[4,3712]{1,0:T(4,128)(2,1)S(1)}, bf16[4,3712]{1,0:T(4,128)(2,1)S(1)}, u32[]{:S(2)}, u32[]{:S(2)}) collective-permute-start(bf16[4,3712]{1,0:T(4,128)(2,1)S(1)} %get-tuple-element.4), channel_id=1, source_target_pairs={{0,2},{2,0},{4,6},{6,4},{1,3},{3,1},{5,7},{7,5},{8,10},{10,8},{12,... | collective-permute-start | bytes 89096 | tf_op jit(solution)/shard_map/ppermute | solution.py:16
  12.6 2.5 %collective-permute-start.3 = (bf16[4,3712]{1,0:T(4,128)(2,1)S(1)}, bf16[4,3712]{1,0:T(4,128)(2,1)S(1)}, u32[]{:S(2)}, u32[]{:S(2)}) collective-permute-start(bf16[4,3712]{1,0:T(4,128)(2,1)S(1)} %get-tuple-element.5), channel_id=1, source_target_pairs={{0,6},{2,4},{4,2},{6,0},{1,7},{3,5},{5,3},{7,1},{8,14},{10,12},{12... | collective-permute-start | bytes 89096 | tf_op jit(solution)/shard_map/ppermute | solution.py:16
  15.2 3.1 %collective-permute-done.3 = bf16[4,3712]{1,0:T(4,128)(2,1)S(1)} collective-permute-done((bf16[4,3712]{1,0:T(4,128)(2,1)S(1)}, bf16[4,3712]{1,0:T(4,128)(2,1)S(1)}, u32[]{:S(2)}, u32[]{:S(2)}) %collective-permute-start.3) | collective-permute-done | bytes 29728 | tf_op jit(solution)/shard_map/ppermute | solution.py:16
  18.3 1.9 %collective-permute-done.2 = bf16[4,3712]{1,0:T(4,128)(2,1)S(1)} collective-permute-done((bf16[4,3712]{1,0:T(4,128)(2,1)S(1)}, bf16[4,3712]{1,0:T(4,128)(2,1)S(1)}, u32[]{:S(2)}, u32[]{:S(2)}) %collective-permute-start.2) | collective-permute-done | bytes 29728 | tf_op jit(solution)/shard_map/ppermute | solution.py:16
  20.7 2.6 %multiply_add_fusion = f32[4,2,256,512]{3,2,1,0:T(8,128)S(1)} fusion(f32[4,2,256,512]{3,2,1,0:T(8,128)} %param.15, f32[4,2,512]{2,1,0:T(2,128)S(1)} %mul.133, f32[4,2,256]{2,1,0:T(2,128)S(1)} %mul.131, f32[4,2,256]{2,1,0:T(2,128)S(1)} %mul.128), kind=kLoop, calls=%fused_computation.2 | loop fusion | flops 3145728 | bytes 8421376 | tf_op jit(solution)/shard_map/add | solution.py:53
  23.3 2.0 %copy-done.1 = f32[4,2,256,512]{3,2,1,0:T(8,128)} copy-done((f32[4,2,256,512]{3,2,1,0:T(8,128)}, f32[4,2,256,512]{3,2,1,0:T(8,128)S(1)}, u32[]{:S(2)}) %copy-start.1) | copy-done | bytes 4194328
  25.3 2.1 %fusion.49 = f32[4,2,1,512]{3,2,1,0:T(1,128)S(1)} fusion(f32[4,2,256,1]{2,3,1,0:T(1,128)S(1)} %reshape.95, f32[4,2,256,512]{3,2,1,0:T(8,128)S(1)} %multiply_add_fusion), kind=kOutput, calls=%fused_computation.86 | convolution fusion | flops 12582912 | bytes 4218880 | tf_op jit(solution)/shard_map/bhk,bhkv->bhv/dot_general | solution.py:54
  27.6 1.5 %collective-permute-start.6 = (bf16[4,1024]{1,0:T(4,128)(2,1)S(1)}, bf16[4,1024]{1,0:T(4,128)(2,1)S(1)}, u32[]{:S(2)}, u32[]{:S(2)}) collective-permute-start(bf16[4,1024]{1,0:T(4,128)(2,1)S(1)} %fusion.31), channel_id=1, source_target_pairs={{0,6},{2,4},{4,2},{6,0},{1,7},{3,5},{5,3},{7,1},{8,14},{10,12},{12... | collective-permute-start | bytes 24584 | tf_op jit(solution)/shard_map/ppermute | solution.py:16
  29.6 2.5 %collective-permute-start.4 = (bf16[4,1024]{1,0:T(4,128)(2,1)S(1)}, bf16[4,1024]{1,0:T(4,128)(2,1)S(1)}, u32[]{:S(2)}, u32[]{:S(2)}) collective-permute-start(bf16[4,1024]{1,0:T(4,128)(2,1)S(1)} %fusion.31), channel_id=1, source_target_pairs={{0,2},{2,0},{4,6},{6,4},{1,3},{3,1},{5,7},{7,5},{8,10},{10,8},{12,... | collective-permute-start | bytes 24584 | tf_op jit(solution)/shard_map/ppermute | solution.py:16
  34.7 1.2 %collective-permute-done.7 = bf16[16,512]{1,0:T(8,128)(2,1)S(1)} collective-permute-done((bf16[16,512]{1,0:T(8,128)(2,1)S(1)}, bf16[16,512]{1,0:T(8,128)(2,1)S(1)}, u32[]{:S(2)}, u32[]{:S(2)}) %collective-permute-start.7) | collective-permute-done | bytes 16416 | tf_op jit(solution)/shard_map/ppermute | solution.py:10
  35.9 2.4 %collective-permute-start.10 = (bf16[16,512]{1,0:T(8,128)(2,1)S(1)}, bf16[16,512]{1,0:T(8,128)(2,1)S(1)}, u32[]{:S(2)}, u32[]{:S(2)}) collective-permute-start(bf16[16,512]{1,0:T(8,128)(2,1)S(1)} %fusion.15), channel_id=1, source_target_pairs={{0,6},{2,4},{4,2},{6,0},{1,7},{3,5},{5,3},{7,1},{8,14},{10,12},{12... | collective-permute-start | bytes 49160 | tf_op jit(solution)/shard_map/ppermute | solution.py:16
  38.3 1.1 %collective-permute-start.9 = (bf16[16,512]{1,0:T(8,128)(2,1)S(1)}, bf16[16,512]{1,0:T(8,128)(2,1)S(1)}, u32[]{:S(2)}, u32[]{:S(2)}) collective-permute-start(bf16[16,512]{1,0:T(8,128)(2,1)S(1)} %fusion.15), channel_id=1, source_target_pairs={{0,4},{2,6},{4,0},{6,2},{1,5},{3,7},{5,1},{7,3},{8,12},{10,14},{12... | collective-permute-start | bytes 49160 | tf_op jit(solution)/shard_map/ppermute | solution.py:16
  40.3 1.3 %collective-permute-done.10 = bf16[16,512]{1,0:T(8,128)(2,1)S(1)} collective-permute-done((bf16[16,512]{1,0:T(8,128)(2,1)S(1)}, bf16[16,512]{1,0:T(8,128)(2,1)S(1)}, u32[]{:S(2)}, u32[]{:S(2)}) %collective-permute-start.10) | collective-permute-done | bytes 16416 | tf_op jit(solution)/shard_map/ppermute | solution.py:16
  41.6 1.3 %collective-permute-done.9 = bf16[16,512]{1,0:T(8,128)(2,1)S(1)} collective-permute-done((bf16[16,512]{1,0:T(8,128)(2,1)S(1)}, bf16[16,512]{1,0:T(8,128)(2,1)S(1)}, u32[]{:S(2)}, u32[]{:S(2)}) %collective-permute-start.9) | collective-permute-done | bytes 16416 | tf_op jit(solution)/shard_map/ppermute | solution.py:16
  44.0 4.7 %fusion.5 = f32[16,2048]{1,0:T(8,128)S(1)} fusion(bf16[1024,2048]{1,0:T(8,128)(2,1)} %param.27, bf16[2048,1024]{1,0:T(8,128)(2,1)} %param.26, f32[16,2048]{1,0:T(8,128)S(1)} %bitcast.51, f32[2048]{0:T(1024)S(1)} %copy-done.4, f32[16]{0:T(128)S(1)} %add_rsqrt_fusion.1), kind=kOutput, calls=%fused_computation.11 | convolution fusion | flops 134348800 | bytes 8659008 | tf_op jit(solution)/shard_map/dot_general | solution.py:73
  49.1 1.2 %collective-permute-done.11 = bf16[16,4,256]{2,0,1:T(8,128)(2,1)S(1)} collective-permute-done((bf16[16,4,256]{2,0,1:T(8,128)(2,1)S(1)}, bf16[16,4,256]{2,0,1:T(8,128)(2,1)S(1)}, u32[]{:S(2)}, u32[]{:S(2)}) %collective-permute-start.11) | collective-permute-done | bytes 32800 | tf_op jit(solution)/shard_map/ppermute | solution.py:10
  51.3 2.3 %collective-permute-start.14 = (bf16[16,256]{1,0:T(8,128)(2,1)S(1)}, bf16[16,256]{1,0:T(8,128)(2,1)S(1)}, u32[]{:S(2)}, u32[]{:S(2)}) collective-permute-start(bf16[16,256]{1,0:T(8,128)(2,1)S(1)} %get-tuple-element.11), channel_id=1, source_target_pairs={{0,6},{2,4},{4,2},{6,0},{1,7},{3,5},{5,3},{7,1},{8,14},{10,12},{12... | collective-permute-start | bytes 24584 | tf_op jit(solution)/shard_map/ppermute | solution.py:16
  54.0 2.7 %collective-permute-done.14 = bf16[16,256]{1,0:T(8,128)(2,1)S(1)} collective-permute-done((bf16[16,256]{1,0:T(8,128)(2,1)S(1)}, bf16[16,256]{1,0:T(8,128)(2,1)S(1)}, u32[]{:S(2)}, u32[]{:S(2)}) %collective-permute-start.14) | collective-permute-done | bytes 8224 | tf_op jit(solution)/shard_map/ppermute | solution.py:16
  56.8 1.4 %collective-permute-done.13 = bf16[16,256]{1,0:T(8,128)(2,1)S(1)} collective-permute-done((bf16[16,256]{1,0:T(8,128)(2,1)S(1)}, bf16[16,256]{1,0:T(8,128)(2,1)S(1)}, u32[]{:S(2)}, u32[]{:S(2)}) %collective-permute-start.13) | collective-permute-done | bytes 8224 | tf_op jit(solution)/shard_map/ppermute | solution.py:16
  (67 shorter events, 10.9 us)
Async XLA Ops:
  0.6 6.3 %copy-start = (bf16[512,1024]{1,0:T(8,128)(2,1)S(1)}, bf16[512,1024]{1,0:T(8,128)(2,1)}, u32[]{:S(2)}) copy-start(bf16[512,1024]{1,0:T(8,128)(2,1)} %param.20) | copy-start | bytes 3145732
  0.6 19.9 %copy-start.5 = (f32[512]{0:T(512)S(1)}, f32[512]{0:T(512)}, u32[]{:S(2)}) copy-start(f32[512]{0:T(512)} %param.22) | copy-start | bytes 6148
  0.7 1.6 %collective-permute-start = (bf16[16,256]{1,0:T(8,128)(2,1)}, bf16[16,256]{1,0:T(8,128)(2,1)S(1)}, u32[]{:S(2)}, u32[]{:S(2)}) collective-permute-start(bf16[16,256]{1,0:T(8,128)(2,1)} %param.14), channel_id=1, source_target_pairs={{0,1},{1,0},{2,3},{3,2},{4,5},{5,4},{6,7},{7,6},{8,9},{9,8},{10,11... | collective-permute-start | bytes 24584 | tf_op jit(solution)/shard_map/ppermute | solution.py:10
  9.7 5.6 %collective-permute-start.1 = (bf16[4,3712]{1,0:T(4,128)(2,1)S(1)}, bf16[4,3712]{1,0:T(4,128)(2,1)S(1)}, u32[]{:S(2)}, u32[]{:S(2)}) collective-permute-start(bf16[4,3712]{1,0:T(4,128)(2,1)S(1)} %get-tuple-element.4), channel_id=1, source_target_pairs={{0,2},{2,0},{4,6},{6,4},{1,3},{3,1},{5,7},{7,5},{8,10},{10,8},{12,... | collective-permute-start | bytes 89096 | tf_op jit(solution)/shard_map/ppermute | solution.py:16
  12.6 5.7 %collective-permute-start.3 = (bf16[4,3712]{1,0:T(4,128)(2,1)S(1)}, bf16[4,3712]{1,0:T(4,128)(2,1)S(1)}, u32[]{:S(2)}, u32[]{:S(2)}) collective-permute-start(bf16[4,3712]{1,0:T(4,128)(2,1)S(1)} %get-tuple-element.5), channel_id=1, source_target_pairs={{0,6},{2,4},{4,2},{6,0},{1,7},{3,5},{5,3},{7,1},{8,14},{10,12},{12... | collective-permute-start | bytes 89096 | tf_op jit(solution)/shard_map/ppermute | solution.py:16
  15.1 5.1 %collective-permute-start.2 = (bf16[4,3712]{1,0:T(4,128)(2,1)S(1)}, bf16[4,3712]{1,0:T(4,128)(2,1)S(1)}, u32[]{:S(2)}, u32[]{:S(2)}) collective-permute-start(bf16[4,3712]{1,0:T(4,128)(2,1)S(1)} %get-tuple-element.6), channel_id=1, source_target_pairs={{0,4},{2,6},{4,0},{6,2},{1,5},{3,7},{5,1},{7,3},{8,12},{10,14},{12... | collective-permute-start | bytes 89096 | tf_op jit(solution)/shard_map/ppermute | solution.py:16
  23.3 2.0 %copy-start.1 = (f32[4,2,256,512]{3,2,1,0:T(8,128)}, f32[4,2,256,512]{3,2,1,0:T(8,128)S(1)}, u32[]{:S(2)}) copy-start(f32[4,2,256,512]{3,2,1,0:T(8,128)S(1)} %multiply_add_fusion) | copy-start | bytes 12582916
  25.3 2.2 %copy-start.6 = (f32[512]{0:T(512)S(1)}, f32[512]{0:T(512)}, u32[]{:S(2)}) copy-start(f32[512]{0:T(512)} %param.23) | copy-start | bytes 6148
  25.3 9.1 %copy-start.2 = (bf16[1024,512]{1,0:T(8,128)(2,1)S(1)}, bf16[1024,512]{1,0:T(8,128)(2,1)}, u32[]{:S(2)}) copy-start(bf16[1024,512]{1,0:T(8,128)(2,1)} %param.24) | copy-start | bytes 3145732
  25.3 10.6 %copy-start.3 = (bf16[16,256]{1,0:T(8,128)(2,1)S(1)}, bf16[16,256]{1,0:T(8,128)(2,1)}, u32[]{:S(2)}) copy-start(bf16[16,256]{1,0:T(8,128)(2,1)} %param.14) | copy-start | bytes 24580
  25.3 18.7 %copy-start.4 = (f32[2048]{0:T(1024)S(1)}, f32[2048]{0:T(1024)}, u32[]{:S(2)}) copy-start(f32[2048]{0:T(1024)} %param.25) | copy-start | bytes 24580
  27.6 5.5 %collective-permute-start.6 = (bf16[4,1024]{1,0:T(4,128)(2,1)S(1)}, bf16[4,1024]{1,0:T(4,128)(2,1)S(1)}, u32[]{:S(2)}, u32[]{:S(2)}) collective-permute-start(bf16[4,1024]{1,0:T(4,128)(2,1)S(1)} %fusion.31), channel_id=1, source_target_pairs={{0,6},{2,4},{4,2},{6,0},{1,7},{3,5},{5,3},{7,1},{8,14},{10,12},{12... | collective-permute-start | bytes 24584 | tf_op jit(solution)/shard_map/ppermute | solution.py:16
  29.1 4.5 %collective-permute-start.5 = (bf16[4,1024]{1,0:T(4,128)(2,1)S(1)}, bf16[4,1024]{1,0:T(4,128)(2,1)S(1)}, u32[]{:S(2)}, u32[]{:S(2)}) collective-permute-start(bf16[4,1024]{1,0:T(4,128)(2,1)S(1)} %fusion.31), channel_id=1, source_target_pairs={{0,4},{2,6},{4,0},{6,2},{1,5},{3,7},{5,1},{7,3},{8,12},{10,14},{12... | collective-permute-start | bytes 24584 | tf_op jit(solution)/shard_map/ppermute | solution.py:16
  29.6 4.1 %collective-permute-start.4 = (bf16[4,1024]{1,0:T(4,128)(2,1)S(1)}, bf16[4,1024]{1,0:T(4,128)(2,1)S(1)}, u32[]{:S(2)}, u32[]{:S(2)}) collective-permute-start(bf16[4,1024]{1,0:T(4,128)(2,1)S(1)} %fusion.31), channel_id=1, source_target_pairs={{0,2},{2,0},{4,6},{6,4},{1,3},{3,1},{5,7},{7,5},{8,10},{10,8},{12,... | collective-permute-start | bytes 24584 | tf_op jit(solution)/shard_map/ppermute | solution.py:16
  34.7 1.2 %collective-permute-start.7 = (bf16[16,512]{1,0:T(8,128)(2,1)S(1)}, bf16[16,512]{1,0:T(8,128)(2,1)S(1)}, u32[]{:S(2)}, u32[]{:S(2)}) collective-permute-start(bf16[16,512]{1,0:T(8,128)(2,1)S(1)} %get-tuple-element.13), channel_id=1, source_target_pairs={{0,1},{1,0},{2,3},{3,2},{4,5},{5,4},{6,7},{7,6},{8,9},{9,8},{10,11... | collective-permute-start | bytes 49160 | tf_op jit(solution)/shard_map/ppermute | solution.py:10
  35.9 5.7 %collective-permute-start.10 = (bf16[16,512]{1,0:T(8,128)(2,1)S(1)}, bf16[16,512]{1,0:T(8,128)(2,1)S(1)}, u32[]{:S(2)}, u32[]{:S(2)}) collective-permute-start(bf16[16,512]{1,0:T(8,128)(2,1)S(1)} %fusion.15), channel_id=1, source_target_pairs={{0,6},{2,4},{4,2},{6,0},{1,7},{3,5},{5,3},{7,1},{8,14},{10,12},{12... | collective-permute-start | bytes 49160 | tf_op jit(solution)/shard_map/ppermute | solution.py:16
  38.3 4.6 %collective-permute-start.9 = (bf16[16,512]{1,0:T(8,128)(2,1)S(1)}, bf16[16,512]{1,0:T(8,128)(2,1)S(1)}, u32[]{:S(2)}, u32[]{:S(2)}) collective-permute-start(bf16[16,512]{1,0:T(8,128)(2,1)S(1)} %fusion.15), channel_id=1, source_target_pairs={{0,4},{2,6},{4,0},{6,2},{1,5},{3,7},{5,1},{7,3},{8,12},{10,14},{12... | collective-permute-start | bytes 49160 | tf_op jit(solution)/shard_map/ppermute | solution.py:16
  39.4 3.7 %collective-permute-start.8 = (bf16[16,512]{1,0:T(8,128)(2,1)S(1)}, bf16[16,512]{1,0:T(8,128)(2,1)S(1)}, u32[]{:S(2)}, u32[]{:S(2)}) collective-permute-start(bf16[16,512]{1,0:T(8,128)(2,1)S(1)} %fusion.15), channel_id=1, source_target_pairs={{0,2},{2,0},{4,6},{6,4},{1,3},{3,1},{5,7},{7,5},{8,10},{10,8},{12,... | collective-permute-start | bytes 49160 | tf_op jit(solution)/shard_map/ppermute | solution.py:16
  49.0 1.3 %collective-permute-start.11 = (bf16[16,4,256]{2,0,1:T(8,128)(2,1)S(1)}, bf16[16,4,256]{2,0,1:T(8,128)(2,1)S(1)}, u32[]{:S(2)}, u32[]{:S(2)}) collective-permute-start(bf16[16,4,256]{2,0,1:T(8,128)(2,1)S(1)} %fusion.16), channel_id=1, source_target_pairs={{0,1},{1,0},{2,3},{3,2},{4,5},{5,4},{6,7},{7,6},{8,9},{9,8},{10,11... | collective-permute-start | bytes 98312 | tf_op jit(solution)/shard_map/ppermute | solution.py:10
  50.3 3.7 %collective-permute-start.12 = (bf16[16,256]{1,0:T(8,128)(2,1)S(1)}, bf16[16,256]{1,0:T(8,128)(2,1)S(1)}, u32[]{:S(2)}, u32[]{:S(2)}) collective-permute-start(bf16[16,256]{1,0:T(8,128)(2,1)S(1)} %get-tuple-element.10), channel_id=1, source_target_pairs={{0,2},{2,0},{4,6},{6,4},{1,3},{3,1},{5,7},{7,5},{8,10},{10,8},{12,... | collective-permute-start | bytes 24584 | tf_op jit(solution)/shard_map/ppermute | solution.py:16
  51.3 5.4 %collective-permute-start.14 = (bf16[16,256]{1,0:T(8,128)(2,1)S(1)}, bf16[16,256]{1,0:T(8,128)(2,1)S(1)}, u32[]{:S(2)}, u32[]{:S(2)}) collective-permute-start(bf16[16,256]{1,0:T(8,128)(2,1)S(1)} %get-tuple-element.11), channel_id=1, source_target_pairs={{0,6},{2,4},{4,2},{6,0},{1,7},{3,5},{5,3},{7,1},{8,14},{10,12},{12... | collective-permute-start | bytes 24584 | tf_op jit(solution)/shard_map/ppermute | solution.py:16
  53.6 4.5 %collective-permute-start.13 = (bf16[16,256]{1,0:T(8,128)(2,1)S(1)}, bf16[16,256]{1,0:T(8,128)(2,1)S(1)}, u32[]{:S(2)}, u32[]{:S(2)}) collective-permute-start(bf16[16,256]{1,0:T(8,128)(2,1)S(1)} %get-tuple-element.12), channel_id=1, source_target_pairs={{0,4},{2,6},{4,0},{6,2},{1,5},{3,7},{5,1},{7,3},{8,12},{10,14},{12... | collective-permute-start | bytes 24584 | tf_op jit(solution)/shard_map/ppermute | solution.py:16

commit v2 on v1

v2 whole, which is shorter than its diff:
```python
import functools

import jax
import jax.numpy as jnp
from jax import lax
from jax.experimental import pallas as pl
from jax.experimental.pallas import tpu as pltpu
from jax.sharding import PartitionSpec as P


epsilon = 1e-06
bf16, f32 = jnp.bfloat16, jnp.float32
VMEM = pl.BlockSpec(memory_space=pltpu.VMEM)
HEAVY = pl.CostEstimate(flops=2 * 10**10, bytes_accessed=2**20, transcendentals=0)


def swap_cores(value):
    return lax.ppermute(value, "tp", [(0, 1), (1, 0)])


def spread(pieces, kv_size):
    came = []
    for k in range(1, kv_size):
        came.append(lax.ppermute(pieces[k], "kv", [(i, i ^ k) for i in range(kv_size)]))
    return [pieces[0]] + came


def here():
    return lax.axis_index("kv"), lax.axis_index("tp")


def aligned(start, step):
    return pl.multiple_of(start * step, step)


def clear_kernel(squares_ref):
    squares_ref[...] = jnp.zeros_like(squares_ref)


def project_kernel(squares_ref, own_ref, other_ref, gain_ref, *refs):
    *weights, total = refs
    weights, outs = weights[:5], weights[5:]
    count = len(outs)
    seqs = outs[0].shape[0]
    me, core = here()
    half = other_ref.shape[1]
    own, other = own_ref[...].astype(f32), other_ref[...].astype(f32)
    squares = squares_ref[...] + (
        jnp.sum(own * own, axis=1, keepdims=True) + jnp.sum(other * other, axis=1, keepdims=True))
    high = squares.astype(bf16).astype(f32)
    own_scaled = (own * gain_ref[:, pl.ds(aligned(core, half), half)]).astype(bf16)
    other_scaled = (other * gain_ref[:, pl.ds(aligned(1 - core, half), half)]).astype(bf16)
    own_rows, other_rows = pl.ds(aligned(core, half), half), pl.ds(aligned(1 - core, half), half)
    start = 0
    blocks = [
        jnp.dot(own_scaled, w[own_rows, :], preferred_element_type=f32)
        + jnp.dot(other_scaled, w[other_rows, :], preferred_element_type=f32)
        for w in weights
    ] + [high, squares - high]
    for block in blocks:
        for d in range(count):
            total[d, :, start: start + block.shape[1]] = block[d * seqs: (d + 1) * seqs]
        start += block.shape[1]
    for k, out in zip(range(count - 1, -1, -1), outs):
        out[...] = total[me ^ k].astype(out.dtype)


def project(squares, tokens, other, mix_gain, weights, kv_size):
    seqs = other.shape[0] // kv_size
    width = sum(w.shape[1] for w in weights) + 256
    outs = [jax.ShapeDtypeStruct((seqs, width), f32 if k == 0 else bf16) for k in range(kv_size - 1, -1, -1)]
    return pl.pallas_call(
        project_kernel,
        out_shape=outs,
        in_specs=[VMEM] * (4 + len(weights)),
        out_specs=[VMEM] * kv_size,
        scratch_shapes=[pltpu.VMEM((kv_size, seqs, width), f32)],
        compiler_params=pltpu.CompilerParams(vmem_limit_bytes=8 * 2**20),
        cost_estimate=HEAVY,
        name="project",
    )(squares, tokens, other, mix_gain.reshape(1, -1), *weights)[::-1]


def readout_kernel(kv_size, depth, *refs):
    parts = refs[:kv_size]
    state_ref, offset_ref, gain_ref, gated_ref, columns_ref, values_ref = refs[kv_size:]
    seqs, heads, keys, vals = state_ref.shape
    kw, vw = heads * keys, heads * vals
    base = 3 * kw + 2 * vw

    def summed(start, width):
        return sum(p[:, start: start + width].astype(f32) for p in parts)

    sums = summed(base, 128)[:, :1] + summed(base + 128, 128)[:, :1]
    row_scale = lax.rsqrt(sums / depth + epsilon)
    queries = summed(0, kw) * row_scale * keys ** (-0.5)
    new_keys = summed(kw, kw) * row_scale
    retain = jax.nn.sigmoid(summed(2 * kw, kw) * row_scale + offset_ref[...])
    values = summed(3 * kw, vw) * row_scale
    gates = summed(3 * kw + vw, vw) * row_scale
    values_ref[...] = values
    fill = jnp.zeros((-3 * seqs % 8, kw), f32)
    columns = jnp.concatenate([queries * retain, retain, new_keys] + ([fill] if fill.shape[0] else []), axis=0).T
    columns_ref[...] = columns
    silu = gates * jax.nn.sigmoid(gates)
    for h in range(heads):
        qk = jnp.sum(queries[:, h * keys: (h + 1) * keys] * new_keys[:, h * keys: (h + 1) * keys], axis=1,
                     keepdims=True)
        reads = []
        for b in range(seqs):
            weight = columns[h * keys: (h + 1) * keys, b: b + 1]
            reads.append(jnp.sum(weight * state_ref[b, h], axis=0, keepdims=True))
        read = jnp.concatenate(reads, axis=0) + qk * values[:, h * vals: (h + 1) * vals]
        read = read * lax.rsqrt(jnp.mean(read * read, axis=1, keepdims=True) + epsilon) * gain_ref[...]
        gated_ref[:, h * vals: (h + 1) * vals] = (read * silu[:, h * vals: (h + 1) * vals]).astype(bf16)


def readout(parts, state, decay_offset, head_gain, depth):
    seqs, heads, keys, vals = state.shape
    height = 3 * seqs + (-3 * seqs % 8)
    outs = [
        jax.ShapeDtypeStruct((seqs, heads * vals), bf16),
        jax.ShapeDtypeStruct((heads * keys, height), f32),
        jax.ShapeDtypeStruct((seqs, heads * vals), f32),
    ]
    return pl.pallas_call(
        functools.partial(readout_kernel, len(parts), depth),
        out_shape=outs,
        in_specs=[VMEM] * (len(parts) + 3),
        out_specs=[VMEM] * 3,
        compiler_params=pltpu.CompilerParams(vmem_limit_bytes=12 * 2**20),
        cost_estimate=HEAVY,
        name="readout",
    )(*parts, state, decay_offset.reshape(1, -1), head_gain.reshape(1, -1))


def update_kernel(columns_ref, values_ref, state_ref, out_ref):
    seqs = values_ref.shape[0]
    b, h = pl.program_id(0), pl.program_id(1)
    keys, vals = out_ref.shape[2:]
    block = columns_ref[pl.ds(aligned(h, keys), keys), :]
    lanes = lax.broadcasted_iota(jnp.int32, (1, block.shape[1]), 1)
    keep = jnp.sum(jnp.where(lanes == seqs + b, block, 0.0), axis=1, keepdims=True)
    key = jnp.sum(jnp.where(lanes == 2 * seqs + b, block, 0.0), axis=1, keepdims=True)
    value = values_ref[pl.ds(b, 1), pl.ds(aligned(h, vals), vals)]
    out_ref[0, 0] = keep * state_ref[0, 0] + key * value


def update(columns, values, state):
    seqs, heads, keys, vals = state.shape
    tile = pl.BlockSpec((1, 1, keys, vals), lambda b, h: (b, h, 0, 0))
    return pl.pallas_call(
        update_kernel,
        out_shape=jax.ShapeDtypeStruct(state.shape, f32),
        grid=(seqs, heads),
        in_specs=[VMEM, VMEM, tile],
        out_specs=tile,
        compiler_params=pltpu.CompilerParams(vmem_limit_bytes=8 * 2**20),
        cost_estimate=HEAVY,
        name="update",
    )(columns, values, state)


def branch_kernel(*refs):
    *parts, w_ref, keep_ref, send_ref, rows = refs
    me, _ = here()
    for k, part in enumerate(parts):
        rows[me ^ k] = part[...].astype(f32)
    gated = jnp.concatenate([rows[d] for d in range(len(parts))], axis=0).astype(bf16)
    branch = jnp.dot(gated, w_ref[...], preferred_element_type=f32)
    keep_ref[...] = branch
    send_ref[...] = branch.astype(bf16)


def branch_of(parts, w_out):
    rows = parts[0].shape[0] * len(parts)
    outs = [jax.ShapeDtypeStruct((rows, w_out.shape[1]), kind) for kind in (f32, bf16)]
    return pl.pallas_call(
        branch_kernel,
        out_shape=outs,
        in_specs=[VMEM] * (len(parts) + 1),
        out_specs=[VMEM] * 2,
        scratch_shapes=[pltpu.VMEM((len(parts), *parts[0].shape), f32)],
        compiler_params=pltpu.CompilerParams(vmem_limit_bytes=4 * 2**20),
        cost_estimate=HEAVY,
        name="branch",
    )(*parts, w_out)


def mixer_kernel(*refs):
    *parts, gain_ref, up_ref, down_ref, keep_ref, give_ref, total = refs
    me, core = here()
    width = parts[0].shape[1]
    depth = width * len(parts)
    own = width // 2
    squares, hidden = 0.0, 0.0
    for k, part in enumerate(parts):
        owner = me ^ k
        stream = part[...].astype(f32)
        squares += jnp.sum(stream * stream, axis=1, keepdims=True)
        normed = (stream * gain_ref[:, pl.ds(aligned(owner, width), width)]).astype(bf16)
        hidden += jnp.dot(normed, up_ref[pl.ds(aligned(owner, width), width), :], preferred_element_type=f32)
    hidden = hidden * lax.rsqrt(squares / depth + epsilon)
    squared = jnp.square(jnp.maximum(hidden, 0.0)).astype(bf16)
    total[...] = jnp.dot(squared, down_ref[...], preferred_element_type=f32)
    for d in range(len(parts)):
        keep_ref[d] = total[:, pl.ds(aligned(2 * d + core, own), own)]
        give_ref[d] = total[:, pl.ds(aligned(2 * d + 1 - core, own), own)].astype(bf16)


def mixer(parts, mlp_gain, w_up, w_down):
    rows, width = parts[0].shape
    outs = [jax.ShapeDtypeStruct((len(parts), rows, width // 2), kind) for kind in (f32, bf16)]
    return pl.pallas_call(
        mixer_kernel,
        out_shape=outs,
        in_specs=[VMEM] * (len(parts) + 3),
        out_specs=[VMEM] * 2,
        scratch_shapes=[pltpu.VMEM((rows, w_down.shape[1]), f32)],
        compiler_params=pltpu.CompilerParams(vmem_limit_bytes=16 * 2**20),
        cost_estimate=HEAVY,
        name="mixer",
    )(*parts, mlp_gain.reshape(1, -1), w_up, w_down)


def stream_kernel(branch_ref, came_ref, own_ref, other_ref, stream_ref):
    _, core = here()
    half = own_ref.shape[1]
    for ref, side in ((own_ref, core), (other_ref, 1 - core)):
        at = pl.ds(aligned(side, half), half)
        total = branch_ref[:, at] + came_ref[:, at].astype(f32)
        stream_ref[:, at] = (ref[...].astype(f32) + total).astype(bf16)


def pair_kernel(keep_ref, came_ref, *outs):
    me, _ = here()
    for k, out in zip(range(len(outs) - 1, -1, -1), outs):
        out[...] = (keep_ref[me ^ k] + came_ref[me ^ k].astype(f32)).astype(out.dtype)


def last_kernel(stream_ref, *refs):
    *parts, out_ref = refs
    _, core = here()
    half = out_ref.shape[1]
    total = sum(p[...].astype(f32) for p in parts)
    out_ref[...] = (stream_ref[:, pl.ds(aligned(core, half), half)].astype(f32) + total).astype(bf16)


def small(body, outs, *args):
    return pl.pallas_call(
        body,
        out_shape=outs,
        in_specs=[VMEM] * len(args),
        out_specs=jax.tree.map(lambda _: VMEM, outs),
        compiler_params=pltpu.CompilerParams(vmem_limit_bytes=2 * 2**20),
        cost_estimate=HEAVY,
    )(*args)


def fused_steps(kv_size, tokens, state, mix_gain, weights, decay_offset, head_gain, w_out, mlp_gain, w_up, w_down):
    rows, half = tokens.shape
    depth = 2 * half * kv_size
    like = jax.ShapeDtypeStruct
    other = swap_cores(tokens)
    squares = small(clear_kernel, like((rows, 128), f32))
    parts = spread(project(squares, tokens, other, mix_gain, weights, kv_size), kv_size)
    gated, columns, values = readout(parts, state, decay_offset, head_gain, depth)
    arrived = spread([gated] * kv_size, kv_size)
    new_state = update(columns, values, state)
    branch, branch_sent = branch_of(arrived, w_out)
    stream = small(stream_kernel, like((rows, 2 * half), bf16), branch, swap_cores(branch_sent), tokens, other)
    keep, give = mixer(spread([stream] * kv_size, kv_size), mlp_gain, w_up, w_down)
    outs = [like((rows, half), f32 if k == 0 else bf16) for k in range(kv_size - 1, -1, -1)]
    pieces = spread(small(pair_kernel, outs, keep, swap_cores(give))[::-1], kv_size)
    return small(last_kernel, like((rows, half), bf16), stream, *pieces), new_state


def plain_steps(kv_size, tokens, state, mix_gain, weights, decay_offset, head_gain, w_out, mlp_gain, w_up, w_down):
    seqs, heads, keys, vals = state.shape
    rows, half = tokens.shape
    depth = 2 * half * kv_size
    core = lax.axis_index("tp")

    def exchange(blocks):
        return lax.all_to_all(blocks, "kv", 0, 0, tiled=True)

    def pick(pair):
        return jnp.where(core == 0, pair[0], pair[1]), jnp.where(core == 0, pair[1], pair[0])

    other = swap_cores(tokens)
    tok = jnp.concatenate(pick((tokens, other)), axis=1).astype(f32)
    squares = jnp.sum(tok * tok, axis=1, keepdims=True)
    scaled = (tok * mix_gain).astype(bf16)
    high = squares.astype(bf16).astype(f32)
    total = jnp.concatenate([jnp.dot(scaled, w, preferred_element_type=f32) for w in weights]
                            + [jnp.broadcast_to(x, (rows, 128)) for x in (high, squares - high)], axis=1)
    came = exchange(total.astype(bf16).reshape(kv_size, seqs, -1))
    total = jnp.sum(came.astype(f32), axis=0)
    kw, vw = heads * keys, heads * vals
    sums = total[:, 3 * kw + 2 * vw] + total[:, 3 * kw + 2 * vw + 128]
    total = total * lax.rsqrt(sums / depth + epsilon)[:, None]
    queries = (total[:, :kw] * keys ** (-0.5)).reshape(seqs, heads, keys)
    new_keys = total[:, kw: 2 * kw].reshape(seqs, heads, keys)
    retain = jax.nn.sigmoid(total[:, 2 * kw: 3 * kw] + decay_offset).reshape(seqs, heads, keys)
    values = total[:, 3 * kw: 3 * kw + vw].reshape(seqs, heads, vals)
    gates = total[:, 3 * kw + vw: 3 * kw + 2 * vw]
    new_state = retain[..., None] * state + new_keys[..., None] * values[:, :, None, :]
    read = jnp.einsum("bhk,bhkv->bhv", queries, new_state, precision=lax.Precision.HIGHEST)
    read = read * lax.rsqrt(jnp.mean(read * read, axis=2, keepdims=True) + epsilon) * head_gain
    gated = (read.reshape(seqs, vw) * jax.nn.silu(gates)).astype(bf16)
    gated = lax.all_gather(gated, "kv", axis=0, tiled=True)
    branch = jnp.dot(gated, w_out, preferred_element_type=f32)
    branch = branch + swap_cores(branch.astype(bf16)).astype(f32)
    stream_cols = (tok + branch).astype(bf16)
    stream = lax.all_gather(stream_cols, "kv", axis=1, tiled=True).astype(f32)
    scale = lax.rsqrt(jnp.mean(stream * stream, axis=1, keepdims=True) + epsilon)
    normed = (stream * mlp_gain).astype(bf16)
    hidden = jnp.dot(normed, w_up, preferred_element_type=f32) * scale
    squared = jnp.square(jax.nn.relu(hidden)).astype(bf16)
    down = jnp.dot(squared, w_down, preferred_element_type=f32)
    keep, give = pick(down.reshape(rows, kv_size, 2, half).transpose(2, 1, 0, 3))
    pair = keep + swap_cores(give.astype(bf16)).astype(f32)
    down_own = jnp.sum(exchange(pair.astype(bf16)).astype(f32), axis=0)
    stream_own, _ = pick((stream_cols[:, :half], stream_cols[:, half:]))
    return (stream_own.astype(f32) + down_own).astype(bf16), new_state


def shards(kv_size, tokens, state, mix_gain, w_query, w_key, w_decay, w_value, w_gate, *rest):
    steps = fused_steps if tokens.shape[1] % 128 == 0 and kv_size in (2, 4, 8) else plain_steps
    return steps(kv_size, tokens, state, mix_gain, (w_query, w_key, w_decay, w_value, w_gate), *rest)


def solution(mesh):
    kv_size = mesh.shape["kv"]
    in_specs = (
        P("dp", ("kv", "tp")),
        P(("dp", "kv"), "tp", None, None),
        P("kv"),
        P("kv", "tp"),
        P("kv", "tp"),
        P("kv", "tp"),
        P("kv", "tp"),
        P("kv", "tp"),
        P("tp"),
        P(),
        P("tp", "kv"),
        P(),
        P(None, ("kv", "tp")),
        P(("kv", "tp"), None),
    )
    out_specs = (P("dp", ("kv", "tp")), P(("dp", "kv"), "tp", None, None))

    def body(*args):
        return shards(kv_size, *args)

    return jax.shard_map(body, mesh=mesh, in_specs=in_specs, out_specs=out_specs, check_vma=False)
```

time: 59.2 us -> 42.1 us (0.71)
  matrix products: 13.4 us -> 0 us
  Pallas kernels: 0 us -> 7.67 us
  other arithmetic: 5.03 us -> 0 us
  local copies, waits for them, and re-layouts: 3.83 us -> 0.38 us
  waiting for transfers between devices: 17 us -> 13.6 us
  starting transfers between devices: 18.7 us -> 19.6 us
    dot_general x8 -> x0, matrix products: 13.4 us -> none  [the longest x5 6.39 us: shards(): jnp.dot(scaled, w, preferred_element_type=f32)]
    pallas_call x0 -> x9, Pallas kernels: none -> 7.67 us  [the longest x1 3.96 us: update(): pl.pallas_call(update_kernel, out_shape=jax.ShapeDtypeStruct(state.shape,...]
    ppermute x12, waiting for transfers between devices: 13.6 us -> 10.2 us  [spread(): lax.ppermute(pieces[k], 'kv', [(i, i ^ k) for i in range(kv_size)])]
    add x2 -> x0, other arithmetic: 2.64 us -> none  [the longest x1 2.6 us: shards(): retain[..., None] * state + new_keys[..., None] * values[:, :, None, :]]
    unnamed x15 -> x28, local copies, waits for them, and re-layouts: 2.04 us -> 0.38 us
    reduce_sum x3 -> x0, other arithmetic: 1.19 us -> none  [the longest x1 0.89 us: shards(): squares = jnp.sum(tok_float * tok_float, axis=1, keepdims=True)]
    gather x3 -> x0, local copies, waits for them, and re-layouts: 1.15 us -> none  [the longest x2 0.6 us: shards(): jnp.take(jnp.stack(arrived), order, axis=0).reshape(kv_size * seq_dev, vw)]
    ppermute x12, starting transfers between devices: 18 us -> 19 us  [spread(): lax.ppermute(pieces[k], 'kv', [(i, i ^ k) for i in range(kv_size)])]
  transfers between devices with their start and end apart: 15 -> 15, of which waited for: 14 -> 10; matrix products, arithmetic and copies ran while one was open for 0% -> 0% of each run, Pallas kernels for 0% -> 9%
where the time goes in v2:
time: 42.1 us; the launch traced here: 42 us
  starting transfers between devices  19.6 us (47%)
  waiting for transfers between devices  13.6 us (32%)
  Pallas kernels  7.67 us (18%)
  between operations  0.76 us (2%)
    ppermute x12, starting transfers between devices, spread(): lax.ppermute(pieces[k], 'kv', [(i, i ^ k) for i in range(kv_size)])  19 us
    ppermute x12, waiting for transfers between devices, spread(): lax.ppermute(pieces[k], 'kv', [(i, i ^ k) for i in range(kv_size)])  10.2 us
    pallas_call x1, Pallas kernels, update(): pl.pallas_call(update_kernel, out_shape=jax.ShapeDtypeStruct(state.shape,...  3.96 us
    ppermute x3, waiting for transfers between devices, swap_cores(): return lax.ppermute(value, 'tp', [(0, 1), (1, 0)])  3.43 us
    pallas_call x1, Pallas kernels, mixer(): pl.pallas_call(mixer_kernel, out_shape=outs, in_specs=[VMEM] * (len(parts...  1.24 us
    pallas_call x1, Pallas kernels, readout(): pl.pallas_call(functools.partial(readout_kernel, len(parts), depth), out_...  0.96 us
  transfers between devices with their start and end apart: 15, of which 10 were waited for; matrix products, arithmetic and copies ran while one was open for 0% of the time, Pallas kernels for 9%

profile of v2, /device:TPU:0, one launch (start us, length us, event | category | flops | bytes accessed | tf_op | source)
XLA Modules:
  0.0 42.0 jit_solution(3230313663088674354)
XLA Ops:
  0.7 0.6 %collective-permute-start = (bf16[16,256]{1,0:T(8,128)(2,1)}, bf16[16,256]{1,0:T(8,128)(2,1)S(1)}, u32[]{:S(2)}, u32[]{:S(2)}) collective-permute-start(bf16[16,256]{1,0:T(8,128)(2,1)} %own_ref.3), channel_id=1, source_target_pairs={{0,1},{1,0},{2,3},{3,2},{4,5},{5,4},{6,7},{7,6},{8,9},{9,8},{10,11... | collective-permute-start | bytes 24584 | tf_op jit(solution)/shard_map/ppermute | solution.py:18
  1.3 1.0 %collective-permute-done.other_ref = bf16[16,256]{1,0:T(8,128)(2,1)S(1)} collective-permute-done((bf16[16,256]{1,0:T(8,128)(2,1)}, bf16[16,256]{1,0:T(8,128)(2,1)S(1)}, u32[]{:S(2)}, u32[]{:S(2)}) %collective-permute-start) | collective-permute-done | bytes 8224 | tf_op jit(solution)/shard_map/ppermute | solution.py:18
  2.6 0.6 %project.1 = (bf16[4,3840]{1,0:T(4,128)(2,1)S(1)}, bf16[4,3840]{1,0:T(4,128)(2,1)S(1)}, bf16[4,3840]{1,0:T(4,128)(2,1)S(1)}, f32[4,3840]{1,0:T(4,128)S(1)}) custom-call(f32[16,128]{1,0:T(8,128)S(1)} %shard_map.149.squares_ref, bf16[16,256]{1,0:T(8,128)(2,1)S(1)} %copy-done.9, bf16[16,256]{1,0:T(8,128)(2,1)S(1)} %collective-permute-done.other_ref, ...), custom_call_target="tpu_custom_call" | custom-call | flops 20000000000 | bytes 1048576 | tf_op jit(solution)/shard_map/project/pallas_call | solution.py:72
  3.3 3.1 %collective-permute-start.1 = (bf16[4,3840]{1,0:T(4,128)(2,1)S(1)}, bf16[4,3840]{1,0:T(4,128)(2,1)S(1)}, u32[]{:S(2)}, u32[]{:S(2)}) collective-permute-start(bf16[4,3840]{1,0:T(4,128)(2,1)S(1)} %get-tuple-element.18), channel_id=1, source_target_pairs={{0,2},{2,0},{4,6},{6,4},{1,3},{3,1},{5,7},{7,5},{8,10},{10,8},{12,... | collective-permute-start | bytes 92168 | tf_op jit(solution)/shard_map/ppermute | solution.py:24
  6.4 2.6 %collective-permute-start.2 = (bf16[4,3840]{1,0:T(4,128)(2,1)S(1)}, bf16[4,3840]{1,0:T(4,128)(2,1)S(1)}, u32[]{:S(2)}, u32[]{:S(2)}) collective-permute-start(bf16[4,3840]{1,0:T(4,128)(2,1)S(1)} %get-tuple-element.19), channel_id=1, source_target_pairs={{0,4},{2,6},{4,0},{6,2},{1,5},{3,7},{5,1},{7,3},{8,12},{10,14},{12... | collective-permute-start | bytes 92168 | tf_op jit(solution)/shard_map/ppermute | solution.py:24
  9.0 2.7 %collective-permute-done.2.refs_2_ = bf16[4,3840]{1,0:T(4,128)(2,1)S(1)} collective-permute-done((bf16[4,3840]{1,0:T(4,128)(2,1)S(1)}, bf16[4,3840]{1,0:T(4,128)(2,1)S(1)}, u32[]{:S(2)}, u32[]{:S(2)}) %collective-permute-start.2) | collective-permute-done | bytes 30752 | tf_op jit(solution)/shard_map/ppermute | solution.py:24
  11.7 3.0 %collective-permute-done.3.refs_3_ = bf16[4,3840]{1,0:T(4,128)(2,1)S(1)} collective-permute-done((bf16[4,3840]{1,0:T(4,128)(2,1)S(1)}, bf16[4,3840]{1,0:T(4,128)(2,1)S(1)}, u32[]{:S(2)}, u32[]{:S(2)}) %collective-permute-start.3) | collective-permute-done | bytes 30752 | tf_op jit(solution)/shard_map/ppermute | solution.py:24
  14.7 1.0 %readout.1 = (bf16[4,1024]{1,0:T(4,128)(2,1)S(1)}, f32[512,16]{1,0:T(8,128)S(1)}, f32[4,1024]{1,0:T(4,128)S(1)}) custom-call(f32[4,3840]{1,0:T(4,128)S(1)} %get-tuple-element.17.refs_0_, bf16[4,3840]{1,0:T(4,128)(2,1)S(1)} %collective-permute-done.1.refs_1_, bf16[4,3840]{1,0:T(4,128)(2,1)S(1)} %collective-permute-done.2.refs_2_, ...), custom_call_target="tpu_custom_call" | custom-call | flops 20000000000 | bytes 1048576 | tf_op jit(solution)/shard_map/readout/pallas_call | solution.py:126
  16.1 3.9 %collective-permute-start.4 = (bf16[4,1024]{1,0:T(4,128)(2,1)S(1)}, bf16[4,1024]{1,0:T(4,128)(2,1)S(1)}, u32[]{:S(2)}, u32[]{:S(2)}) collective-permute-start(bf16[4,1024]{1,0:T(4,128)(2,1)S(1)} %get-tuple-element.21.refs_0_), channel_id=1, source_target_pairs={{0,2},{2,0},{4,6},{6,4},{1,3},{3,1},{5,7},{7,5},{8,10},{10,8},{12,... | collective-permute-start | bytes 24584 | tf_op jit(solution)/shard_map/ppermute | solution.py:24
  20.1 1.1 %collective-permute-done.6.refs_3_ = bf16[4,1024]{1,0:T(4,128)(2,1)S(1)} collective-permute-done((bf16[4,1024]{1,0:T(4,128)(2,1)S(1)}, bf16[4,1024]{1,0:T(4,128)(2,1)S(1)}, u32[]{:S(2)}, u32[]{:S(2)}) %collective-permute-start.6) | collective-permute-done | bytes 8224 | tf_op jit(solution)/shard_map/ppermute | solution.py:24
  21.1 0.6 %collective-permute-done.4.refs_1_ = bf16[4,1024]{1,0:T(4,128)(2,1)S(1)} collective-permute-done((bf16[4,1024]{1,0:T(4,128)(2,1)S(1)}, bf16[4,1024]{1,0:T(4,128)(2,1)S(1)}, u32[]{:S(2)}, u32[]{:S(2)}) %collective-permute-start.4) | collective-permute-done | bytes 8224 | tf_op jit(solution)/shard_map/ppermute | solution.py:24
  21.9 1.2 %collective-permute-done.7.came_ref = bf16[16,512]{1,0:T(8,128)(2,1)S(1)} collective-permute-done((bf16[16,512]{1,0:T(8,128)(2,1)S(1)}, bf16[16,512]{1,0:T(8,128)(2,1)S(1)}, u32[]{:S(2)}, u32[]{:S(2)}) %collective-permute-start.7) | collective-permute-done | bytes 16416 | tf_op jit(solution)/shard_map/ppermute | solution.py:18
  23.2 2.4 %collective-permute-start.10 = (bf16[16,512]{1,0:T(8,128)(2,1)S(1)}, bf16[16,512]{1,0:T(8,128)(2,1)S(1)}, u32[]{:S(2)}, u32[]{:S(2)}) collective-permute-start(bf16[16,512]{1,0:T(8,128)(2,1)S(1)} %shard_map.150.refs_0_.stream_ref), channel_id=1, source_target_pairs={{0,6},{2,4},{4,2},{6,0},{1,7},{3,5},{5,3},{7,1},{8,14},{10,12},{12... | collective-permute-start | bytes 49160 | tf_op jit(solution)/shard_map/ppermute | solution.py:24
  25.6 1.1 %collective-permute-start.9 = (bf16[16,512]{1,0:T(8,128)(2,1)S(1)}, bf16[16,512]{1,0:T(8,128)(2,1)S(1)}, u32[]{:S(2)}, u32[]{:S(2)}) collective-permute-start(bf16[16,512]{1,0:T(8,128)(2,1)S(1)} %shard_map.150.refs_0_.stream_ref), channel_id=1, source_target_pairs={{0,4},{2,6},{4,0},{6,2},{1,5},{3,7},{5,1},{7,3},{8,12},{10,14},{12... | collective-permute-start | bytes 49160 | tf_op jit(solution)/shard_map/ppermute | solution.py:24
  26.7 0.9 %collective-permute-start.8 = (bf16[16,512]{1,0:T(8,128)(2,1)S(1)}, bf16[16,512]{1,0:T(8,128)(2,1)S(1)}, u32[]{:S(2)}, u32[]{:S(2)}) collective-permute-start(bf16[16,512]{1,0:T(8,128)(2,1)S(1)} %shard_map.150.refs_0_.stream_ref), channel_id=1, source_target_pairs={{0,2},{2,0},{4,6},{6,4},{1,3},{3,1},{5,7},{7,5},{8,10},{10,8},{12,... | collective-permute-start | bytes 49160 | tf_op jit(solution)/shard_map/ppermute | solution.py:24
  27.6 1.2 %collective-permute-done.10.refs_3_ = bf16[16,512]{1,0:T(8,128)(2,1)S(1)} collective-permute-done((bf16[16,512]{1,0:T(8,128)(2,1)S(1)}, bf16[16,512]{1,0:T(8,128)(2,1)S(1)}, u32[]{:S(2)}, u32[]{:S(2)}) %collective-permute-start.10) | collective-permute-done | bytes 16416 | tf_op jit(solution)/shard_map/ppermute | solution.py:24
  28.8 1.5 %collective-permute-done.9.refs_2_ = bf16[16,512]{1,0:T(8,128)(2,1)S(1)} collective-permute-done((bf16[16,512]{1,0:T(8,128)(2,1)S(1)}, bf16[16,512]{1,0:T(8,128)(2,1)S(1)}, u32[]{:S(2)}, u32[]{:S(2)}) %collective-permute-start.9) | collective-permute-done | bytes 16416 | tf_op jit(solution)/shard_map/ppermute | solution.py:24
  30.5 1.2 %mixer.1 = (f32[4,16,256]{2,1,0:T(8,128)S(1)}, bf16[4,16,256]{2,1,0:T(8,128)(2,1)S(1)}) custom-call(bf16[16,512]{1,0:T(8,128)(2,1)S(1)} %shard_map.150.refs_0_.stream_ref, bf16[16,512]{1,0:T(8,128)(2,1)S(1)} %collective-permute-done.8.refs_1_, bf16[16,512]{1,0:T(8,128)(2,1)S(1)} %collective-permute-done.9.refs_2_, ...), custom_call_target="tpu_custom_call" | custom-call | flops 20000000000 | bytes 1048576 | tf_op jit(solution)/shard_map/mixer/pallas_call | solution.py:214
  31.7 1.2 %collective-permute-done.11.came_ref = bf16[4,16,256]{2,1,0:T(8,128)(2,1)S(1)} collective-permute-done((bf16[4,16,256]{2,1,0:T(8,128)(2,1)S(1)}, bf16[4,16,256]{2,1,0:T(8,128)(2,1)S(1)}, u32[]{:S(2)}, u32[]{:S(2)}) %collective-permute-start.11) | collective-permute-done | bytes 32800 | tf_op jit(solution)/shard_map/ppermute | solution.py:18
  32.9 1.0 %collective-permute-start.12 = (bf16[16,256]{1,0:T(8,128)(2,1)S(1)}, bf16[16,256]{1,0:T(8,128)(2,1)S(1)}, u32[]{:S(2)}, u32[]{:S(2)}) collective-permute-start(bf16[16,256]{1,0:T(8,128)(2,1)S(1)} %get-tuple-element.27), channel_id=1, source_target_pairs={{0,2},{2,0},{4,6},{6,4},{1,3},{3,1},{5,7},{7,5},{8,10},{10,8},{12,... | collective-permute-start | bytes 24584 | tf_op jit(solution)/shard_map/ppermute | solution.py:24
  33.9 1.1 %collective-permute-start.13 = (bf16[16,256]{1,0:T(8,128)(2,1)S(1)}, bf16[16,256]{1,0:T(8,128)(2,1)S(1)}, u32[]{:S(2)}, u32[]{:S(2)}) collective-permute-start(bf16[16,256]{1,0:T(8,128)(2,1)S(1)} %get-tuple-element.28), channel_id=1, source_target_pairs={{0,4},{2,6},{4,0},{6,2},{1,5},{3,7},{5,1},{7,3},{8,12},{10,14},{12... | collective-permute-start | bytes 24584 | tf_op jit(solution)/shard_map/ppermute | solution.py:24
  35.0 2.4 %collective-permute-start.14 = (bf16[16,256]{1,0:T(8,128)(2,1)S(1)}, bf16[16,256]{1,0:T(8,128)(2,1)S(1)}, u32[]{:S(2)}, u32[]{:S(2)}) collective-permute-start(bf16[16,256]{1,0:T(8,128)(2,1)S(1)} %get-tuple-element.29), channel_id=1, source_target_pairs={{0,6},{2,4},{4,2},{6,0},{1,7},{3,5},{5,3},{7,1},{8,14},{10,12},{12... | collective-permute-start | bytes 24584 | tf_op jit(solution)/shard_map/ppermute | solution.py:24
  37.4 4.0 %update.1 = f32[4,2,256,512]{3,2,1,0:T(8,128)} custom-call(f32[512,16]{1,0:T(8,128)S(1)} %get-tuple-element.30.columns_ref, f32[4,1024]{1,0:T(4,128)S(1)} %get-tuple-element.31.values_ref, f32[4,2,256,512]{3,2,1,0:T(8,128)S(1)} %copy-done.2), custom_call_target="tpu_custom_call" | custom-call | flops 20000000000 | bytes 1048576 | tf_op jit(solution)/shard_map/update/pallas_call | solution.py:152
  41.4 0.6 %shard_map.152 = bf16[16,256]{1,0:T(8,128)(2,1)} custom-call(bf16[16,512]{1,0:T(8,128)(2,1)S(1)} %shard_map.150.refs_0_.stream_ref, f32[16,256]{1,0:T(8,128)S(1)} %get-tuple-element.26.refs_0_, bf16[16,256]{1,0:T(8,128)(2,1)S(1)} %collective-permute-done.12.refs_1_, bf16[16,256]{1,0:T(8,128)(2,1)S(1)} %collective-permute-done.13.refs_2_, ...), custom_call_target="tpu_custom_call" | custom-call | flops 20000000000 | bytes 1048576 | tf_op jit(solution)/shard_map/pallas_call | solution.py:250
  (43 shorter events, 1.3 us)
Async XLA Ops:
  0.7 2.0 %copy-start.6 = (bf16[512,512]{1,0:T(8,128)(2,1)S(1)}, bf16[512,512]{1,0:T(8,128)(2,1)}, u32[]{:S(2)}) copy-start(bf16[512,512]{1,0:T(8,128)(2,1)} %refs_0_.1) | copy-start | bytes 1572868
  0.7 1.9 %copy-start.11 = (f32[512]{0:T(512)S(1)}, f32[512]{0:T(512)}, u32[]{:S(2)}) copy-start(f32[512]{0:T(512)} %param.16) | copy-start | bytes 6148
  0.7 1.6 %collective-permute-start = (bf16[16,256]{1,0:T(8,128)(2,1)}, bf16[16,256]{1,0:T(8,128)(2,1)S(1)}, u32[]{:S(2)}, u32[]{:S(2)}) collective-permute-start(bf16[16,256]{1,0:T(8,128)(2,1)} %own_ref.3), channel_id=1, source_target_pairs={{0,1},{1,0},{2,3},{3,2},{4,5},{5,4},{6,7},{7,6},{8,9},{9,8},{10,11... | collective-permute-start | bytes 24584 | tf_op jit(solution)/shard_map/ppermute | solution.py:18
  2.6 12.1 %copy-start.2 = (f32[4,2,256,512]{3,2,1,0:T(8,128)S(1)}, f32[4,2,256,512]{3,2,1,0:T(8,128)}, u32[]{:S(2)}) copy-start(f32[4,2,256,512]{3,2,1,0:T(8,128)} %state_ref.1) | copy-start | bytes 12582916
  2.6 12.1 %copy-start.12 = (f32[512]{0:T(512)S(1)}, f32[512]{0:T(512)}, u32[]{:S(2)}) copy-start(f32[512]{0:T(512)} %param.22) | copy-start | bytes 6148
  2.6 12.1 %copy-start.13 = (f32[512]{0:T(512)S(1)}, f32[512]{0:T(512)}, u32[]{:S(2)}) copy-start(f32[512]{0:T(512)} %param.23) | copy-start | bytes 6148
  3.3 5.7 %collective-permute-start.1 = (bf16[4,3840]{1,0:T(4,128)(2,1)S(1)}, bf16[4,3840]{1,0:T(4,128)(2,1)S(1)}, u32[]{:S(2)}, u32[]{:S(2)}) collective-permute-start(bf16[4,3840]{1,0:T(4,128)(2,1)S(1)} %get-tuple-element.18), channel_id=1, source_target_pairs={{0,2},{2,0},{4,6},{6,4},{1,3},{3,1},{5,7},{7,5},{8,10},{10,8},{12,... | collective-permute-start | bytes 92168 | tf_op jit(solution)/shard_map/ppermute | solution.py:24
  6.4 5.3 %collective-permute-start.2 = (bf16[4,3840]{1,0:T(4,128)(2,1)S(1)}, bf16[4,3840]{1,0:T(4,128)(2,1)S(1)}, u32[]{:S(2)}, u32[]{:S(2)}) collective-permute-start(bf16[4,3840]{1,0:T(4,128)(2,1)S(1)} %get-tuple-element.19), channel_id=1, source_target_pairs={{0,4},{2,6},{4,0},{6,2},{1,5},{3,7},{5,1},{7,3},{8,12},{10,14},{12... | collective-permute-start | bytes 92168 | tf_op jit(solution)/shard_map/ppermute | solution.py:24
  9.0 5.7 %collective-permute-start.3 = (bf16[4,3840]{1,0:T(4,128)(2,1)S(1)}, bf16[4,3840]{1,0:T(4,128)(2,1)S(1)}, u32[]{:S(2)}, u32[]{:S(2)}) collective-permute-start(bf16[4,3840]{1,0:T(4,128)(2,1)S(1)} %get-tuple-element.20), channel_id=1, source_target_pairs={{0,6},{2,4},{4,2},{6,0},{1,7},{3,5},{5,3},{7,1},{8,14},{10,12},{12... | collective-permute-start | bytes 92168 | tf_op jit(solution)/shard_map/ppermute | solution.py:24
  14.7 7.0 %copy-start.5 = (bf16[1024,512]{1,0:T(8,128)(2,1)S(1)}, bf16[1024,512]{1,0:T(8,128)(2,1)}, u32[]{:S(2)}) copy-start(bf16[1024,512]{1,0:T(8,128)(2,1)} %refs_4_.5) | copy-start | bytes 3145732
  15.7 5.5 %collective-permute-start.6 = (bf16[4,1024]{1,0:T(4,128)(2,1)S(1)}, bf16[4,1024]{1,0:T(4,128)(2,1)S(1)}, u32[]{:S(2)}, u32[]{:S(2)}) collective-permute-start(bf16[4,1024]{1,0:T(4,128)(2,1)S(1)} %get-tuple-element.21.refs_0_), channel_id=1, source_target_pairs={{0,6},{2,4},{4,2},{6,0},{1,7},{3,5},{5,3},{7,1},{8,14},{10,12},{12... | collective-permute-start | bytes 24584 | tf_op jit(solution)/shard_map/ppermute | solution.py:24
  16.0 5.1 %collective-permute-start.5 = (bf16[4,1024]{1,0:T(4,128)(2,1)S(1)}, bf16[4,1024]{1,0:T(4,128)(2,1)S(1)}, u32[]{:S(2)}, u32[]{:S(2)}) collective-permute-start(bf16[4,1024]{1,0:T(4,128)(2,1)S(1)} %get-tuple-element.21.refs_0_), channel_id=1, source_target_pairs={{0,4},{2,6},{4,0},{6,2},{1,5},{3,7},{5,1},{7,3},{8,12},{10,14},{12... | collective-permute-start | bytes 24584 | tf_op jit(solution)/shard_map/ppermute | solution.py:24
  16.1 5.6 %collective-permute-start.4 = (bf16[4,1024]{1,0:T(4,128)(2,1)S(1)}, bf16[4,1024]{1,0:T(4,128)(2,1)S(1)}, u32[]{:S(2)}, u32[]{:S(2)}) collective-permute-start(bf16[4,1024]{1,0:T(4,128)(2,1)S(1)} %get-tuple-element.21.refs_0_), channel_id=1, source_target_pairs={{0,2},{2,0},{4,6},{6,4},{1,3},{3,1},{5,7},{7,5},{8,10},{10,8},{12,... | collective-permute-start | bytes 24584 | tf_op jit(solution)/shard_map/ppermute | solution.py:24
  21.9 1.2 %collective-permute-start.7 = (bf16[16,512]{1,0:T(8,128)(2,1)S(1)}, bf16[16,512]{1,0:T(8,128)(2,1)S(1)}, u32[]{:S(2)}, u32[]{:S(2)}) collective-permute-start(bf16[16,512]{1,0:T(8,128)(2,1)S(1)} %get-tuple-element.23), channel_id=1, source_target_pairs={{0,1},{1,0},{2,3},{3,2},{4,5},{5,4},{6,7},{7,6},{8,9},{9,8},{10,11... | collective-permute-start | bytes 49160 | tf_op jit(solution)/shard_map/ppermute | solution.py:18
  23.1 7.3 %copy-start = (bf16[2048,1024]{1,0:T(8,128)(2,1)S(1)}, bf16[2048,1024]{1,0:T(8,128)(2,1)}, u32[]{:S(2)}) copy-start(bf16[2048,1024]{1,0:T(8,128)(2,1)} %refs_5_.1) | copy-start | bytes 12582916
  23.1 7.3 %copy-start.1 = (bf16[1024,2048]{1,0:T(8,128)(2,1)S(1)}, bf16[1024,2048]{1,0:T(8,128)(2,1)}, u32[]{:S(2)}) copy-start(bf16[1024,2048]{1,0:T(8,128)(2,1)} %refs_6_.1) | copy-start | bytes 12582916
  23.1 7.3 %copy-start.10 = (f32[2048]{0:T(1024)S(1)}, f32[2048]{0:T(1024)}, u32[]{:S(2)}) copy-start(f32[2048]{0:T(1024)} %param.25) | copy-start | bytes 24580
  23.2 5.6 %collective-permute-start.10 = (bf16[16,512]{1,0:T(8,128)(2,1)S(1)}, bf16[16,512]{1,0:T(8,128)(2,1)S(1)}, u32[]{:S(2)}, u32[]{:S(2)}) collective-permute-start(bf16[16,512]{1,0:T(8,128)(2,1)S(1)} %shard_map.150.refs_0_.stream_ref), channel_id=1, source_target_pairs={{0,6},{2,4},{4,2},{6,0},{1,7},{3,5},{5,3},{7,1},{8,14},{10,12},{12... | collective-permute-start | bytes 49160 | tf_op jit(solution)/shard_map/ppermute | solution.py:24
  25.6 4.6 %collective-permute-start.9 = (bf16[16,512]{1,0:T(8,128)(2,1)S(1)}, bf16[16,512]{1,0:T(8,128)(2,1)S(1)}, u32[]{:S(2)}, u32[]{:S(2)}) collective-permute-start(bf16[16,512]{1,0:T(8,128)(2,1)S(1)} %shard_map.150.refs_0_.stream_ref), channel_id=1, source_target_pairs={{0,4},{2,6},{4,0},{6,2},{1,5},{3,7},{5,1},{7,3},{8,12},{10,14},{12... | collective-permute-start | bytes 49160 | tf_op jit(solution)/shard_map/ppermute | solution.py:24
  26.7 3.7 %collective-permute-start.8 = (bf16[16,512]{1,0:T(8,128)(2,1)S(1)}, bf16[16,512]{1,0:T(8,128)(2,1)S(1)}, u32[]{:S(2)}, u32[]{:S(2)}) collective-permute-start(bf16[16,512]{1,0:T(8,128)(2,1)S(1)} %shard_map.150.refs_0_.stream_ref), channel_id=1, source_target_pairs={{0,2},{2,0},{4,6},{6,4},{1,3},{3,1},{5,7},{7,5},{8,10},{10,8},{12,... | collective-permute-start | bytes 49160 | tf_op jit(solution)/shard_map/ppermute | solution.py:24
  31.7 1.2 %collective-permute-start.11 = (bf16[4,16,256]{2,1,0:T(8,128)(2,1)S(1)}, bf16[4,16,256]{2,1,0:T(8,128)(2,1)S(1)}, u32[]{:S(2)}, u32[]{:S(2)}) collective-permute-start(bf16[4,16,256]{2,1,0:T(8,128)(2,1)S(1)} %get-tuple-element.25), channel_id=1, source_target_pairs={{0,1},{1,0},{2,3},{3,2},{4,5},{5,4},{6,7},{7,6},{8,9},{9,8},{10,11... | collective-permute-start | bytes 98312 | tf_op jit(solution)/shard_map/ppermute | solution.py:18
  32.9 8.4 %collective-permute-start.12 = (bf16[16,256]{1,0:T(8,128)(2,1)S(1)}, bf16[16,256]{1,0:T(8,128)(2,1)S(1)}, u32[]{:S(2)}, u32[]{:S(2)}) collective-permute-start(bf16[16,256]{1,0:T(8,128)(2,1)S(1)} %get-tuple-element.27), channel_id=1, source_target_pairs={{0,2},{2,0},{4,6},{6,4},{1,3},{3,1},{5,7},{7,5},{8,10},{10,8},{12,... | collective-permute-start | bytes 24584 | tf_op jit(solution)/shard_map/ppermute | solution.py:24
  33.9 7.5 %collective-permute-start.13 = (bf16[16,256]{1,0:T(8,128)(2,1)S(1)}, bf16[16,256]{1,0:T(8,128)(2,1)S(1)}, u32[]{:S(2)}, u32[]{:S(2)}) collective-permute-start(bf16[16,256]{1,0:T(8,128)(2,1)S(1)} %get-tuple-element.28), channel_id=1, source_target_pairs={{0,4},{2,6},{4,0},{6,2},{1,5},{3,7},{5,1},{7,3},{8,12},{10,14},{12... | collective-permute-start | bytes 24584 | tf_op jit(solution)/shard_map/ppermute | solution.py:24
  35.0 6.4 %collective-permute-start.14 = (bf16[16,256]{1,0:T(8,128)(2,1)S(1)}, bf16[16,256]{1,0:T(8,128)(2,1)S(1)}, u32[]{:S(2)}, u32[]{:S(2)}) collective-permute-start(bf16[16,256]{1,0:T(8,128)(2,1)S(1)} %get-tuple-element.29), channel_id=1, source_target_pairs={{0,6},{2,4},{4,2},{6,0},{1,7},{3,5},{5,3},{7,1},{8,14},{10,12},{12... | collective-permute-start | bytes 24584 | tf_op jit(solution)/shard_map/ppermute | solution.py:24
  (5 other events, 8.5 us)

commit v3 on v2

--- a/solution.py
+++ b/solution.py
@@ -18,10 +18,11 @@
     return lax.ppermute(value, "tp", [(0, 1), (1, 0)])
 
 
-def spread(pieces, kv_size):
+def spread(pieces, kv_size, cross):
     came = []
     for k in range(1, kv_size):
-        came.append(lax.ppermute(pieces[k], "kv", [(i, i ^ k) for i in range(kv_size)]))
+        pairs = [(2 * i + c, 2 * (i ^ k) + (c ^ cross)) for i in range(kv_size) for c in (0, 1)]
+        came.append(lax.ppermute(pieces[k], ("kv", "tp"), pairs))
     return [pieces[0]] + came
 
 
@@ -134,57 +135,68 @@
     )(*parts, state, decay_offset.reshape(1, -1), head_gain.reshape(1, -1))
 
 
-def update_kernel(columns_ref, values_ref, state_ref, out_ref):
-    seqs = values_ref.shape[0]
-    b, h = pl.program_id(0), pl.program_id(1)
-    keys, vals = out_ref.shape[2:]
-    block = columns_ref[pl.ds(aligned(h, keys), keys), :]
-    lanes = lax.broadcasted_iota(jnp.int32, (1, block.shape[1]), 1)
-    keep = jnp.sum(jnp.where(lanes == seqs + b, block, 0.0), axis=1, keepdims=True)
-    key = jnp.sum(jnp.where(lanes == 2 * seqs + b, block, 0.0), axis=1, keepdims=True)
-    value = values_ref[pl.ds(b, 1), pl.ds(aligned(h, vals), vals)]
-    out_ref[0, 0] = keep * state_ref[0, 0] + key * value
-
-
-def update(columns, values, state):
-    seqs, heads, keys, vals = state.shape
-    tile = pl.BlockSpec((1, 1, keys, vals), lambda b, h: (b, h, 0, 0))
-    return pl.pallas_call(
-        update_kernel,
+def update_kernel(first, count, columns_ref, values_ref, state_ref, *refs):
+    out_hbm, tiles, sems = refs[-3:]
+    seqs, heads, keys, vals = state_ref.shape
+    copies = []
+    for n in range(count):
+        b = first + n
+        for h in range(heads):
+            rows = slice(h * keys, (h + 1) * keys)
+            keep = columns_ref[rows, seqs + b: seqs + b + 1]
+            key = columns_ref[rows, 2 * seqs + b: 2 * seqs + b + 1]
+            value = values_ref[b: b + 1, h * vals: (h + 1) * vals]
+            tiles[n, h] = keep * state_ref[b, h] + key * value
+            copies.append(pltpu.make_async_copy(tiles.at[n, h], out_hbm.at[b, h], sems.at[n, h]))
+            copies[-1].start()
+    for copy in copies:
+        copy.wait()
+
+
+def update(columns, values, state, first, count, *written):
+    return pl.pallas_call(
+        functools.partial(update_kernel, first, count),
         out_shape=jax.ShapeDtypeStruct(state.shape, f32),
-        grid=(seqs, heads),
-        in_specs=[VMEM, VMEM, tile],
-        out_specs=tile,
+        in_specs=[VMEM, VMEM, VMEM] + [pl.BlockSpec(memory_space=pl.ANY)] * len(written),
+        out_specs=pl.BlockSpec(memory_space=pl.ANY),
+        scratch_shapes=[pltpu.VMEM((count, *state.shape[1:]), f32), pltpu.SemaphoreType.DMA((count, state.shape[1]))],
+        input_output_aliases={3: 0} if written else {},
         compiler_params=pltpu.CompilerParams(vmem_limit_bytes=8 * 2**20),
         cost_estimate=HEAVY,
         name="update",
-    )(columns, values, state)
+    )(columns, values, state, *written)
 
 
 def branch_kernel(*refs):
-    *parts, w_ref, keep_ref, send_ref, rows = refs
+    *parts, own_w, other_w, keep_ref, send_ref, rows = refs
     me, _ = here()
-    for k, part in enumerate(parts):
-        rows[me ^ k] = part[...].astype(f32)
-    gated = jnp.concatenate([rows[d] for d in range(len(parts))], axis=0).astype(bf16)
-    branch = jnp.dot(gated, w_ref[...], preferred_element_type=f32)
-    keep_ref[...] = branch
-    send_ref[...] = branch.astype(bf16)
-
-
-def branch_of(parts, w_out):
+    count, seqs = len(parts), parts[0].shape[0]
+    pad = [jnp.zeros((-seqs % 8, parts[0].shape[1]), f32)] if seqs % 8 else []
+    own = jnp.concatenate([parts[0][...].astype(f32)] + pad, axis=0).astype(bf16)
+    far = jnp.concatenate([part[...].astype(f32) for part in parts[1:]] + [parts[0][...].astype(f32)], axis=0)
+    own = jnp.dot(own, own_w[...], preferred_element_type=f32)
+    far = jnp.dot(far.astype(bf16), other_w[...], preferred_element_type=f32)
+    rows[me] = own[:seqs]
+    for k in range(1, count):
+        rows[me ^ k] = far[(k - 1) * seqs: k * seqs]
+    for d in range(count):
+        keep_ref[d * seqs: (d + 1) * seqs, :] = rows[d]
+    send_ref[...] = keep_ref[...].astype(bf16)
+
+
+def branch_of(parts, own_w, other_w):
     rows = parts[0].shape[0] * len(parts)
-    outs = [jax.ShapeDtypeStruct((rows, w_out.shape[1]), kind) for kind in (f32, bf16)]
+    outs = [jax.ShapeDtypeStruct((rows, own_w.shape[1]), kind) for kind in (f32, bf16)]
     return pl.pallas_call(
         branch_kernel,
         out_shape=outs,
-        in_specs=[VMEM] * (len(parts) + 1),
+        in_specs=[VMEM] * (len(parts) + 2),
         out_specs=[VMEM] * 2,
-        scratch_shapes=[pltpu.VMEM((len(parts), *parts[0].shape), f32)],
+        scratch_shapes=[pltpu.VMEM((len(parts), parts[0].shape[0], own_w.shape[1]), f32)],
         compiler_params=pltpu.CompilerParams(vmem_limit_bytes=4 * 2**20),
         cost_estimate=HEAVY,
         name="branch",
-    )(*parts, w_out)
+    )(*parts, own_w, other_w)
 
 
 def mixer_kernel(*refs):
@@ -203,9 +215,10 @@
     hidden = hidden * lax.rsqrt(squares / depth + epsilon)
     squared = jnp.square(jnp.maximum(hidden, 0.0)).astype(bf16)
     total[...] = jnp.dot(squared, down_ref[...], preferred_element_type=f32)
-    for d in range(len(parts)):
-        keep_ref[d] = total[:, pl.ds(aligned(2 * d + core, own), own)]
-        give_ref[d] = total[:, pl.ds(aligned(2 * d + 1 - core, own), own)].astype(bf16)
+    for k in range(len(parts)):
+        side = core if k == 0 else 1 - core
+        keep_ref[k] = total[:, pl.ds(aligned(2 * (me ^ k) + side, own), own)]
+        give_ref[k] = total[:, pl.ds(aligned(2 * (me ^ k) + 1 - side, own), own)].astype(bf16)
 
 
 def mixer(parts, mlp_gain, w_up, w_down):
@@ -233,9 +246,8 @@
 
 
 def pair_kernel(keep_ref, came_ref, *outs):
-    me, _ = here()
     for k, out in zip(range(len(outs) - 1, -1, -1), outs):
-        out[...] = (keep_ref[me ^ k] + came_ref[me ^ k].astype(f32)).astype(out.dtype)
+        out[...] = (keep_ref[k] + came_ref[k].astype(f32)).astype(out.dtype)
 
 
 def last_kernel(stream_ref, *refs):
@@ -263,15 +275,17 @@
     like = jax.ShapeDtypeStruct
     other = swap_cores(tokens)
     squares = small(clear_kernel, like((rows, 128), f32))
-    parts = spread(project(squares, tokens, other, mix_gain, weights, kv_size), kv_size)
+    parts = spread(project(squares, tokens, other, mix_gain, weights, kv_size), kv_size, 0)
     gated, columns, values = readout(parts, state, decay_offset, head_gain, depth)
-    arrived = spread([gated] * kv_size, kv_size)
-    new_state = update(columns, values, state)
-    branch, branch_sent = branch_of(arrived, w_out)
+    arrived = spread([gated] * kv_size, kv_size, 1)
+    new_state = update(columns, values, state, 0, 2)
+    new_state = update(columns, values, state, 2, 2, new_state)
+    w_other = swap_cores(w_out)
+    branch, branch_sent = branch_of(arrived, w_out, w_other)
     stream = small(stream_kernel, like((rows, 2 * half), bf16), branch, swap_cores(branch_sent), tokens, other)
-    keep, give = mixer(spread([stream] * kv_size, kv_size), mlp_gain, w_up, w_down)
+    keep, give = mixer(spread([stream] * kv_size, kv_size, 1), mlp_gain, w_up, w_down)
     outs = [like((rows, half), f32 if k == 0 else bf16) for k in range(kv_size - 1, -1, -1)]
-    pieces = spread(small(pair_kernel, outs, keep, swap_cores(give))[::-1], kv_size)
+    pieces = spread(small(pair_kernel, outs, keep, swap_cores(give))[::-1], kv_size, 1)
     return small(last_kernel, like((rows, half), bf16), stream, *pieces), new_state
 
 

time: 42.1 us -> 40.1 us (0.952)
  starting transfers between devices: 19.6 us -> 17.4 us
  waiting for transfers between devices: 13.6 us -> 14.4 us
  Pallas kernels: 7.67 us -> 6.94 us
    ppermute x12, starting transfers between devices: 19 us -> 15.9 us  [spread(): came.append(lax.ppermute(pieces[k], ('kv', 'tp'), pairs))]
    ppermute x12, waiting for transfers between devices: 10.2 us -> 12.5 us  [spread(): came.append(lax.ppermute(pieces[k], ('kv', 'tp'), pairs))]
    ppermute x3 -> x4, waiting for transfers between devices: 3.43 us -> 1.88 us  [swap_cores(): return lax.ppermute(value, 'tp', [(0, 1), (1, 0)])]
    ppermute x3 -> x4, starting transfers between devices: 0.57 us -> 1.52 us  [swap_cores(): return lax.ppermute(value, 'tp', [(0, 1), (1, 0)])]
    pallas_call x1 -> x2, Pallas kernels: 3.96 us -> 3.08 us  [update(): pl.pallas_call(functools.partial(update_kernel, first, count), out_shape=...]
  transfers between devices with their start and end apart: 15 -> 16, of which waited for: 10 -> 8; matrix products, arithmetic and copies ran while one was open for 0% -> 0% of each run, Pallas kernels for 9% -> 10%
where the time goes in v3:
time: 40.1 us; the launch traced here: 40 us
  starting transfers between devices  17.4 us (43%)
  waiting for transfers between devices  14.4 us (36%)
  Pallas kernels  6.94 us (17%)
  between operations  0.82 us (2%)
    ppermute x12, starting transfers between devices, spread(): came.append(lax.ppermute(pieces[k], ('kv', 'tp'), pairs))  15.9 us
    ppermute x12, waiting for transfers between devices, spread(): came.append(lax.ppermute(pieces[k], ('kv', 'tp'), pairs))  12.5 us
    pallas_call x2, Pallas kernels, update(): pl.pallas_call(functools.partial(update_kernel, first, count), out_shape=...  3.08 us
    ppermute x4, waiting for transfers between devices, swap_cores(): return lax.ppermute(value, 'tp', [(0, 1), (1, 0)])  1.88 us
    ppermute x4, starting transfers between devices, swap_cores(): return lax.ppermute(value, 'tp', [(0, 1), (1, 0)])  1.52 us
    pallas_call x1, Pallas kernels, mixer(): pl.pallas_call(mixer_kernel, out_shape=outs, in_specs=[VMEM] * (len(parts...  1.24 us
    pallas_call x1, Pallas kernels, readout(): pl.pallas_call(functools.partial(readout_kernel, len(parts), depth), out_...  0.96 us
  transfers between devices with their start and end apart: 16, of which 8 were waited for; matrix products, arithmetic and copies ran while one was open for 0% of the time, Pallas kernels for 10%

profile of v3, /device:TPU:0, one launch (start us, length us, event | category | flops | bytes accessed | tf_op | source)
XLA Modules:
  0.0 40.0 jit_solution(16478966342803986786)
XLA Ops:
  1.3 1.0 %collective-permute-done.other_ref = bf16[16,256]{1,0:T(8,128)(2,1)S(1)} collective-permute-done((bf16[16,256]{1,0:T(8,128)(2,1)}, bf16[16,256]{1,0:T(8,128)(2,1)S(1)}, u32[]{:S(2)}, u32[]{:S(2)}) %collective-permute-start) | collective-permute-done | bytes 8224 | tf_op jit(solution)/shard_map/ppermute | solution.py:18
  2.7 0.6 %project.1 = (bf16[4,3840]{1,0:T(4,128)(2,1)S(1)}, bf16[4,3840]{1,0:T(4,128)(2,1)S(1)}, bf16[4,3840]{1,0:T(4,128)(2,1)S(1)}, f32[4,3840]{1,0:T(4,128)S(1)}) custom-call(f32[16,128]{1,0:T(8,128)S(1)} %shard_map.149.squares_ref, bf16[16,256]{1,0:T(8,128)(2,1)S(1)} %copy-done.9, bf16[16,256]{1,0:T(8,128)(2,1)S(1)} %collective-permute-done.other_ref, ...), custom_call_target="tpu_custom_call" | custom-call | flops 20000000000 | bytes 1048576 | tf_op jit(solution)/shard_map/project/pallas_call | solution.py:73
  3.3 3.1 %collective-permute-start.1 = (bf16[4,3840]{1,0:T(4,128)(2,1)S(1)}, bf16[4,3840]{1,0:T(4,128)(2,1)S(1)}, u32[]{:S(2)}, u32[]{:S(2)}) collective-permute-start(bf16[4,3840]{1,0:T(4,128)(2,1)S(1)} %get-tuple-element.18), channel_id=1, source_target_pairs={{0,2},{1,3},{2,0},{3,1},{4,6},{5,7},{6,4},{7,5},{8,10},{9,11},{10,... | collective-permute-start | bytes 92168 | tf_op jit(solution)/shard_map/ppermute | solution.py:25
  6.4 2.6 %collective-permute-start.2 = (bf16[4,3840]{1,0:T(4,128)(2,1)S(1)}, bf16[4,3840]{1,0:T(4,128)(2,1)S(1)}, u32[]{:S(2)}, u32[]{:S(2)}) collective-permute-start(bf16[4,3840]{1,0:T(4,128)(2,1)S(1)} %get-tuple-element.19), channel_id=1, source_target_pairs={{0,4},{1,5},{2,6},{3,7},{4,0},{5,1},{6,2},{7,3},{8,12},{9,13},{10,... | collective-permute-start | bytes 92168 | tf_op jit(solution)/shard_map/ppermute | solution.py:25
  9.0 2.7 %collective-permute-done.2.refs_2_ = bf16[4,3840]{1,0:T(4,128)(2,1)S(1)} collective-permute-done((bf16[4,3840]{1,0:T(4,128)(2,1)S(1)}, bf16[4,3840]{1,0:T(4,128)(2,1)S(1)}, u32[]{:S(2)}, u32[]{:S(2)}) %collective-permute-start.2) | collective-permute-done | bytes 30752 | tf_op jit(solution)/shard_map/ppermute | solution.py:25
  11.8 3.0 %collective-permute-done.3.refs_3_ = bf16[4,3840]{1,0:T(4,128)(2,1)S(1)} collective-permute-done((bf16[4,3840]{1,0:T(4,128)(2,1)S(1)}, bf16[4,3840]{1,0:T(4,128)(2,1)S(1)}, u32[]{:S(2)}, u32[]{:S(2)}) %collective-permute-start.3) | collective-permute-done | bytes 30752 | tf_op jit(solution)/shard_map/ppermute | solution.py:25
  14.7 1.0 %readout.1 = (bf16[4,1024]{1,0:T(4,128)(2,1)S(1)}, f32[512,16]{1,0:T(8,128)S(1)}, f32[4,1024]{1,0:T(4,128)S(1)}) custom-call(f32[4,3840]{1,0:T(4,128)S(1)} %get-tuple-element.17.refs_0_, bf16[4,3840]{1,0:T(4,128)(2,1)S(1)} %collective-permute-done.1.refs_1_, bf16[4,3840]{1,0:T(4,128)(2,1)S(1)} %collective-permute-done.2.refs_2_, ...), custom_call_target="tpu_custom_call" | custom-call | flops 20000000000 | bytes 1048576 | tf_op jit(solution)/shard_map/readout/pallas_call | solution.py:127
  15.8 1.8 %collective-permute-start.4 = (bf16[4,1024]{1,0:T(4,128)(2,1)S(1)}, bf16[4,1024]{1,0:T(4,128)(2,1)S(1)}, u32[]{:S(2)}, u32[]{:S(2)}) collective-permute-start(bf16[4,1024]{1,0:T(4,128)(2,1)S(1)} %get-tuple-element.21.refs_0_), channel_id=1, source_target_pairs={{0,3},{1,2},{2,1},{3,0},{4,7},{5,6},{6,5},{7,4},{8,11},{9,10},{10,... | collective-permute-start | bytes 24584 | tf_op jit(solution)/shard_map/ppermute | solution.py:25
  17.6 2.9 %collective-permute-done.6.refs_3_ = bf16[4,1024]{1,0:T(4,128)(2,1)S(1)} collective-permute-done((bf16[4,1024]{1,0:T(4,128)(2,1)S(1)}, bf16[4,1024]{1,0:T(4,128)(2,1)S(1)}, u32[]{:S(2)}, u32[]{:S(2)}) %collective-permute-start.6) | collective-permute-done | bytes 8224 | tf_op jit(solution)/shard_map/ppermute | solution.py:25
  21.0 0.7 %collective-permute-start.8 = (bf16[16,512]{1,0:T(8,128)(2,1)S(1)}, bf16[16,512]{1,0:T(8,128)(2,1)S(1)}, u32[]{:S(2)}, u32[]{:S(2)}) collective-permute-start(bf16[16,512]{1,0:T(8,128)(2,1)S(1)} %get-tuple-element.23), channel_id=1, source_target_pairs={{0,1},{1,0},{2,3},{3,2},{4,5},{5,4},{6,7},{7,6},{8,9},{9,8},{10,11... | collective-permute-start | bytes 49160 | tf_op jit(solution)/shard_map/ppermute | solution.py:18
  21.7 0.8 %collective-permute-done.8.came_ref = bf16[16,512]{1,0:T(8,128)(2,1)S(1)} collective-permute-done((bf16[16,512]{1,0:T(8,128)(2,1)S(1)}, bf16[16,512]{1,0:T(8,128)(2,1)S(1)}, u32[]{:S(2)}, u32[]{:S(2)}) %collective-permute-start.8) | collective-permute-done | bytes 16416 | tf_op jit(solution)/shard_map/ppermute | solution.py:18
  22.6 2.4 %collective-permute-start.11 = (bf16[16,512]{1,0:T(8,128)(2,1)S(1)}, bf16[16,512]{1,0:T(8,128)(2,1)S(1)}, u32[]{:S(2)}, u32[]{:S(2)}) collective-permute-start(bf16[16,512]{1,0:T(8,128)(2,1)S(1)} %shard_map.150.refs_0_.stream_ref), channel_id=1, source_target_pairs={{0,7},{1,6},{2,5},{3,4},{4,3},{5,2},{6,1},{7,0},{8,15},{9,14},{10,... | collective-permute-start | bytes 49160 | tf_op jit(solution)/shard_map/ppermute | solution.py:25
  25.0 0.8 %collective-permute-start.10 = (bf16[16,512]{1,0:T(8,128)(2,1)S(1)}, bf16[16,512]{1,0:T(8,128)(2,1)S(1)}, u32[]{:S(2)}, u32[]{:S(2)}) collective-permute-start(bf16[16,512]{1,0:T(8,128)(2,1)S(1)} %shard_map.150.refs_0_.stream_ref), channel_id=1, source_target_pairs={{0,5},{1,4},{2,7},{3,6},{4,1},{5,0},{6,3},{7,2},{8,13},{9,12},{10,... | collective-permute-start | bytes 49160 | tf_op jit(solution)/shard_map/ppermute | solution.py:25
  25.8 0.9 %collective-permute-start.9 = (bf16[16,512]{1,0:T(8,128)(2,1)S(1)}, bf16[16,512]{1,0:T(8,128)(2,1)S(1)}, u32[]{:S(2)}, u32[]{:S(2)}) collective-permute-start(bf16[16,512]{1,0:T(8,128)(2,1)S(1)} %shard_map.150.refs_0_.stream_ref), channel_id=1, source_target_pairs={{0,3},{1,2},{2,1},{3,0},{4,7},{5,6},{6,5},{7,4},{8,11},{9,10},{10,... | collective-permute-start | bytes 49160 | tf_op jit(solution)/shard_map/ppermute | solution.py:25
  26.7 1.0 %collective-permute-done.11.refs_3_ = bf16[16,512]{1,0:T(8,128)(2,1)S(1)} collective-permute-done((bf16[16,512]{1,0:T(8,128)(2,1)S(1)}, bf16[16,512]{1,0:T(8,128)(2,1)S(1)}, u32[]{:S(2)}, u32[]{:S(2)}) %collective-permute-start.11) | collective-permute-done | bytes 16416 | tf_op jit(solution)/shard_map/ppermute | solution.py:25
  27.7 1.4 %collective-permute-done.10.refs_2_ = bf16[16,512]{1,0:T(8,128)(2,1)S(1)} collective-permute-done((bf16[16,512]{1,0:T(8,128)(2,1)S(1)}, bf16[16,512]{1,0:T(8,128)(2,1)S(1)}, u32[]{:S(2)}, u32[]{:S(2)}) %collective-permute-start.10) | collective-permute-done | bytes 16416 | tf_op jit(solution)/shard_map/ppermute | solution.py:25
  29.2 1.2 %mixer.1 = (f32[4,16,256]{2,1,0:T(8,128)S(1)}, bf16[4,16,256]{2,1,0:T(8,128)(2,1)S(1)}) custom-call(bf16[16,512]{1,0:T(8,128)(2,1)S(1)} %shard_map.150.refs_0_.stream_ref, bf16[16,512]{1,0:T(8,128)(2,1)S(1)} %collective-permute-done.9.refs_1_, bf16[16,512]{1,0:T(8,128)(2,1)S(1)} %collective-permute-done.10.refs_2_, ...), custom_call_target="tpu_custom_call" | custom-call | flops 20000000000 | bytes 1048576 | tf_op jit(solution)/shard_map/mixer/pallas_call | solution.py:227
  30.6 1.5 %update.2.refs_0_ = f32[4,2,256,512]{3,2,1,0:T(8,128)} custom-call(f32[512,16]{1,0:T(8,128)S(1)} %get-tuple-element.30.columns_ref, f32[4,1024]{1,0:T(4,128)S(1)} %get-tuple-element.31.values_ref, f32[4,2,256,512]{3,2,1,0:T(8,128)S(1)} %copy-done.2), custom_call_target="tpu_custom_call" | custom-call | flops 20000000000 | bytes 1048576 | tf_op jit(solution)/shard_map/update/pallas_call | solution.py:157
  32.2 0.8 %collective-permute-start.13 = (bf16[16,256]{1,0:T(8,128)(2,1)S(1)}, bf16[16,256]{1,0:T(8,128)(2,1)S(1)}, u32[]{:S(2)}, u32[]{:S(2)}) collective-permute-start(bf16[16,256]{1,0:T(8,128)(2,1)S(1)} %get-tuple-element.27), channel_id=1, source_target_pairs={{0,3},{1,2},{2,1},{3,0},{4,7},{5,6},{6,5},{7,4},{8,11},{9,10},{10,... | collective-permute-start | bytes 24584 | tf_op jit(solution)/shard_map/ppermute | solution.py:25
  33.0 1.5 %collective-permute-start.14 = (bf16[16,256]{1,0:T(8,128)(2,1)S(1)}, bf16[16,256]{1,0:T(8,128)(2,1)S(1)}, u32[]{:S(2)}, u32[]{:S(2)}) collective-permute-start(bf16[16,256]{1,0:T(8,128)(2,1)S(1)} %get-tuple-element.28), channel_id=1, source_target_pairs={{0,5},{1,4},{2,7},{3,6},{4,1},{5,0},{6,3},{7,2},{8,13},{9,12},{10,... | collective-permute-start | bytes 24584 | tf_op jit(solution)/shard_map/ppermute | solution.py:25
  34.5 1.8 %collective-permute-start.15 = (bf16[16,256]{1,0:T(8,128)(2,1)S(1)}, bf16[16,256]{1,0:T(8,128)(2,1)S(1)}, u32[]{:S(2)}, u32[]{:S(2)}) collective-permute-start(bf16[16,256]{1,0:T(8,128)(2,1)S(1)} %get-tuple-element.29), channel_id=1, source_target_pairs={{0,7},{1,6},{2,5},{3,4},{4,3},{5,2},{6,1},{7,0},{8,15},{9,14},{10,... | collective-permute-start | bytes 24584 | tf_op jit(solution)/shard_map/ppermute | solution.py:25
  36.3 1.5 %update.3 = f32[4,2,256,512]{3,2,1,0:T(8,128)} custom-call(f32[512,16]{1,0:T(8,128)S(1)} %get-tuple-element.30.columns_ref, f32[4,1024]{1,0:T(4,128)S(1)} %get-tuple-element.31.values_ref, f32[4,2,256,512]{3,2,1,0:T(8,128)S(1)} %copy-done.2, f32[4,2,256,512]{3,2,1,0:T(8,128)} %update.2.refs_0_), custom_call_target="tpu_custom_call", output_to_operand_aliasing={{}: (3, {})} | custom-call | flops 20000000000 | bytes 1048576 | tf_op jit(solution)/shard_map/update/pallas_call | solution.py:157
  37.9 1.5 %collective-permute-done.15.refs_3_ = bf16[16,256]{1,0:T(8,128)(2,1)S(1)} collective-permute-done((bf16[16,256]{1,0:T(8,128)(2,1)S(1)}, bf16[16,256]{1,0:T(8,128)(2,1)S(1)}, u32[]{:S(2)}, u32[]{:S(2)}) %collective-permute-start.15) | collective-permute-done | bytes 8224 | tf_op jit(solution)/shard_map/ppermute | solution.py:25
  39.4 0.6 %shard_map.152 = bf16[16,256]{1,0:T(8,128)(2,1)} custom-call(bf16[16,512]{1,0:T(8,128)(2,1)S(1)} %shard_map.150.refs_0_.stream_ref, f32[16,256]{1,0:T(8,128)S(1)} %get-tuple-element.26.refs_0_, bf16[16,256]{1,0:T(8,128)(2,1)S(1)} %collective-permute-done.13.refs_1_, bf16[16,256]{1,0:T(8,128)(2,1)S(1)} %collective-permute-done.14.refs_2_, ...), custom_call_target="tpu_custom_call" | custom-call | flops 20000000000 | bytes 1048576 | tf_op jit(solution)/shard_map/pallas_call | solution.py:262
  (46 shorter events, 1.8 us)
Async XLA Ops:
  0.7 2.0 %copy-start.6 = (bf16[512,512]{1,0:T(8,128)(2,1)S(1)}, bf16[512,512]{1,0:T(8,128)(2,1)}, u32[]{:S(2)}) copy-start(bf16[512,512]{1,0:T(8,128)(2,1)} %refs_0_.1) | copy-start | bytes 1572868
  0.7 1.6 %collective-permute-start = (bf16[16,256]{1,0:T(8,128)(2,1)}, bf16[16,256]{1,0:T(8,128)(2,1)S(1)}, u32[]{:S(2)}, u32[]{:S(2)}) collective-permute-start(bf16[16,256]{1,0:T(8,128)(2,1)} %own_ref.3), channel_id=1, source_target_pairs={{0,1},{1,0},{2,3},{3,2},{4,5},{5,4},{6,7},{7,6},{8,9},{9,8},{10,11... | collective-permute-start | bytes 24584 | tf_op jit(solution)/shard_map/ppermute | solution.py:18
  2.6 6.4 %copy-start.5 = (bf16[1024,512]{1,0:T(8,128)(2,1)S(1)}, bf16[1024,512]{1,0:T(8,128)(2,1)}, u32[]{:S(2)}) copy-start(bf16[1024,512]{1,0:T(8,128)(2,1)} %refs_4_.5) | copy-start | bytes 3145732
  2.6 12.1 %copy-start.2 = (f32[4,2,256,512]{3,2,1,0:T(8,128)S(1)}, f32[4,2,256,512]{3,2,1,0:T(8,128)}, u32[]{:S(2)}) copy-start(f32[4,2,256,512]{3,2,1,0:T(8,128)} %state_ref.3) | copy-start | bytes 12582916
  2.6 12.1 %copy-start.12 = (f32[512]{0:T(512)S(1)}, f32[512]{0:T(512)}, u32[]{:S(2)}) copy-start(f32[512]{0:T(512)} %param.22) | copy-start | bytes 6148
  2.6 12.1 %copy-start.13 = (f32[512]{0:T(512)S(1)}, f32[512]{0:T(512)}, u32[]{:S(2)}) copy-start(f32[512]{0:T(512)} %param.23) | copy-start | bytes 6148
  3.3 5.7 %collective-permute-start.1 = (bf16[4,3840]{1,0:T(4,128)(2,1)S(1)}, bf16[4,3840]{1,0:T(4,128)(2,1)S(1)}, u32[]{:S(2)}, u32[]{:S(2)}) collective-permute-start(bf16[4,3840]{1,0:T(4,128)(2,1)S(1)} %get-tuple-element.18), channel_id=1, source_target_pairs={{0,2},{1,3},{2,0},{3,1},{4,6},{5,7},{6,4},{7,5},{8,10},{9,11},{10,... | collective-permute-start | bytes 92168 | tf_op jit(solution)/shard_map/ppermute | solution.py:25
  6.4 5.3 %collective-permute-start.2 = (bf16[4,3840]{1,0:T(4,128)(2,1)S(1)}, bf16[4,3840]{1,0:T(4,128)(2,1)S(1)}, u32[]{:S(2)}, u32[]{:S(2)}) collective-permute-start(bf16[4,3840]{1,0:T(4,128)(2,1)S(1)} %get-tuple-element.19), channel_id=1, source_target_pairs={{0,4},{1,5},{2,6},{3,7},{4,0},{5,1},{6,2},{7,3},{8,12},{9,13},{10,... | collective-permute-start | bytes 92168 | tf_op jit(solution)/shard_map/ppermute | solution.py:25
  9.0 5.7 %collective-permute-start.3 = (bf16[4,3840]{1,0:T(4,128)(2,1)S(1)}, bf16[4,3840]{1,0:T(4,128)(2,1)S(1)}, u32[]{:S(2)}, u32[]{:S(2)}) collective-permute-start(bf16[4,3840]{1,0:T(4,128)(2,1)S(1)} %get-tuple-element.20), channel_id=1, source_target_pairs={{0,6},{1,7},{2,4},{3,5},{4,2},{5,3},{6,0},{7,1},{8,14},{9,15},{10,... | collective-permute-start | bytes 92168 | tf_op jit(solution)/shard_map/ppermute | solution.py:25
  9.0 11.5 %collective-permute-start.7 = (bf16[1024,512]{1,0:T(8,128)(2,1)S(1)}, bf16[1024,512]{1,0:T(8,128)(2,1)S(1)}, u32[]{:S(2)}, u32[]{:S(2)}) collective-permute-start(bf16[1024,512]{1,0:T(8,128)(2,1)S(1)} %copy-done.5), channel_id=1, source_target_pairs={{0,1},{1,0},{2,3},{3,2},{4,5},{5,4},{6,7},{7,6},{8,9},{9,8},{10,11... | collective-permute-start | bytes 3145736 | tf_op jit(solution)/shard_map/ppermute | solution.py:18
  15.7 4.9 %collective-permute-start.6 = (bf16[4,1024]{1,0:T(4,128)(2,1)S(1)}, bf16[4,1024]{1,0:T(4,128)(2,1)S(1)}, u32[]{:S(2)}, u32[]{:S(2)}) collective-permute-start(bf16[4,1024]{1,0:T(4,128)(2,1)S(1)} %get-tuple-element.21.refs_0_), channel_id=1, source_target_pairs={{0,7},{1,6},{2,5},{3,4},{4,3},{5,2},{6,1},{7,0},{8,15},{9,14},{10,... | collective-permute-start | bytes 24584 | tf_op jit(solution)/shard_map/ppermute | solution.py:25
  15.7 4.9 %collective-permute-start.5 = (bf16[4,1024]{1,0:T(4,128)(2,1)S(1)}, bf16[4,1024]{1,0:T(4,128)(2,1)S(1)}, u32[]{:S(2)}, u32[]{:S(2)}) collective-permute-start(bf16[4,1024]{1,0:T(4,128)(2,1)S(1)} %get-tuple-element.21.refs_0_), channel_id=1, source_target_pairs={{0,5},{1,4},{2,7},{3,6},{4,1},{5,0},{6,3},{7,2},{8,13},{9,12},{10,... | collective-permute-start | bytes 24584 | tf_op jit(solution)/shard_map/ppermute | solution.py:25
  15.8 4.7 %collective-permute-start.4 = (bf16[4,1024]{1,0:T(4,128)(2,1)S(1)}, bf16[4,1024]{1,0:T(4,128)(2,1)S(1)}, u32[]{:S(2)}, u32[]{:S(2)}) collective-permute-start(bf16[4,1024]{1,0:T(4,128)(2,1)S(1)} %get-tuple-element.21.refs_0_), channel_id=1, source_target_pairs={{0,3},{1,2},{2,1},{3,0},{4,7},{5,6},{6,5},{7,4},{8,11},{9,10},{10,... | collective-permute-start | bytes 24584 | tf_op jit(solution)/shard_map/ppermute | solution.py:25
  21.0 1.6 %collective-permute-start.8 = (bf16[16,512]{1,0:T(8,128)(2,1)S(1)}, bf16[16,512]{1,0:T(8,128)(2,1)S(1)}, u32[]{:S(2)}, u32[]{:S(2)}) collective-permute-start(bf16[16,512]{1,0:T(8,128)(2,1)S(1)} %get-tuple-element.23), channel_id=1, source_target_pairs={{0,1},{1,0},{2,3},{3,2},{4,5},{5,4},{6,7},{7,6},{8,9},{9,8},{10,11... | collective-permute-start | bytes 49160 | tf_op jit(solution)/shard_map/ppermute | solution.py:18
  22.5 6.6 %copy-start = (bf16[2048,1024]{1,0:T(8,128)(2,1)S(1)}, bf16[2048,1024]{1,0:T(8,128)(2,1)}, u32[]{:S(2)}) copy-start(bf16[2048,1024]{1,0:T(8,128)(2,1)} %refs_5_.1) | copy-start | bytes 12582916
  22.6 6.6 %copy-start.1 = (bf16[1024,2048]{1,0:T(8,128)(2,1)S(1)}, bf16[1024,2048]{1,0:T(8,128)(2,1)}, u32[]{:S(2)}) copy-start(bf16[1024,2048]{1,0:T(8,128)(2,1)} %refs_6_.1) | copy-start | bytes 12582916
  22.6 6.6 %copy-start.10 = (f32[2048]{0:T(1024)S(1)}, f32[2048]{0:T(1024)}, u32[]{:S(2)}) copy-start(f32[2048]{0:T(1024)} %param.25) | copy-start | bytes 24580
  22.6 5.1 %collective-permute-start.11 = (bf16[16,512]{1,0:T(8,128)(2,1)S(1)}, bf16[16,512]{1,0:T(8,128)(2,1)S(1)}, u32[]{:S(2)}, u32[]{:S(2)}) collective-permute-start(bf16[16,512]{1,0:T(8,128)(2,1)S(1)} %shard_map.150.refs_0_.stream_ref), channel_id=1, source_target_pairs={{0,7},{1,6},{2,5},{3,4},{4,3},{5,2},{6,1},{7,0},{8,15},{9,14},{10,... | collective-permute-start | bytes 49160 | tf_op jit(solution)/shard_map/ppermute | solution.py:25
  25.0 4.2 %collective-permute-start.10 = (bf16[16,512]{1,0:T(8,128)(2,1)S(1)}, bf16[16,512]{1,0:T(8,128)(2,1)S(1)}, u32[]{:S(2)}, u32[]{:S(2)}) collective-permute-start(bf16[16,512]{1,0:T(8,128)(2,1)S(1)} %shard_map.150.refs_0_.stream_ref), channel_id=1, source_target_pairs={{0,5},{1,4},{2,7},{3,6},{4,1},{5,0},{6,3},{7,2},{8,13},{9,12},{10,... | collective-permute-start | bytes 49160 | tf_op jit(solution)/shard_map/ppermute | solution.py:25
  25.8 3.4 %collective-permute-start.9 = (bf16[16,512]{1,0:T(8,128)(2,1)S(1)}, bf16[16,512]{1,0:T(8,128)(2,1)S(1)}, u32[]{:S(2)}, u32[]{:S(2)}) collective-permute-start(bf16[16,512]{1,0:T(8,128)(2,1)S(1)} %shard_map.150.refs_0_.stream_ref), channel_id=1, source_target_pairs={{0,3},{1,2},{2,1},{3,0},{4,7},{5,6},{6,5},{7,4},{8,11},{9,10},{10,... | collective-permute-start | bytes 49160 | tf_op jit(solution)/shard_map/ppermute | solution.py:25
  30.4 1.8 %collective-permute-start.12 = (bf16[4,16,256]{2,1,0:T(8,128)(2,1)S(1)}, bf16[4,16,256]{2,1,0:T(8,128)(2,1)S(1)}, u32[]{:S(2)}, u32[]{:S(2)}) collective-permute-start(bf16[4,16,256]{2,1,0:T(8,128)(2,1)S(1)} %get-tuple-element.25), channel_id=1, source_target_pairs={{0,1},{1,0},{2,3},{3,2},{4,5},{5,4},{6,7},{7,6},{8,9},{9,8},{10,11... | collective-permute-start | bytes 98312 | tf_op jit(solution)/shard_map/ppermute | solution.py:18
  32.2 5.7 %collective-permute-start.13 = (bf16[16,256]{1,0:T(8,128)(2,1)S(1)}, bf16[16,256]{1,0:T(8,128)(2,1)S(1)}, u32[]{:S(2)}, u32[]{:S(2)}) collective-permute-start(bf16[16,256]{1,0:T(8,128)(2,1)S(1)} %get-tuple-element.27), channel_id=1, source_target_pairs={{0,3},{1,2},{2,1},{3,0},{4,7},{5,6},{6,5},{7,4},{8,11},{9,10},{10,... | collective-permute-start | bytes 24584 | tf_op jit(solution)/shard_map/ppermute | solution.py:25
  33.0 4.9 %collective-permute-start.14 = (bf16[16,256]{1,0:T(8,128)(2,1)S(1)}, bf16[16,256]{1,0:T(8,128)(2,1)S(1)}, u32[]{:S(2)}, u32[]{:S(2)}) collective-permute-start(bf16[16,256]{1,0:T(8,128)(2,1)S(1)} %get-tuple-element.28), channel_id=1, source_target_pairs={{0,5},{1,4},{2,7},{3,6},{4,1},{5,0},{6,3},{7,2},{8,13},{9,12},{10,... | collective-permute-start | bytes 24584 | tf_op jit(solution)/shard_map/ppermute | solution.py:25
  34.5 4.9 %collective-permute-start.15 = (bf16[16,256]{1,0:T(8,128)(2,1)S(1)}, bf16[16,256]{1,0:T(8,128)(2,1)S(1)}, u32[]{:S(2)}, u32[]{:S(2)}) collective-permute-start(bf16[16,256]{1,0:T(8,128)(2,1)S(1)} %get-tuple-element.29), channel_id=1, source_target_pairs={{0,7},{1,6},{2,5},{3,4},{4,3},{5,2},{6,1},{7,0},{8,15},{9,14},{10,... | collective-permute-start | bytes 24584 | tf_op jit(solution)/shard_map/ppermute | solution.py:25
  (6 other events, 10.4 us)

commit v4 on v3

--- a/solution.py
+++ b/solution.py
@@ -12,6 +12,7 @@
 bf16, f32 = jnp.bfloat16, jnp.float32
 VMEM = pl.BlockSpec(memory_space=pltpu.VMEM)
 HEAVY = pl.CostEstimate(flops=2 * 10**10, bytes_accessed=2**20, transcendentals=0)
+LIGHT = pl.CostEstimate(flops=2**17, bytes_accessed=2**17, transcendentals=0)
 
 
 def swap_cores(value):
@@ -82,46 +83,65 @@
     )(squares, tokens, other, mix_gain.reshape(1, -1), *weights)[::-1]
 
 
+def narrow_kernel(state_ref, out_ref):
+    out_ref[...] = state_ref[...].astype(bf16)
+
+
+def narrow(state):
+    return pl.pallas_call(
+        narrow_kernel,
+        out_shape=jax.ShapeDtypeStruct(state.shape, bf16),
+        in_specs=[VMEM],
+        out_specs=VMEM,
+        compiler_params=pltpu.CompilerParams(vmem_limit_bytes=8 * 2**20),
+        cost_estimate=LIGHT,
+        name="narrow",
+    )(state)
+
+
 def readout_kernel(kv_size, depth, *refs):
     parts = refs[:kv_size]
-    state_ref, offset_ref, gain_ref, gated_ref, columns_ref, values_ref = refs[kv_size:]
+    state_ref, offset_ref, gain_ref, gated_ref, factors_ref, values_ref = refs[kv_size:]
     seqs, heads, keys, vals = state_ref.shape
     kw, vw = heads * keys, heads * vals
-    base = 3 * kw + 2 * vw
 
     def summed(start, width):
         return sum(p[:, start: start + width].astype(f32) for p in parts)
 
+    base = 3 * kw + 2 * vw
     sums = summed(base, 128)[:, :1] + summed(base + 128, 128)[:, :1]
     row_scale = lax.rsqrt(sums / depth + epsilon)
     queries = summed(0, kw) * row_scale * keys ** (-0.5)
     new_keys = summed(kw, kw) * row_scale
     retain = jax.nn.sigmoid(summed(2 * kw, kw) * row_scale + offset_ref[...])
+    kept = (queries * retain).astype(bf16)
+    row = lax.broadcasted_iota(jnp.int32, (seqs, 1), 0)
+    reads = []
+    for h in range(heads):
+        at = slice(h * keys, (h + 1) * keys)
+        read = 0.0
+        for b in range(seqs):
+            product = jnp.dot(kept[:, at], state_ref[b, h], preferred_element_type=f32)
+            read += jnp.where(row == b, product, 0.0)
+        reads.append(read)
     values = summed(3 * kw, vw) * row_scale
     gates = summed(3 * kw + vw, vw) * row_scale
-    values_ref[...] = values
-    fill = jnp.zeros((-3 * seqs % 8, kw), f32)
-    columns = jnp.concatenate([queries * retain, retain, new_keys] + ([fill] if fill.shape[0] else []), axis=0).T
-    columns_ref[...] = columns
     silu = gates * jax.nn.sigmoid(gates)
     for h in range(heads):
-        qk = jnp.sum(queries[:, h * keys: (h + 1) * keys] * new_keys[:, h * keys: (h + 1) * keys], axis=1,
-                     keepdims=True)
-        reads = []
-        for b in range(seqs):
-            weight = columns[h * keys: (h + 1) * keys, b: b + 1]
-            reads.append(jnp.sum(weight * state_ref[b, h], axis=0, keepdims=True))
-        read = jnp.concatenate(reads, axis=0) + qk * values[:, h * vals: (h + 1) * vals]
+        at, to = slice(h * keys, (h + 1) * keys), slice(h * vals, (h + 1) * vals)
+        read = reads[h] + jnp.sum(queries[:, at] * new_keys[:, at], axis=1, keepdims=True) * values[:, to]
         read = read * lax.rsqrt(jnp.mean(read * read, axis=1, keepdims=True) + epsilon) * gain_ref[...]
-        gated_ref[:, h * vals: (h + 1) * vals] = (read * silu[:, h * vals: (h + 1) * vals]).astype(bf16)
-
-
-def readout(parts, state, decay_offset, head_gain, depth):
+        gated_ref[:, to] = (read * silu[:, to]).astype(bf16)
+    values_ref[...] = values
+    factors_ref[0] = retain
+    factors_ref[1] = new_keys
+
+
+def readout(parts, state, narrowed, decay_offset, head_gain, depth):
     seqs, heads, keys, vals = state.shape
-    height = 3 * seqs + (-3 * seqs % 8)
     outs = [
         jax.ShapeDtypeStruct((seqs, heads * vals), bf16),
-        jax.ShapeDtypeStruct((heads * keys, height), f32),
+        jax.ShapeDtypeStruct((2, seqs, heads * keys), f32),
         jax.ShapeDtypeStruct((seqs, heads * vals), f32),
     ]
     return pl.pallas_call(
@@ -129,22 +149,25 @@
         out_shape=outs,
         in_specs=[VMEM] * (len(parts) + 3),
         out_specs=[VMEM] * 3,
-        compiler_params=pltpu.CompilerParams(vmem_limit_bytes=12 * 2**20),
+        compiler_params=pltpu.CompilerParams(vmem_limit_bytes=8 * 2**20),
         cost_estimate=HEAVY,
         name="readout",
-    )(*parts, state, decay_offset.reshape(1, -1), head_gain.reshape(1, -1))
-
-
-def update_kernel(first, count, columns_ref, values_ref, state_ref, *refs):
+    )(*parts, narrowed, decay_offset.reshape(1, -1), head_gain.reshape(1, -1))
+
+
+def update_kernel(first, count, factors_ref, values_ref, state_ref, *refs):
     out_hbm, tiles, sems = refs[-3:]
     seqs, heads, keys, vals = state_ref.shape
+    rows = [factors_ref[n] for n in (0, 1)]
+    if 2 * seqs % 8:
+        rows.append(jnp.zeros((-2 * seqs % 8, heads * keys), f32))
+    columns = jnp.concatenate(rows, axis=0).T
     copies = []
     for n in range(count):
         b = first + n
         for h in range(heads):
-            rows = slice(h * keys, (h + 1) * keys)
-            keep = columns_ref[rows, seqs + b: seqs + b + 1]
-            key = columns_ref[rows, 2 * seqs + b: 2 * seqs + b + 1]
+            at = slice(h * keys, (h + 1) * keys)
+            keep, key = columns[at, b: b + 1], columns[at, seqs + b: seqs + b + 1]
             value = values_ref[b: b + 1, h * vals: (h + 1) * vals]
             tiles[n, h] = keep * state_ref[b, h] + key * value
             copies.append(pltpu.make_async_copy(tiles.at[n, h], out_hbm.at[b, h], sems.at[n, h]))
@@ -153,7 +176,7 @@
         copy.wait()
 
 
-def update(columns, values, state, first, count, *written):
+def update(factors, values, state, first, count, *written):
     return pl.pallas_call(
         functools.partial(update_kernel, first, count),
         out_shape=jax.ShapeDtypeStruct(state.shape, f32),
@@ -162,78 +185,117 @@
         scratch_shapes=[pltpu.VMEM((count, *state.shape[1:]), f32), pltpu.SemaphoreType.DMA((count, state.shape[1]))],
         input_output_aliases={3: 0} if written else {},
         compiler_params=pltpu.CompilerParams(vmem_limit_bytes=8 * 2**20),
-        cost_estimate=HEAVY,
+        cost_estimate=LIGHT,
         name="update",
-    )(columns, values, state, *written)
-
-
-def branch_kernel(*refs):
-    *parts, own_w, other_w, keep_ref, send_ref, rows = refs
+    )(factors, values, state, *written)
+
+
+def own_branch_kernel(gated_ref, w_ref, out_ref):
+    seqs, width = gated_ref.shape
+    gated = gated_ref[...].astype(f32)
+    if seqs % 8:
+        gated = jnp.concatenate([gated, jnp.zeros((-seqs % 8, width), f32)], axis=0)
+    out_ref[...] = jnp.dot(gated.astype(bf16), w_ref[...], preferred_element_type=f32)[:seqs]
+
+
+def branch_kernel(own_ref, *refs):
+    *parts, w_ref, keep_ref, send_ref, rows = refs
     me, _ = here()
-    count, seqs = len(parts), parts[0].shape[0]
-    pad = [jnp.zeros((-seqs % 8, parts[0].shape[1]), f32)] if seqs % 8 else []
-    own = jnp.concatenate([parts[0][...].astype(f32)] + pad, axis=0).astype(bf16)
-    far = jnp.concatenate([part[...].astype(f32) for part in parts[1:]] + [parts[0][...].astype(f32)], axis=0)
-    own = jnp.dot(own, own_w[...], preferred_element_type=f32)
-    far = jnp.dot(far.astype(bf16), other_w[...], preferred_element_type=f32)
-    rows[me] = own[:seqs]
-    for k in range(1, count):
+    seqs = own_ref.shape[0]
+    far = jnp.concatenate([part[...].astype(f32) for part in parts] + [jnp.zeros(parts[0].shape, f32)], axis=0)
+    far = jnp.dot(far.astype(bf16), w_ref[...], preferred_element_type=f32)
+    rows[me] = own_ref[...]
+    for k in range(1, len(parts) + 1):
         rows[me ^ k] = far[(k - 1) * seqs: k * seqs]
-    for d in range(count):
+    for d in range(len(parts) + 1):
         keep_ref[d * seqs: (d + 1) * seqs, :] = rows[d]
     send_ref[...] = keep_ref[...].astype(bf16)
 
 
 def branch_of(parts, own_w, other_w):
-    rows = parts[0].shape[0] * len(parts)
-    outs = [jax.ShapeDtypeStruct((rows, own_w.shape[1]), kind) for kind in (f32, bf16)]
+    seqs, width = parts[0].shape[0], own_w.shape[1]
+    rows = seqs * len(parts)
+    own = small(own_branch_kernel, jax.ShapeDtypeStruct((seqs, width), f32), parts[0], own_w, cost=LIGHT)
+    outs = [jax.ShapeDtypeStruct((rows, width), kind) for kind in (f32, bf16)]
     return pl.pallas_call(
         branch_kernel,
         out_shape=outs,
-        in_specs=[VMEM] * (len(parts) + 2),
+        in_specs=[VMEM] * (len(parts) + 1),
         out_specs=[VMEM] * 2,
-        scratch_shapes=[pltpu.VMEM((len(parts), parts[0].shape[0], own_w.shape[1]), f32)],
+        scratch_shapes=[pltpu.VMEM((len(parts), seqs, width), f32)],
         compiler_params=pltpu.CompilerParams(vmem_limit_bytes=4 * 2**20),
         cost_estimate=HEAVY,
         name="branch",
-    )(*parts, own_w, other_w)
-
-
-def mixer_kernel(*refs):
+    )(own, *parts[1:], other_w)
+
+
+def hidden_of(owner, part, gain_ref, up_ref):
+    width = part.shape[1]
+    stream = part[...].astype(f32)
+    normed = (stream * gain_ref[:, pl.ds(aligned(owner, width), width)]).astype(bf16)
+    product = jnp.dot(normed, up_ref[pl.ds(aligned(owner, width), width), :], preferred_element_type=f32)
+    return jnp.sum(stream * stream, axis=1, keepdims=True), product
+
+
+def first_mixer_kernel(steps, *refs):
+    *parts, gain_ref, up_ref, _, squares_ref, hidden_ref = refs
+    me, _ = here()
+    squares, hidden = 0.0, 0.0
+    for k, part in zip(steps, parts):
+        square, product = hidden_of(me ^ k, part, gain_ref, up_ref)
+        squares += square
+        hidden += product
+    squares_ref[...] = jnp.broadcast_to(squares, squares_ref.shape)
+    hidden_ref[...] = hidden
+
+
+def mixer_kernel(steps, squares_ref, hidden_ref, *refs):
     *parts, gain_ref, up_ref, down_ref, keep_ref, give_ref, total = refs
     me, core = here()
     width = parts[0].shape[1]
-    depth = width * len(parts)
     own = width // 2
-    squares, hidden = 0.0, 0.0
-    for k, part in enumerate(parts):
-        owner = me ^ k
-        stream = part[...].astype(f32)
-        squares += jnp.sum(stream * stream, axis=1, keepdims=True)
-        normed = (stream * gain_ref[:, pl.ds(aligned(owner, width), width)]).astype(bf16)
-        hidden += jnp.dot(normed, up_ref[pl.ds(aligned(owner, width), width), :], preferred_element_type=f32)
-    hidden = hidden * lax.rsqrt(squares / depth + epsilon)
+    squares, hidden = squares_ref[:, :1], hidden_ref[...]
+    for k, part in zip(steps, parts):
+        square, product = hidden_of(me ^ k, part, gain_ref, up_ref)
+        squares += square
+        hidden += product
+    hidden = hidden * lax.rsqrt(squares / up_ref.shape[0] + epsilon)
     squared = jnp.square(jnp.maximum(hidden, 0.0)).astype(bf16)
     total[...] = jnp.dot(squared, down_ref[...], preferred_element_type=f32)
-    for k in range(len(parts)):
+    for k in range(keep_ref.shape[0]):
         side = core if k == 0 else 1 - core
         keep_ref[k] = total[:, pl.ds(aligned(2 * (me ^ k) + side, own), own)]
         give_ref[k] = total[:, pl.ds(aligned(2 * (me ^ k) + 1 - side, own), own)].astype(bf16)
 
 
 def mixer(parts, mlp_gain, w_up, w_down):
+    count = len(parts)
     rows, width = parts[0].shape
-    outs = [jax.ShapeDtypeStruct((len(parts), rows, width // 2), kind) for kind in (f32, bf16)]
-    return pl.pallas_call(
-        mixer_kernel,
+    early = (0, count - 1)
+    late = tuple(range(1, count - 1))
+    gain = mlp_gain.reshape(1, -1)
+    params = dict(
+        compiler_params=pltpu.CompilerParams(vmem_limit_bytes=6 * 2**20),
+        cost_estimate=LIGHT,
+    )
+    begun = pl.pallas_call(
+        functools.partial(first_mixer_kernel, early),
+        out_shape=[jax.ShapeDtypeStruct((rows, 128), f32), jax.ShapeDtypeStruct((rows, w_up.shape[1]), f32)],
+        in_specs=[VMEM] * 5,
+        out_specs=[VMEM] * 2,
+        name="first_mixer",
+        **params,
+    )(*[parts[k] for k in early], gain, w_up, w_down)
+    outs = [jax.ShapeDtypeStruct((count, rows, width // 2), kind) for kind in (f32, bf16)]
+    return pl.pallas_call(
+        functools.partial(mixer_kernel, late),
         out_shape=outs,
-        in_specs=[VMEM] * (len(parts) + 3),
+        in_specs=[VMEM] * (5 + len(late)),
         out_specs=[VMEM] * 2,
         scratch_shapes=[pltpu.VMEM((rows, w_down.shape[1]), f32)],
-        compiler_params=pltpu.CompilerParams(vmem_limit_bytes=16 * 2**20),
-        cost_estimate=HEAVY,
         name="mixer",
-    )(*parts, mlp_gain.reshape(1, -1), w_up, w_down)
+        **params,
+    )(*begun, *[parts[k] for k in late], gain, w_up, w_down)
 
 
 def stream_kernel(branch_ref, came_ref, own_ref, other_ref, stream_ref):
@@ -258,14 +320,14 @@
     out_ref[...] = (stream_ref[:, pl.ds(aligned(core, half), half)].astype(f32) + total).astype(bf16)
 
 
-def small(body, outs, *args):
+def small(body, outs, *args, cost=HEAVY):
     return pl.pallas_call(
         body,
         out_shape=outs,
         in_specs=[VMEM] * len(args),
         out_specs=jax.tree.map(lambda _: VMEM, outs),
         compiler_params=pltpu.CompilerParams(vmem_limit_bytes=2 * 2**20),
-        cost_estimate=HEAVY,
+        cost_estimate=cost,
     )(*args)
 
 
@@ -276,10 +338,12 @@
     other = swap_cores(tokens)
     squares = small(clear_kernel, like((rows, 128), f32))
     parts = spread(project(squares, tokens, other, mix_gain, weights, kv_size), kv_size, 0)
-    gated, columns, values = readout(parts, state, decay_offset, head_gain, depth)
+    narrowed = narrow(state)
+    gated, factors, values = readout(parts, state, narrowed, decay_offset, head_gain, depth)
     arrived = spread([gated] * kv_size, kv_size, 1)
-    new_state = update(columns, values, state, 0, 2)
-    new_state = update(columns, values, state, 2, 2, new_state)
+    new_state = update(factors, values, state, 0, 1)
+    new_state = update(factors, values, state, 1, 1, new_state)
+    new_state = update(factors, values, state, 2, 2, new_state)
     w_other = swap_cores(w_out)
     branch, branch_sent = branch_of(arrived, w_out, w_other)
     stream = small(stream_kernel, like((rows, 2 * half), bf16), branch, swap_cores(branch_sent), tokens, other)
@@ -340,7 +404,7 @@
 
 
 def shards(kv_size, tokens, state, mix_gain, w_query, w_key, w_decay, w_value, w_gate, *rest):
-    steps = fused_steps if tokens.shape[1] % 128 == 0 and kv_size in (2, 4, 8) else plain_steps
+    steps = fused_steps if tokens.shape[1] % 128 == 0 and kv_size in (4, 8) else plain_steps
     return steps(kv_size, tokens, state, mix_gain, (w_query, w_key, w_decay, w_value, w_gate), *rest)
 
 

time: 40.1 us -> 39.8 us (level)
  waiting for transfers between devices: 14.4 us -> 13.1 us
  Pallas kernels: 6.94 us -> 8.08 us
    ppermute x12, waiting for transfers between devices: 12.5 us -> 10.2 us  [spread(): came.append(lax.ppermute(pieces[k], ('kv', 'tp'), pairs))]
    pallas_call x2 -> x3, Pallas kernels: 3.08 us -> 4.25 us  [update(): pl.pallas_call(functools.partial(update_kernel, first, count), out_shape=...]
    ppermute x4, waiting for transfers between devices: 1.88 us -> 2.92 us  [swap_cores(): return lax.ppermute(value, 'tp', [(0, 1), (1, 0)])]
    pallas_call x1, Pallas kernels: 0.96 us -> 0.53 us  [readout(): pl.pallas_call(functools.partial(readout_kernel, len(parts), depth), out_...]
    pallas_call x1 -> x3, Pallas kernels: 1.24 us -> 1.55 us  [the longest x1 0.96 us: mixer(): pl.pallas_call(functools.partial(mixer_kernel, late), out_shape=outs, in_...]
    pallas_call x4 -> x5, Pallas kernels: 0.63 us -> 0.87 us  [small(): pl.pallas_call(body, out_shape=outs, in_specs=[VMEM] * len(args), out_spe...]
  transfers between devices with their start and end apart: 16 -> 16, of which waited for: 8 -> 8; matrix products, arithmetic and copies ran while one was open for 0% -> 0% of each run, Pallas kernels for 10% -> 14%
where the time goes in v4:
time: 39.8 us; the launch traced here: 39.7 us
  starting transfers between devices  17.2 us (43%)
  waiting for transfers between devices  13.1 us (33%)
  Pallas kernels  8.08 us (20%)
  between operations  0.85 us (2%)
    ppermute x12, starting transfers between devices, spread(): came.append(lax.ppermute(pieces[k], ('kv', 'tp'), pairs))  15.7 us
    ppermute x12, waiting for transfers between devices, spread(): came.append(lax.ppermute(pieces[k], ('kv', 'tp'), pairs))  10.2 us
    pallas_call x3, Pallas kernels, update(): pl.pallas_call(functools.partial(update_kernel, first, count), out_shape=...  4.25 us
    ppermute x4, waiting for transfers between devices, swap_cores(): return lax.ppermute(value, 'tp', [(0, 1), (1, 0)])  2.92 us
    ppermute x4, starting transfers between devices, swap_cores(): return lax.ppermute(value, 'tp', [(0, 1), (1, 0)])  1.52 us
    pallas_call x1, Pallas kernels, mixer(): pl.pallas_call(functools.partial(mixer_kernel, late), out_shape=outs, in_...  0.96 us
    pallas_call x5, Pallas kernels, small(): pl.pallas_call(body, out_shape=outs, in_specs=[VMEM] * len(args), out_spe...  0.87 us
  transfers between devices with their start and end apart: 16, of which 8 were waited for; matrix products, arithmetic and copies ran while one was open for 0% of the time, Pallas kernels for 14%

profile of v4, /device:TPU:0, one launch (start us, length us, event | category | flops | bytes accessed | tf_op | source)
XLA Modules:
  0.0 39.7 jit_solution(13666189694388005498)
XLA Ops:
  1.3 1.0 %collective-permute-done.other_ref = bf16[16,256]{1,0:T(8,128)(2,1)S(1)} collective-permute-done((bf16[16,256]{1,0:T(8,128)(2,1)}, bf16[16,256]{1,0:T(8,128)(2,1)S(1)}, u32[]{:S(2)}, u32[]{:S(2)}) %collective-permute-start) | collective-permute-done | bytes 8224 | tf_op jit(solution)/shard_map/ppermute | solution.py:19
  2.6 0.6 %project.1 = (bf16[4,3840]{1,0:T(4,128)(2,1)S(1)}, bf16[4,3840]{1,0:T(4,128)(2,1)S(1)}, bf16[4,3840]{1,0:T(4,128)(2,1)S(1)}, f32[4,3840]{1,0:T(4,128)S(1)}) custom-call(f32[16,128]{1,0:T(8,128)S(1)} %shard_map.149.squares_ref, bf16[16,256]{1,0:T(8,128)(2,1)S(1)} %copy-done.10, bf16[16,256]{1,0:T(8,128)(2,1)S(1)} %collective-permute-done.other_ref, ...), custom_call_target="tpu_custom_call" | custom-call | flops 20000000000 | bytes 1048576 | tf_op jit(solution)/shard_map/project/pallas_call | solution.py:74
  3.3 3.1 %collective-permute-start.1 = (bf16[4,3840]{1,0:T(4,128)(2,1)S(1)}, bf16[4,3840]{1,0:T(4,128)(2,1)S(1)}, u32[]{:S(2)}, u32[]{:S(2)}) collective-permute-start(bf16[4,3840]{1,0:T(4,128)(2,1)S(1)} %get-tuple-element.20), channel_id=1, source_target_pairs={{0,2},{1,3},{2,0},{3,1},{4,6},{5,7},{6,4},{7,5},{8,10},{9,11},{10,... | collective-permute-start | bytes 92168 | tf_op jit(solution)/shard_map/ppermute | solution.py:26
  6.4 2.6 %collective-permute-start.2 = (bf16[4,3840]{1,0:T(4,128)(2,1)S(1)}, bf16[4,3840]{1,0:T(4,128)(2,1)S(1)}, u32[]{:S(2)}, u32[]{:S(2)}) collective-permute-start(bf16[4,3840]{1,0:T(4,128)(2,1)S(1)} %get-tuple-element.21), channel_id=1, source_target_pairs={{0,4},{1,5},{2,6},{3,7},{4,0},{5,1},{6,2},{7,3},{8,12},{9,13},{10,... | collective-permute-start | bytes 92168 | tf_op jit(solution)/shard_map/ppermute | solution.py:26
  9.3 2.5 %collective-permute-done.2.refs_2_ = bf16[4,3840]{1,0:T(4,128)(2,1)S(1)} collective-permute-done((bf16[4,3840]{1,0:T(4,128)(2,1)S(1)}, bf16[4,3840]{1,0:T(4,128)(2,1)S(1)}, u32[]{:S(2)}, u32[]{:S(2)}) %collective-permute-start.2) | collective-permute-done | bytes 30752 | tf_op jit(solution)/shard_map/ppermute | solution.py:26
  11.8 3.0 %collective-permute-done.3.refs_3_ = bf16[4,3840]{1,0:T(4,128)(2,1)S(1)} collective-permute-done((bf16[4,3840]{1,0:T(4,128)(2,1)S(1)}, bf16[4,3840]{1,0:T(4,128)(2,1)S(1)}, u32[]{:S(2)}, u32[]{:S(2)}) %collective-permute-start.3) | collective-permute-done | bytes 30752 | tf_op jit(solution)/shard_map/ppermute | solution.py:26
  15.4 1.8 %collective-permute-start.4 = (bf16[4,1024]{1,0:T(4,128)(2,1)S(1)}, bf16[4,1024]{1,0:T(4,128)(2,1)S(1)}, u32[]{:S(2)}, u32[]{:S(2)}) collective-permute-start(bf16[4,1024]{1,0:T(4,128)(2,1)S(1)} %get-tuple-element.23.gated_ref), channel_id=1, source_target_pairs={{0,3},{1,2},{2,1},{3,0},{4,7},{5,6},{6,5},{7,4},{8,11},{9,10},{10,... | collective-permute-start | bytes 24584 | tf_op jit(solution)/shard_map/ppermute | solution.py:26
  17.4 2.7 %collective-permute-done.6.refs_2_ = bf16[4,1024]{1,0:T(4,128)(2,1)S(1)} collective-permute-done((bf16[4,1024]{1,0:T(4,128)(2,1)S(1)}, bf16[4,1024]{1,0:T(4,128)(2,1)S(1)}, u32[]{:S(2)}, u32[]{:S(2)}) %collective-permute-start.6) | collective-permute-done | bytes 8224 | tf_op jit(solution)/shard_map/ppermute | solution.py:26
  20.4 0.7 %collective-permute-start.8 = (bf16[16,512]{1,0:T(8,128)(2,1)S(1)}, bf16[16,512]{1,0:T(8,128)(2,1)S(1)}, u32[]{:S(2)}, u32[]{:S(2)}) collective-permute-start(bf16[16,512]{1,0:T(8,128)(2,1)S(1)} %get-tuple-element.25), channel_id=1, source_target_pairs={{0,1},{1,0},{2,3},{3,2},{4,5},{5,4},{6,7},{7,6},{8,9},{9,8},{10,11... | collective-permute-start | bytes 49160 | tf_op jit(solution)/shard_map/ppermute | solution.py:19
  21.1 0.8 %collective-permute-done.8.came_ref = bf16[16,512]{1,0:T(8,128)(2,1)S(1)} collective-permute-done((bf16[16,512]{1,0:T(8,128)(2,1)S(1)}, bf16[16,512]{1,0:T(8,128)(2,1)S(1)}, u32[]{:S(2)}, u32[]{:S(2)}) %collective-permute-start.8) | collective-permute-done | bytes 16416 | tf_op jit(solution)/shard_map/ppermute | solution.py:19
  22.0 2.4 %collective-permute-start.9 = (bf16[16,512]{1,0:T(8,128)(2,1)S(1)}, bf16[16,512]{1,0:T(8,128)(2,1)S(1)}, u32[]{:S(2)}, u32[]{:S(2)}) collective-permute-start(bf16[16,512]{1,0:T(8,128)(2,1)S(1)} %shard_map.151.refs_0_.stream_ref), channel_id=1, source_target_pairs={{0,7},{1,6},{2,5},{3,4},{4,3},{5,2},{6,1},{7,0},{8,15},{9,14},{10,... | collective-permute-start | bytes 49160 | tf_op jit(solution)/shard_map/ppermute | solution.py:26
  24.4 0.8 %collective-permute-start.11 = (bf16[16,512]{1,0:T(8,128)(2,1)S(1)}, bf16[16,512]{1,0:T(8,128)(2,1)S(1)}, u32[]{:S(2)}, u32[]{:S(2)}) collective-permute-start(bf16[16,512]{1,0:T(8,128)(2,1)S(1)} %shard_map.151.refs_0_.stream_ref), channel_id=1, source_target_pairs={{0,5},{1,4},{2,7},{3,6},{4,1},{5,0},{6,3},{7,2},{8,13},{9,12},{10,... | collective-permute-start | bytes 49160 | tf_op jit(solution)/shard_map/ppermute | solution.py:26
  25.2 0.9 %collective-permute-start.10 = (bf16[16,512]{1,0:T(8,128)(2,1)S(1)}, bf16[16,512]{1,0:T(8,128)(2,1)S(1)}, u32[]{:S(2)}, u32[]{:S(2)}) collective-permute-start(bf16[16,512]{1,0:T(8,128)(2,1)S(1)} %shard_map.151.refs_0_.stream_ref), channel_id=1, source_target_pairs={{0,3},{1,2},{2,1},{3,0},{4,7},{5,6},{6,5},{7,4},{8,11},{9,10},{10,... | collective-permute-start | bytes 49160 | tf_op jit(solution)/shard_map/ppermute | solution.py:26
  26.1 1.0 %collective-permute-done.9.refs_1_ = bf16[16,512]{1,0:T(8,128)(2,1)S(1)} collective-permute-done((bf16[16,512]{1,0:T(8,128)(2,1)S(1)}, bf16[16,512]{1,0:T(8,128)(2,1)S(1)}, u32[]{:S(2)}, u32[]{:S(2)}) %collective-permute-start.9) | collective-permute-done | bytes 16416 | tf_op jit(solution)/shard_map/ppermute | solution.py:26
  27.5 1.0 %collective-permute-done.11.refs_1_ = bf16[16,512]{1,0:T(8,128)(2,1)S(1)} collective-permute-done((bf16[16,512]{1,0:T(8,128)(2,1)S(1)}, bf16[16,512]{1,0:T(8,128)(2,1)S(1)}, u32[]{:S(2)}, u32[]{:S(2)}) %collective-permute-start.11) | collective-permute-done | bytes 16416 | tf_op jit(solution)/shard_map/ppermute | solution.py:26
  28.6 1.0 %mixer.1 = (f32[4,16,256]{2,1,0:T(8,128)S(1)}, bf16[4,16,256]{2,1,0:T(8,128)(2,1)S(1)}) custom-call(f32[16,128]{1,0:T(8,128)S(1)} %get-tuple-element.26.squares_ref, f32[16,1024]{1,0:T(8,128)S(1)} %get-tuple-element.27.hidden_ref, bf16[16,512]{1,0:T(8,128)(2,1)S(1)} %collective-permute-done.10.refs_0_, bf16[16,512]{1,0:T(8,128)(2,1)S(1)} %collective-permute-done.11.refs_1_, ...), custom_call_target="tpu_custom_call" | custom-call | flops 131072 | bytes 131072 | tf_op jit(solution)/shard_map/mixer/pallas_call | solution.py:290
  29.8 1.0 %collective-permute-done.12.came_ref = bf16[4,16,256]{2,1,0:T(8,128)(2,1)S(1)} collective-permute-done((bf16[4,16,256]{2,1,0:T(8,128)(2,1)S(1)}, bf16[4,16,256]{2,1,0:T(8,128)(2,1)S(1)}, u32[]{:S(2)}, u32[]{:S(2)}) %collective-permute-start.12) | collective-permute-done | bytes 32800 | tf_op jit(solution)/shard_map/ppermute | solution.py:19
  30.8 0.8 %collective-permute-start.13 = (bf16[16,256]{1,0:T(8,128)(2,1)S(1)}, bf16[16,256]{1,0:T(8,128)(2,1)S(1)}, u32[]{:S(2)}, u32[]{:S(2)}) collective-permute-start(bf16[16,256]{1,0:T(8,128)(2,1)S(1)} %get-tuple-element.31), channel_id=1, source_target_pairs={{0,3},{1,2},{2,1},{3,0},{4,7},{5,6},{6,5},{7,4},{8,11},{9,10},{10,... | collective-permute-start | bytes 24584 | tf_op jit(solution)/shard_map/ppermute | solution.py:26
  31.6 1.6 %collective-permute-start.14 = (bf16[16,256]{1,0:T(8,128)(2,1)S(1)}, bf16[16,256]{1,0:T(8,128)(2,1)S(1)}, u32[]{:S(2)}, u32[]{:S(2)}) collective-permute-start(bf16[16,256]{1,0:T(8,128)(2,1)S(1)} %get-tuple-element.32), channel_id=1, source_target_pairs={{0,5},{1,4},{2,7},{3,6},{4,1},{5,0},{6,3},{7,2},{8,13},{9,12},{10,... | collective-permute-start | bytes 24584 | tf_op jit(solution)/shard_map/ppermute | solution.py:26
  33.2 1.6 %collective-permute-start.15 = (bf16[16,256]{1,0:T(8,128)(2,1)S(1)}, bf16[16,256]{1,0:T(8,128)(2,1)S(1)}, u32[]{:S(2)}, u32[]{:S(2)}) collective-permute-start(bf16[16,256]{1,0:T(8,128)(2,1)S(1)} %get-tuple-element.33), channel_id=1, source_target_pairs={{0,7},{1,6},{2,5},{3,4},{4,3},{5,2},{6,1},{7,0},{8,15},{9,14},{10,... | collective-permute-start | bytes 24584 | tf_op jit(solution)/shard_map/ppermute | solution.py:26
  34.8 1.3 %update.3.refs_0_ = f32[4,2,256,512]{3,2,1,0:T(8,128)} custom-call(f32[2,4,512]{2,1,0:T(4,128)S(1)} %get-tuple-element.34.factors_ref, f32[4,1024]{1,0:T(4,128)S(1)} %get-tuple-element.35.values_ref, f32[4,2,256,512]{3,2,1,0:T(8,128)S(1)} %copy-done), custom_call_target="tpu_custom_call" | custom-call | flops 131072 | bytes 131072 | tf_op jit(solution)/shard_map/update/pallas_call | solution.py:180
  36.1 1.3 %update.4.refs_0_ = f32[4,2,256,512]{3,2,1,0:T(8,128)} custom-call(f32[2,4,512]{2,1,0:T(4,128)S(1)} %get-tuple-element.34.factors_ref, f32[4,1024]{1,0:T(4,128)S(1)} %get-tuple-element.35.values_ref, f32[4,2,256,512]{3,2,1,0:T(8,128)S(1)} %copy-done, f32[4,2,256,512]{3,2,1,0:T(8,128)} %update.3.refs_0_), custom_call_target="tpu_custom_call", output_to_operand_aliasing={{}: (3, {})} | custom-call | flops 131072 | bytes 131072 | tf_op jit(solution)/shard_map/update/pallas_call | solution.py:180
  37.4 1.7 %update.5 = f32[4,2,256,512]{3,2,1,0:T(8,128)} custom-call(f32[2,4,512]{2,1,0:T(4,128)S(1)} %get-tuple-element.34.factors_ref, f32[4,1024]{1,0:T(4,128)S(1)} %get-tuple-element.35.values_ref, f32[4,2,256,512]{3,2,1,0:T(8,128)S(1)} %copy-done, f32[4,2,256,512]{3,2,1,0:T(8,128)} %update.4.refs_0_), custom_call_target="tpu_custom_call", output_to_operand_aliasing={{}: (3, {})} | custom-call | flops 131072 | bytes 131072 | tf_op jit(solution)/shard_map/update/pallas_call | solution.py:180
  39.1 0.6 %shard_map.153 = bf16[16,256]{1,0:T(8,128)(2,1)} custom-call(bf16[16,512]{1,0:T(8,128)(2,1)S(1)} %shard_map.151.refs_0_.stream_ref, f32[16,256]{1,0:T(8,128)S(1)} %get-tuple-element.30.refs_0_, bf16[16,256]{1,0:T(8,128)(2,1)S(1)} %collective-permute-done.13.refs_1_, bf16[16,256]{1,0:T(8,128)(2,1)S(1)} %collective-permute-done.14.refs_2_, ...), custom_call_target="tpu_custom_call" | custom-call | flops 20000000000 | bytes 1048576 | tf_op jit(solution)/shard_map/pallas_call | solution.py:324
  (50 shorter events, 3.0 us)
Async XLA Ops:
  0.7 2.0 %copy-start.7 = (bf16[512,512]{1,0:T(8,128)(2,1)S(1)}, bf16[512,512]{1,0:T(8,128)(2,1)}, u32[]{:S(2)}) copy-start(bf16[512,512]{1,0:T(8,128)(2,1)} %refs_0_.1) | copy-start | bytes 1572868
  0.7 1.6 %collective-permute-start = (bf16[16,256]{1,0:T(8,128)(2,1)}, bf16[16,256]{1,0:T(8,128)(2,1)S(1)}, u32[]{:S(2)}, u32[]{:S(2)}) collective-permute-start(bf16[16,256]{1,0:T(8,128)(2,1)} %own_ref.3), channel_id=1, source_target_pairs={{0,1},{1,0},{2,3},{3,2},{4,5},{5,4},{6,7},{7,6},{8,9},{9,8},{10,11... | collective-permute-start | bytes 24584 | tf_op jit(solution)/shard_map/ppermute | solution.py:19
  2.6 6.4 %copy-start.3 = (bf16[1024,512]{1,0:T(8,128)(2,1)S(1)}, bf16[1024,512]{1,0:T(8,128)(2,1)}, u32[]{:S(2)}) copy-start(bf16[1024,512]{1,0:T(8,128)(2,1)} %w_ref.1) | copy-start | bytes 3145732
  2.6 6.4 %copy-start = (f32[4,2,256,512]{3,2,1,0:T(8,128)S(1)}, f32[4,2,256,512]{3,2,1,0:T(8,128)}, u32[]{:S(2)}) copy-start(f32[4,2,256,512]{3,2,1,0:T(8,128)} %state_ref.7) | copy-start | bytes 12582916
  3.3 11.4 %copy-start.12 = (f32[512]{0:T(512)S(1)}, f32[512]{0:T(512)}, u32[]{:S(2)}) copy-start(f32[512]{0:T(512)} %param.22) | copy-start | bytes 6148
  3.3 11.4 %copy-start.13 = (f32[512]{0:T(512)S(1)}, f32[512]{0:T(512)}, u32[]{:S(2)}) copy-start(f32[512]{0:T(512)} %param.23) | copy-start | bytes 6148
  3.3 5.9 %collective-permute-start.1 = (bf16[4,3840]{1,0:T(4,128)(2,1)S(1)}, bf16[4,3840]{1,0:T(4,128)(2,1)S(1)}, u32[]{:S(2)}, u32[]{:S(2)}) collective-permute-start(bf16[4,3840]{1,0:T(4,128)(2,1)S(1)} %get-tuple-element.20), channel_id=1, source_target_pairs={{0,2},{1,3},{2,0},{3,1},{4,6},{5,7},{6,4},{7,5},{8,10},{9,11},{10,... | collective-permute-start | bytes 92168 | tf_op jit(solution)/shard_map/ppermute | solution.py:26
  6.4 5.3 %collective-permute-start.2 = (bf16[4,3840]{1,0:T(4,128)(2,1)S(1)}, bf16[4,3840]{1,0:T(4,128)(2,1)S(1)}, u32[]{:S(2)}, u32[]{:S(2)}) collective-permute-start(bf16[4,3840]{1,0:T(4,128)(2,1)S(1)} %get-tuple-element.21), channel_id=1, source_target_pairs={{0,4},{1,5},{2,6},{3,7},{4,0},{5,1},{6,2},{7,3},{8,12},{9,13},{10,... | collective-permute-start | bytes 92168 | tf_op jit(solution)/shard_map/ppermute | solution.py:26
  9.0 5.7 %collective-permute-start.3 = (bf16[4,3840]{1,0:T(4,128)(2,1)S(1)}, bf16[4,3840]{1,0:T(4,128)(2,1)S(1)}, u32[]{:S(2)}, u32[]{:S(2)}) collective-permute-start(bf16[4,3840]{1,0:T(4,128)(2,1)S(1)} %get-tuple-element.22), channel_id=1, source_target_pairs={{0,6},{1,7},{2,4},{3,5},{4,2},{5,3},{6,0},{7,1},{8,14},{9,15},{10,... | collective-permute-start | bytes 92168 | tf_op jit(solution)/shard_map/ppermute | solution.py:26
  9.0 11.1 %collective-permute-start.7 = (bf16[1024,512]{1,0:T(8,128)(2,1)S(1)}, bf16[1024,512]{1,0:T(8,128)(2,1)S(1)}, u32[]{:S(2)}, u32[]{:S(2)}) collective-permute-start(bf16[1024,512]{1,0:T(8,128)(2,1)S(1)} %copy-done.3), channel_id=1, source_target_pairs={{0,1},{1,0},{2,3},{3,2},{4,5},{5,4},{6,7},{7,6},{8,9},{9,8},{10,11... | collective-permute-start | bytes 3145736 | tf_op jit(solution)/shard_map/ppermute | solution.py:19
  15.2 4.9 %collective-permute-start.6 = (bf16[4,1024]{1,0:T(4,128)(2,1)S(1)}, bf16[4,1024]{1,0:T(4,128)(2,1)S(1)}, u32[]{:S(2)}, u32[]{:S(2)}) collective-permute-start(bf16[4,1024]{1,0:T(4,128)(2,1)S(1)} %get-tuple-element.23.gated_ref), channel_id=1, source_target_pairs={{0,7},{1,6},{2,5},{3,4},{4,3},{5,2},{6,1},{7,0},{8,15},{9,14},{10,... | collective-permute-start | bytes 24584 | tf_op jit(solution)/shard_map/ppermute | solution.py:26
  15.3 4.9 %collective-permute-start.5 = (bf16[4,1024]{1,0:T(4,128)(2,1)S(1)}, bf16[4,1024]{1,0:T(4,128)(2,1)S(1)}, u32[]{:S(2)}, u32[]{:S(2)}) collective-permute-start(bf16[4,1024]{1,0:T(4,128)(2,1)S(1)} %get-tuple-element.23.gated_ref), channel_id=1, source_target_pairs={{0,5},{1,4},{2,7},{3,6},{4,1},{5,0},{6,3},{7,2},{8,13},{9,12},{10,... | collective-permute-start | bytes 24584 | tf_op jit(solution)/shard_map/ppermute | solution.py:26
  15.4 4.7 %collective-permute-start.4 = (bf16[4,1024]{1,0:T(4,128)(2,1)S(1)}, bf16[4,1024]{1,0:T(4,128)(2,1)S(1)}, u32[]{:S(2)}, u32[]{:S(2)}) collective-permute-start(bf16[4,1024]{1,0:T(4,128)(2,1)S(1)} %get-tuple-element.23.gated_ref), channel_id=1, source_target_pairs={{0,3},{1,2},{2,1},{3,0},{4,7},{5,6},{6,5},{7,4},{8,11},{9,10},{10,... | collective-permute-start | bytes 24584 | tf_op jit(solution)/shard_map/ppermute | solution.py:26
  20.4 1.6 %collective-permute-start.8 = (bf16[16,512]{1,0:T(8,128)(2,1)S(1)}, bf16[16,512]{1,0:T(8,128)(2,1)S(1)}, u32[]{:S(2)}, u32[]{:S(2)}) collective-permute-start(bf16[16,512]{1,0:T(8,128)(2,1)S(1)} %get-tuple-element.25), channel_id=1, source_target_pairs={{0,1},{1,0},{2,3},{3,2},{4,5},{5,4},{6,7},{7,6},{8,9},{9,8},{10,11... | collective-permute-start | bytes 49160 | tf_op jit(solution)/shard_map/ppermute | solution.py:19
  22.0 5.2 %copy-start.1 = (bf16[2048,1024]{1,0:T(8,128)(2,1)S(1)}, bf16[2048,1024]{1,0:T(8,128)(2,1)}, u32[]{:S(2)}) copy-start(bf16[2048,1024]{1,0:T(8,128)(2,1)} %refs_3_.5) | copy-start | bytes 12582916
  22.0 5.2 %copy-start.2 = (bf16[1024,2048]{1,0:T(8,128)(2,1)S(1)}, bf16[1024,2048]{1,0:T(8,128)(2,1)}, u32[]{:S(2)}) copy-start(bf16[1024,2048]{1,0:T(8,128)(2,1)} %refs_4_.5) | copy-start | bytes 12582916
  22.0 5.2 %copy-start.4 = (f32[2048]{0:T(1024)S(1)}, f32[2048]{0:T(1024)}, u32[]{:S(2)}) copy-start(f32[2048]{0:T(1024)} %param.25) | copy-start | bytes 24580
  22.0 5.1 %collective-permute-start.9 = (bf16[16,512]{1,0:T(8,128)(2,1)S(1)}, bf16[16,512]{1,0:T(8,128)(2,1)S(1)}, u32[]{:S(2)}, u32[]{:S(2)}) collective-permute-start(bf16[16,512]{1,0:T(8,128)(2,1)S(1)} %shard_map.151.refs_0_.stream_ref), channel_id=1, source_target_pairs={{0,7},{1,6},{2,5},{3,4},{4,3},{5,2},{6,1},{7,0},{8,15},{9,14},{10,... | collective-permute-start | bytes 49160 | tf_op jit(solution)/shard_map/ppermute | solution.py:26
  24.4 4.2 %collective-permute-start.11 = (bf16[16,512]{1,0:T(8,128)(2,1)S(1)}, bf16[16,512]{1,0:T(8,128)(2,1)S(1)}, u32[]{:S(2)}, u32[]{:S(2)}) collective-permute-start(bf16[16,512]{1,0:T(8,128)(2,1)S(1)} %shard_map.151.refs_0_.stream_ref), channel_id=1, source_target_pairs={{0,5},{1,4},{2,7},{3,6},{4,1},{5,0},{6,3},{7,2},{8,13},{9,12},{10,... | collective-permute-start | bytes 49160 | tf_op jit(solution)/shard_map/ppermute | solution.py:26
  25.2 3.4 %collective-permute-start.10 = (bf16[16,512]{1,0:T(8,128)(2,1)S(1)}, bf16[16,512]{1,0:T(8,128)(2,1)S(1)}, u32[]{:S(2)}, u32[]{:S(2)}) collective-permute-start(bf16[16,512]{1,0:T(8,128)(2,1)S(1)} %shard_map.151.refs_0_.stream_ref), channel_id=1, source_target_pairs={{0,3},{1,2},{2,1},{3,0},{4,7},{5,6},{6,5},{7,4},{8,11},{9,10},{10,... | collective-permute-start | bytes 49160 | tf_op jit(solution)/shard_map/ppermute | solution.py:26
  29.5 1.3 %collective-permute-start.12 = (bf16[4,16,256]{2,1,0:T(8,128)(2,1)S(1)}, bf16[4,16,256]{2,1,0:T(8,128)(2,1)S(1)}, u32[]{:S(2)}, u32[]{:S(2)}) collective-permute-start(bf16[4,16,256]{2,1,0:T(8,128)(2,1)S(1)} %get-tuple-element.29), channel_id=1, source_target_pairs={{0,1},{1,0},{2,3},{3,2},{4,5},{5,4},{6,7},{7,6},{8,9},{9,8},{10,11... | collective-permute-start | bytes 98312 | tf_op jit(solution)/shard_map/ppermute | solution.py:19
  30.8 8.2 %collective-permute-start.13 = (bf16[16,256]{1,0:T(8,128)(2,1)S(1)}, bf16[16,256]{1,0:T(8,128)(2,1)S(1)}, u32[]{:S(2)}, u32[]{:S(2)}) collective-permute-start(bf16[16,256]{1,0:T(8,128)(2,1)S(1)} %get-tuple-element.31), channel_id=1, source_target_pairs={{0,3},{1,2},{2,1},{3,0},{4,7},{5,6},{6,5},{7,4},{8,11},{9,10},{10,... | collective-permute-start | bytes 24584 | tf_op jit(solution)/shard_map/ppermute | solution.py:26
  31.6 7.4 %collective-permute-start.14 = (bf16[16,256]{1,0:T(8,128)(2,1)S(1)}, bf16[16,256]{1,0:T(8,128)(2,1)S(1)}, u32[]{:S(2)}, u32[]{:S(2)}) collective-permute-start(bf16[16,256]{1,0:T(8,128)(2,1)S(1)} %get-tuple-element.32), channel_id=1, source_target_pairs={{0,5},{1,4},{2,7},{3,6},{4,1},{5,0},{6,3},{7,2},{8,13},{9,12},{10,... | collective-permute-start | bytes 24584 | tf_op jit(solution)/shard_map/ppermute | solution.py:26
  33.2 5.9 %collective-permute-start.15 = (bf16[16,256]{1,0:T(8,128)(2,1)S(1)}, bf16[16,256]{1,0:T(8,128)(2,1)S(1)}, u32[]{:S(2)}, u32[]{:S(2)}) collective-permute-start(bf16[16,256]{1,0:T(8,128)(2,1)S(1)} %get-tuple-element.33), channel_id=1, source_target_pairs={{0,7},{1,6},{2,5},{3,4},{4,3},{5,2},{6,1},{7,0},{8,15},{9,14},{10,... | collective-permute-start | bytes 24584 | tf_op jit(solution)/shard_map/ppermute | solution.py:26
  (6 other events, 10.4 us)

commit v5 on v4

--- a/solution.py
+++ b/solution.py
@@ -39,48 +39,74 @@
     squares_ref[...] = jnp.zeros_like(squares_ref)
 
 
-def project_kernel(squares_ref, own_ref, other_ref, gain_ref, *refs):
+def put_blocks(total_ref, start, block):
+    seqs = total_ref.shape[1]
+    for d in range(total_ref.shape[0]):
+        total_ref[d, :, start: start + block.shape[1]] = block[d * seqs: (d + 1) * seqs]
+
+
+def project_parts(own, other, gain_ref, weights):
+    _, core = here()
+    half = own.shape[1]
+    scaled = [
+        ((x * gain_ref[:, pl.ds(aligned(side, half), half)]).astype(bf16), pl.ds(aligned(side, half), half))
+        for x, side in ((own, core), (other, 1 - core))
+    ]
+    return [sum(jnp.dot(x, w[rows, :], preferred_element_type=f32) for x, rows in scaled) for w in weights]
+
+
+def early_kernel(squares_ref, own_ref, other_ref, gain_ref, *refs):
     *weights, total = refs
-    weights, outs = weights[:5], weights[5:]
-    count = len(outs)
-    seqs = outs[0].shape[0]
-    me, core = here()
-    half = other_ref.shape[1]
+    start = 0
+    for block in project_parts(own_ref[...].astype(f32), other_ref[...].astype(f32), gain_ref, weights):
+        put_blocks(total, start, block)
+        start += block.shape[1]
+
+
+def late_kernel(count, squares_ref, own_ref, other_ref, gain_ref, early_ref, *refs):
+    weights, outs, total = refs[:-count - 1], refs[-count - 1: -1], refs[-1]
+    me, _ = here()
     own, other = own_ref[...].astype(f32), other_ref[...].astype(f32)
     squares = squares_ref[...] + (
         jnp.sum(own * own, axis=1, keepdims=True) + jnp.sum(other * other, axis=1, keepdims=True))
     high = squares.astype(bf16).astype(f32)
-    own_scaled = (own * gain_ref[:, pl.ds(aligned(core, half), half)]).astype(bf16)
-    other_scaled = (other * gain_ref[:, pl.ds(aligned(1 - core, half), half)]).astype(bf16)
-    own_rows, other_rows = pl.ds(aligned(core, half), half), pl.ds(aligned(1 - core, half), half)
     start = 0
-    blocks = [
-        jnp.dot(own_scaled, w[own_rows, :], preferred_element_type=f32)
-        + jnp.dot(other_scaled, w[other_rows, :], preferred_element_type=f32)
-        for w in weights
-    ] + [high, squares - high]
-    for block in blocks:
-        for d in range(count):
-            total[d, :, start: start + block.shape[1]] = block[d * seqs: (d + 1) * seqs]
+    for block in project_parts(own, other, gain_ref, weights) + [high, squares - high]:
+        put_blocks(total, start, block)
         start += block.shape[1]
+    width = early_ref.shape[2]
     for k, out in zip(range(count - 1, -1, -1), outs):
-        out[...] = total[me ^ k].astype(out.dtype)
-
-
-def project(squares, tokens, other, mix_gain, weights, kv_size):
+        out[:, :width] = early_ref[me ^ k].astype(out.dtype)
+        out[:, width:] = total[me ^ k].astype(out.dtype)
+
+
+def project(squares, tokens, other, mix_gain, early, late, kv_size):
     seqs = other.shape[0] // kv_size
-    width = sum(w.shape[1] for w in weights) + 256
-    outs = [jax.ShapeDtypeStruct((seqs, width), f32 if k == 0 else bf16) for k in range(kv_size - 1, -1, -1)]
-    return pl.pallas_call(
-        project_kernel,
+    params = dict(
+        compiler_params=pltpu.CompilerParams(vmem_limit_bytes=6 * 2**20),
+    )
+    gain = mix_gain.reshape(1, -1)
+    width, rest = sum(w.shape[1] for w in early), sum(w.shape[1] for w in late) + 256
+    first = pl.pallas_call(
+        early_kernel,
+        out_shape=jax.ShapeDtypeStruct((kv_size, seqs, width), f32),
+        in_specs=[VMEM] * (4 + len(early)),
+        out_specs=VMEM,
+        cost_estimate=LIGHT,
+        name="early",
+        **params,
+    )(squares, tokens, other, gain, *early)
+    outs = [jax.ShapeDtypeStruct((seqs, width + rest), f32 if k == 0 else bf16) for k in range(kv_size - 1, -1, -1)]
+    return pl.pallas_call(
+        functools.partial(late_kernel, kv_size),
         out_shape=outs,
-        in_specs=[VMEM] * (4 + len(weights)),
+        in_specs=[VMEM] * (5 + len(late)),
         out_specs=[VMEM] * kv_size,
-        scratch_shapes=[pltpu.VMEM((kv_size, seqs, width), f32)],
-        compiler_params=pltpu.CompilerParams(vmem_limit_bytes=8 * 2**20),
+        scratch_shapes=[pltpu.VMEM((kv_size, seqs, rest), f32)],
         cost_estimate=HEAVY,
-        name="project",
-    )(squares, tokens, other, mix_gain.reshape(1, -1), *weights)[::-1]
+        name="late",
+        **params,
+    )(squares, tokens, other, gain, first, *late)[::-1]
 
 
 def narrow_kernel(state_ref, out_ref):
@@ -111,9 +137,9 @@
     base = 3 * kw + 2 * vw
     sums = summed(base, 128)[:, :1] + summed(base + 128, 128)[:, :1]
     row_scale = lax.rsqrt(sums / depth + epsilon)
-    queries = summed(0, kw) * row_scale * keys ** (-0.5)
-    new_keys = summed(kw, kw) * row_scale
-    retain = jax.nn.sigmoid(summed(2 * kw, kw) * row_scale + offset_ref[...])
+    queries = summed(2 * vw, kw) * row_scale * keys ** (-0.5)
+    new_keys = summed(2 * vw + kw, kw) * row_scale
+    retain = jax.nn.sigmoid(summed(2 * vw + 2 * kw, kw) * row_scale + offset_ref[...])
     kept = (queries * retain).astype(bf16)
     row = lax.broadcasted_iota(jnp.int32, (seqs, 1), 0)
     reads = []
@@ -124,8 +150,8 @@
             product = jnp.dot(kept[:, at], state_ref[b, h], preferred_element_type=f32)
             read += jnp.where(row == b, product, 0.0)
         reads.append(read)
-    values = summed(3 * kw, vw) * row_scale
-    gates = summed(3 * kw + vw, vw) * row_scale
+    values = summed(0, vw) * row_scale
+    gates = summed(vw, vw) * row_scale
     silu = gates * jax.nn.sigmoid(gates)
     for h in range(heads):
         at, to = slice(h * keys, (h + 1) * keys), slice(h * vals, (h + 1) * vals)
@@ -337,7 +363,7 @@
     like = jax.ShapeDtypeStruct
     other = swap_cores(tokens)
     squares = small(clear_kernel, like((rows, 128), f32))
-    parts = spread(project(squares, tokens, other, mix_gain, weights, kv_size), kv_size, 0)
+    parts = spread(project(squares, tokens, other, mix_gain, weights[3:], weights[:3], kv_size), kv_size, 0)
     narrowed = narrow(state)
     gated, factors, values = readout(parts, state, narrowed, decay_offset, head_gain, depth)
     arrived = spread([gated] * kv_size, kv_size, 1)

time: 39.8 us -> 39.6 us (level)
  no operation moved by 1% of the time
where the time goes in v5:
time: 39.6 us; the launch traced here: 39.4 us
  starting transfers between devices  17.3 us (44%)
  waiting for transfers between devices  12.9 us (33%)
  Pallas kernels  8.2 us (21%)
  between operations  0.88 us (2%)
    ppermute x12, starting transfers between devices, spread(): came.append(lax.ppermute(pieces[k], ('kv', 'tp'), pairs))  15.8 us
    ppermute x12, waiting for transfers between devices, spread(): came.append(lax.ppermute(pieces[k], ('kv', 'tp'), pairs))  10 us
    pallas_call x3, Pallas kernels, update(): pl.pallas_call(functools.partial(update_kernel, first, count), out_shape=...  4.24 us
    ppermute x4, waiting for transfers between devices, swap_cores(): return lax.ppermute(value, 'tp', [(0, 1), (1, 0)])  2.92 us
    ppermute x4, starting transfers between devices, swap_cores(): return lax.ppermute(value, 'tp', [(0, 1), (1, 0)])  1.52 us
    pallas_call x1, Pallas kernels, mixer(): pl.pallas_call(functools.partial(mixer_kernel, late), out_shape=outs, in_...  0.96 us
    pallas_call x5, Pallas kernels, small(): pl.pallas_call(body, out_shape=outs, in_specs=[VMEM] * len(args), out_spe...  0.87 us
  transfers between devices with their start and end apart: 16, of which 8 were waited for; matrix products, arithmetic and copies ran while one was open for 0% of the time, Pallas kernels for 14%

profile of v5, /device:TPU:0, one launch (start us, length us, event | category | flops | bytes accessed | tf_op | source)
XLA Modules:
  0.0 39.4 jit_solution(12625198862109685775)
XLA Ops:
  0.7 0.6 %collective-permute-start = (bf16[16,256]{1,0:T(8,128)(2,1)}, bf16[16,256]{1,0:T(8,128)(2,1)S(1)}, u32[]{:S(2)}, u32[]{:S(2)}) collective-permute-start(bf16[16,256]{1,0:T(8,128)(2,1)} %own_ref.5), channel_id=1, source_target_pairs={{0,1},{1,0},{2,3},{3,2},{4,5},{5,4},{6,7},{7,6},{8,9},{9,8},{10,11... | collective-permute-start | bytes 24584 | tf_op jit(solution)/shard_map/ppermute | solution.py:19
  1.3 1.0 %collective-permute-done.other_ref = bf16[16,256]{1,0:T(8,128)(2,1)S(1)} collective-permute-done((bf16[16,256]{1,0:T(8,128)(2,1)}, bf16[16,256]{1,0:T(8,128)(2,1)S(1)}, u32[]{:S(2)}, u32[]{:S(2)}) %collective-permute-start) | collective-permute-done | bytes 8224 | tf_op jit(solution)/shard_map/ppermute | solution.py:19
  3.1 3.0 %collective-permute-start.1 = (bf16[4,3840]{1,0:T(4,128)(2,1)S(1)}, bf16[4,3840]{1,0:T(4,128)(2,1)S(1)}, u32[]{:S(2)}, u32[]{:S(2)}) collective-permute-start(bf16[4,3840]{1,0:T(4,128)(2,1)S(1)} %get-tuple-element.20), channel_id=1, source_target_pairs={{0,2},{1,3},{2,0},{3,1},{4,6},{5,7},{6,4},{7,5},{8,10},{9,11},{10,... | collective-permute-start | bytes 92168 | tf_op jit(solution)/shard_map/ppermute | solution.py:26
  6.1 2.6 %collective-permute-start.2 = (bf16[4,3840]{1,0:T(4,128)(2,1)S(1)}, bf16[4,3840]{1,0:T(4,128)(2,1)S(1)}, u32[]{:S(2)}, u32[]{:S(2)}) collective-permute-start(bf16[4,3840]{1,0:T(4,128)(2,1)S(1)} %get-tuple-element.21), channel_id=1, source_target_pairs={{0,4},{1,5},{2,6},{3,7},{4,0},{5,1},{6,2},{7,3},{8,12},{9,13},{10,... | collective-permute-start | bytes 92168 | tf_op jit(solution)/shard_map/ppermute | solution.py:26
  9.0 2.5 %collective-permute-done.2.refs_2_ = bf16[4,3840]{1,0:T(4,128)(2,1)S(1)} collective-permute-done((bf16[4,3840]{1,0:T(4,128)(2,1)S(1)}, bf16[4,3840]{1,0:T(4,128)(2,1)S(1)}, u32[]{:S(2)}, u32[]{:S(2)}) %collective-permute-start.2) | collective-permute-done | bytes 30752 | tf_op jit(solution)/shard_map/ppermute | solution.py:26
  11.5 3.0 %collective-permute-done.3.refs_3_ = bf16[4,3840]{1,0:T(4,128)(2,1)S(1)} collective-permute-done((bf16[4,3840]{1,0:T(4,128)(2,1)S(1)}, bf16[4,3840]{1,0:T(4,128)(2,1)S(1)}, u32[]{:S(2)}, u32[]{:S(2)}) %collective-permute-start.3) | collective-permute-done | bytes 30752 | tf_op jit(solution)/shard_map/ppermute | solution.py:26
  15.1 2.0 %collective-permute-start.4 = (bf16[4,1024]{1,0:T(4,128)(2,1)S(1)}, bf16[4,1024]{1,0:T(4,128)(2,1)S(1)}, u32[]{:S(2)}, u32[]{:S(2)}) collective-permute-start(bf16[4,1024]{1,0:T(4,128)(2,1)S(1)} %get-tuple-element.23.gated_ref), channel_id=1, source_target_pairs={{0,3},{1,2},{2,1},{3,0},{4,7},{5,6},{6,5},{7,4},{8,11},{9,10},{10,... | collective-permute-start | bytes 24584 | tf_op jit(solution)/shard_map/ppermute | solution.py:26
  17.3 2.5 %collective-permute-done.6.refs_2_ = bf16[4,1024]{1,0:T(4,128)(2,1)S(1)} collective-permute-done((bf16[4,1024]{1,0:T(4,128)(2,1)S(1)}, bf16[4,1024]{1,0:T(4,128)(2,1)S(1)}, u32[]{:S(2)}, u32[]{:S(2)}) %collective-permute-start.6) | collective-permute-done | bytes 8224 | tf_op jit(solution)/shard_map/ppermute | solution.py:26
  20.1 0.7 %collective-permute-start.8 = (bf16[16,512]{1,0:T(8,128)(2,1)S(1)}, bf16[16,512]{1,0:T(8,128)(2,1)S(1)}, u32[]{:S(2)}, u32[]{:S(2)}) collective-permute-start(bf16[16,512]{1,0:T(8,128)(2,1)S(1)} %get-tuple-element.25), channel_id=1, source_target_pairs={{0,1},{1,0},{2,3},{3,2},{4,5},{5,4},{6,7},{7,6},{8,9},{9,8},{10,11... | collective-permute-start | bytes 49160 | tf_op jit(solution)/shard_map/ppermute | solution.py:19
  20.9 0.8 %collective-permute-done.8.came_ref = bf16[16,512]{1,0:T(8,128)(2,1)S(1)} collective-permute-done((bf16[16,512]{1,0:T(8,128)(2,1)S(1)}, bf16[16,512]{1,0:T(8,128)(2,1)S(1)}, u32[]{:S(2)}, u32[]{:S(2)}) %collective-permute-start.8) | collective-permute-done | bytes 16416 | tf_op jit(solution)/shard_map/ppermute | solution.py:19
  21.7 2.4 %collective-permute-start.9 = (bf16[16,512]{1,0:T(8,128)(2,1)S(1)}, bf16[16,512]{1,0:T(8,128)(2,1)S(1)}, u32[]{:S(2)}, u32[]{:S(2)}) collective-permute-start(bf16[16,512]{1,0:T(8,128)(2,1)S(1)} %shard_map.151.refs_0_.stream_ref), channel_id=1, source_target_pairs={{0,7},{1,6},{2,5},{3,4},{4,3},{5,2},{6,1},{7,0},{8,15},{9,14},{10,... | collective-permute-start | bytes 49160 | tf_op jit(solution)/shard_map/ppermute | solution.py:26
  24.1 0.8 %collective-permute-start.11 = (bf16[16,512]{1,0:T(8,128)(2,1)S(1)}, bf16[16,512]{1,0:T(8,128)(2,1)S(1)}, u32[]{:S(2)}, u32[]{:S(2)}) collective-permute-start(bf16[16,512]{1,0:T(8,128)(2,1)S(1)} %shard_map.151.refs_0_.stream_ref), channel_id=1, source_target_pairs={{0,5},{1,4},{2,7},{3,6},{4,1},{5,0},{6,3},{7,2},{8,13},{9,12},{10,... | collective-permute-start | bytes 49160 | tf_op jit(solution)/shard_map/ppermute | solution.py:26
  25.0 0.9 %collective-permute-start.10 = (bf16[16,512]{1,0:T(8,128)(2,1)S(1)}, bf16[16,512]{1,0:T(8,128)(2,1)S(1)}, u32[]{:S(2)}, u32[]{:S(2)}) collective-permute-start(bf16[16,512]{1,0:T(8,128)(2,1)S(1)} %shard_map.151.refs_0_.stream_ref), channel_id=1, source_target_pairs={{0,3},{1,2},{2,1},{3,0},{4,7},{5,6},{6,5},{7,4},{8,11},{9,10},{10,... | collective-permute-start | bytes 49160 | tf_op jit(solution)/shard_map/ppermute | solution.py:26
  25.9 1.0 %collective-permute-done.9.refs_1_ = bf16[16,512]{1,0:T(8,128)(2,1)S(1)} collective-permute-done((bf16[16,512]{1,0:T(8,128)(2,1)S(1)}, bf16[16,512]{1,0:T(8,128)(2,1)S(1)}, u32[]{:S(2)}, u32[]{:S(2)}) %collective-permute-start.9) | collective-permute-done | bytes 16416 | tf_op jit(solution)/shard_map/ppermute | solution.py:26
  27.3 1.0 %collective-permute-done.11.refs_1_ = bf16[16,512]{1,0:T(8,128)(2,1)S(1)} collective-permute-done((bf16[16,512]{1,0:T(8,128)(2,1)S(1)}, bf16[16,512]{1,0:T(8,128)(2,1)S(1)}, u32[]{:S(2)}, u32[]{:S(2)}) %collective-permute-start.11) | collective-permute-done | bytes 16416 | tf_op jit(solution)/shard_map/ppermute | solution.py:26
  28.3 1.0 %mixer.1 = (f32[4,16,256]{2,1,0:T(8,128)S(1)}, bf16[4,16,256]{2,1,0:T(8,128)(2,1)S(1)}) custom-call(f32[16,128]{1,0:T(8,128)S(1)} %get-tuple-element.26.squares_ref, f32[16,1024]{1,0:T(8,128)S(1)} %get-tuple-element.27.hidden_ref, bf16[16,512]{1,0:T(8,128)(2,1)S(1)} %collective-permute-done.10.refs_0_, bf16[16,512]{1,0:T(8,128)(2,1)S(1)} %collective-permute-done.11.refs_1_, ...), custom_call_target="tpu_custom_call" | custom-call | flops 131072 | bytes 131072 | tf_op jit(solution)/shard_map/mixer/pallas_call | solution.py:316
  29.5 1.0 %collective-permute-done.12.came_ref = bf16[4,16,256]{2,1,0:T(8,128)(2,1)S(1)} collective-permute-done((bf16[4,16,256]{2,1,0:T(8,128)(2,1)S(1)}, bf16[4,16,256]{2,1,0:T(8,128)(2,1)S(1)}, u32[]{:S(2)}, u32[]{:S(2)}) %collective-permute-start.12) | collective-permute-done | bytes 32800 | tf_op jit(solution)/shard_map/ppermute | solution.py:19
  30.6 0.8 %collective-permute-start.13 = (bf16[16,256]{1,0:T(8,128)(2,1)S(1)}, bf16[16,256]{1,0:T(8,128)(2,1)S(1)}, u32[]{:S(2)}, u32[]{:S(2)}) collective-permute-start(bf16[16,256]{1,0:T(8,128)(2,1)S(1)} %get-tuple-element.31), channel_id=1, source_target_pairs={{0,3},{1,2},{2,1},{3,0},{4,7},{5,6},{6,5},{7,4},{8,11},{9,10},{10,... | collective-permute-start | bytes 24584 | tf_op jit(solution)/shard_map/ppermute | solution.py:26
  31.3 1.6 %collective-permute-start.14 = (bf16[16,256]{1,0:T(8,128)(2,1)S(1)}, bf16[16,256]{1,0:T(8,128)(2,1)S(1)}, u32[]{:S(2)}, u32[]{:S(2)}) collective-permute-start(bf16[16,256]{1,0:T(8,128)(2,1)S(1)} %get-tuple-element.32), channel_id=1, source_target_pairs={{0,5},{1,4},{2,7},{3,6},{4,1},{5,0},{6,3},{7,2},{8,13},{9,12},{10,... | collective-permute-start | bytes 24584 | tf_op jit(solution)/shard_map/ppermute | solution.py:26
  32.9 1.6 %collective-permute-start.15 = (bf16[16,256]{1,0:T(8,128)(2,1)S(1)}, bf16[16,256]{1,0:T(8,128)(2,1)S(1)}, u32[]{:S(2)}, u32[]{:S(2)}) collective-permute-start(bf16[16,256]{1,0:T(8,128)(2,1)S(1)} %get-tuple-element.33), channel_id=1, source_target_pairs={{0,7},{1,6},{2,5},{3,4},{4,3},{5,2},{6,1},{7,0},{8,15},{9,14},{10,... | collective-permute-start | bytes 24584 | tf_op jit(solution)/shard_map/ppermute | solution.py:26
  34.5 1.3 %update.3.refs_0_ = f32[4,2,256,512]{3,2,1,0:T(8,128)} custom-call(f32[2,4,512]{2,1,0:T(4,128)S(1)} %get-tuple-element.34.factors_ref, f32[4,1024]{1,0:T(4,128)S(1)} %get-tuple-element.35.values_ref, f32[4,2,256,512]{3,2,1,0:T(8,128)S(1)} %copy-done), custom_call_target="tpu_custom_call" | custom-call | flops 131072 | bytes 131072 | tf_op jit(solution)/shard_map/update/pallas_call | solution.py:206
  35.8 1.3 %update.4.refs_0_ = f32[4,2,256,512]{3,2,1,0:T(8,128)} custom-call(f32[2,4,512]{2,1,0:T(4,128)S(1)} %get-tuple-element.34.factors_ref, f32[4,1024]{1,0:T(4,128)S(1)} %get-tuple-element.35.values_ref, f32[4,2,256,512]{3,2,1,0:T(8,128)S(1)} %copy-done, f32[4,2,256,512]{3,2,1,0:T(8,128)} %update.3.refs_0_), custom_call_target="tpu_custom_call", output_to_operand_aliasing={{}: (3, {})} | custom-call | flops 131072 | bytes 131072 | tf_op jit(solution)/shard_map/update/pallas_call | solution.py:206
  37.1 1.7 %update.5 = f32[4,2,256,512]{3,2,1,0:T(8,128)} custom-call(f32[2,4,512]{2,1,0:T(4,128)S(1)} %get-tuple-element.34.factors_ref, f32[4,1024]{1,0:T(4,128)S(1)} %get-tuple-element.35.values_ref, f32[4,2,256,512]{3,2,1,0:T(8,128)S(1)} %copy-done, f32[4,2,256,512]{3,2,1,0:T(8,128)} %update.4.refs_0_), custom_call_target="tpu_custom_call", output_to_operand_aliasing={{}: (3, {})} | custom-call | flops 131072 | bytes 131072 | tf_op jit(solution)/shard_map/update/pallas_call | solution.py:206
  38.8 0.6 %shard_map.153 = bf16[16,256]{1,0:T(8,128)(2,1)} custom-call(bf16[16,512]{1,0:T(8,128)(2,1)S(1)} %shard_map.151.refs_0_.stream_ref, f32[16,256]{1,0:T(8,128)S(1)} %get-tuple-element.30.refs_0_, bf16[16,256]{1,0:T(8,128)(2,1)S(1)} %collective-permute-done.13.refs_1_, bf16[16,256]{1,0:T(8,128)(2,1)S(1)} %collective-permute-done.14.refs_2_, ...), custom_call_target="tpu_custom_call" | custom-call | flops 20000000000 | bytes 1048576 | tf_op jit(solution)/shard_map/pallas_call | solution.py:350
  (51 shorter events, 2.8 us)
Async XLA Ops:
  0.7 2.0 %copy-start.11 = (bf16[512,512]{1,0:T(8,128)(2,1)S(1)}, bf16[512,512]{1,0:T(8,128)(2,1)}, u32[]{:S(2)}) copy-start(bf16[512,512]{1,0:T(8,128)(2,1)} %refs_2_.1) | copy-start | bytes 1572868
  0.7 1.6 %collective-permute-start = (bf16[16,256]{1,0:T(8,128)(2,1)}, bf16[16,256]{1,0:T(8,128)(2,1)S(1)}, u32[]{:S(2)}, u32[]{:S(2)}) collective-permute-start(bf16[16,256]{1,0:T(8,128)(2,1)} %own_ref.5), channel_id=1, source_target_pairs={{0,1},{1,0},{2,3},{3,2},{4,5},{5,4},{6,7},{7,6},{8,9},{9,8},{10,11... | collective-permute-start | bytes 24584 | tf_op jit(solution)/shard_map/ppermute | solution.py:19
  2.7 6.0 %copy-start.5 = (bf16[1024,512]{1,0:T(8,128)(2,1)S(1)}, bf16[1024,512]{1,0:T(8,128)(2,1)}, u32[]{:S(2)}) copy-start(bf16[1024,512]{1,0:T(8,128)(2,1)} %w_ref.1) | copy-start | bytes 3145732
  2.7 6.0 %copy-start = (f32[4,2,256,512]{3,2,1,0:T(8,128)S(1)}, f32[4,2,256,512]{3,2,1,0:T(8,128)}, u32[]{:S(2)}) copy-start(f32[4,2,256,512]{3,2,1,0:T(8,128)} %state_ref.7) | copy-start | bytes 12582916
  3.1 11.3 %copy-start.12 = (f32[512]{0:T(512)S(1)}, f32[512]{0:T(512)}, u32[]{:S(2)}) copy-start(f32[512]{0:T(512)} %param.22) | copy-start | bytes 6148
  3.1 11.3 %copy-start.13 = (f32[512]{0:T(512)S(1)}, f32[512]{0:T(512)}, u32[]{:S(2)}) copy-start(f32[512]{0:T(512)} %param.23) | copy-start | bytes 6148
  3.1 5.8 %collective-permute-start.1 = (bf16[4,3840]{1,0:T(4,128)(2,1)S(1)}, bf16[4,3840]{1,0:T(4,128)(2,1)S(1)}, u32[]{:S(2)}, u32[]{:S(2)}) collective-permute-start(bf16[4,3840]{1,0:T(4,128)(2,1)S(1)} %get-tuple-element.20), channel_id=1, source_target_pairs={{0,2},{1,3},{2,0},{3,1},{4,6},{5,7},{6,4},{7,5},{8,10},{9,11},{10,... | collective-permute-start | bytes 92168 | tf_op jit(solution)/shard_map/ppermute | solution.py:26
  6.1 5.3 %collective-permute-start.2 = (bf16[4,3840]{1,0:T(4,128)(2,1)S(1)}, bf16[4,3840]{1,0:T(4,128)(2,1)S(1)}, u32[]{:S(2)}, u32[]{:S(2)}) collective-permute-start(bf16[4,3840]{1,0:T(4,128)(2,1)S(1)} %get-tuple-element.21), channel_id=1, source_target_pairs={{0,4},{1,5},{2,6},{3,7},{4,0},{5,1},{6,2},{7,3},{8,12},{9,13},{10,... | collective-permute-start | bytes 92168 | tf_op jit(solution)/shard_map/ppermute | solution.py:26
  8.7 5.7 %collective-permute-start.3 = (bf16[4,3840]{1,0:T(4,128)(2,1)S(1)}, bf16[4,3840]{1,0:T(4,128)(2,1)S(1)}, u32[]{:S(2)}, u32[]{:S(2)}) collective-permute-start(bf16[4,3840]{1,0:T(4,128)(2,1)S(1)} %get-tuple-element.22), channel_id=1, source_target_pairs={{0,6},{1,7},{2,4},{3,5},{4,2},{5,3},{6,0},{7,1},{8,14},{9,15},{10,... | collective-permute-start | bytes 92168 | tf_op jit(solution)/shard_map/ppermute | solution.py:26
  8.7 11.1 %collective-permute-start.7 = (bf16[1024,512]{1,0:T(8,128)(2,1)S(1)}, bf16[1024,512]{1,0:T(8,128)(2,1)S(1)}, u32[]{:S(2)}, u32[]{:S(2)}) collective-permute-start(bf16[1024,512]{1,0:T(8,128)(2,1)S(1)} %copy-done.5), channel_id=1, source_target_pairs={{0,1},{1,0},{2,3},{3,2},{4,5},{5,4},{6,7},{7,6},{8,9},{9,8},{10,11... | collective-permute-start | bytes 3145736 | tf_op jit(solution)/shard_map/ppermute | solution.py:19
  15.0 4.9 %collective-permute-start.6 = (bf16[4,1024]{1,0:T(4,128)(2,1)S(1)}, bf16[4,1024]{1,0:T(4,128)(2,1)S(1)}, u32[]{:S(2)}, u32[]{:S(2)}) collective-permute-start(bf16[4,1024]{1,0:T(4,128)(2,1)S(1)} %get-tuple-element.23.gated_ref), channel_id=1, source_target_pairs={{0,7},{1,6},{2,5},{3,4},{4,3},{5,2},{6,1},{7,0},{8,15},{9,14},{10,... | collective-permute-start | bytes 24584 | tf_op jit(solution)/shard_map/ppermute | solution.py:26
  15.0 4.9 %collective-permute-start.5 = (bf16[4,1024]{1,0:T(4,128)(2,1)S(1)}, bf16[4,1024]{1,0:T(4,128)(2,1)S(1)}, u32[]{:S(2)}, u32[]{:S(2)}) collective-permute-start(bf16[4,1024]{1,0:T(4,128)(2,1)S(1)} %get-tuple-element.23.gated_ref), channel_id=1, source_target_pairs={{0,5},{1,4},{2,7},{3,6},{4,1},{5,0},{6,3},{7,2},{8,13},{9,12},{10,... | collective-permute-start | bytes 24584 | tf_op jit(solution)/shard_map/ppermute | solution.py:26
  15.1 4.8 %collective-permute-start.4 = (bf16[4,1024]{1,0:T(4,128)(2,1)S(1)}, bf16[4,1024]{1,0:T(4,128)(2,1)S(1)}, u32[]{:S(2)}, u32[]{:S(2)}) collective-permute-start(bf16[4,1024]{1,0:T(4,128)(2,1)S(1)} %get-tuple-element.23.gated_ref), channel_id=1, source_target_pairs={{0,3},{1,2},{2,1},{3,0},{4,7},{5,6},{6,5},{7,4},{8,11},{9,10},{10,... | collective-permute-start | bytes 24584 | tf_op jit(solution)/shard_map/ppermute | solution.py:26
  20.1 1.6 %collective-permute-start.8 = (bf16[16,512]{1,0:T(8,128)(2,1)S(1)}, bf16[16,512]{1,0:T(8,128)(2,1)S(1)}, u32[]{:S(2)}, u32[]{:S(2)}) collective-permute-start(bf16[16,512]{1,0:T(8,128)(2,1)S(1)} %get-tuple-element.25), channel_id=1, source_target_pairs={{0,1},{1,0},{2,3},{3,2},{4,5},{5,4},{6,7},{7,6},{8,9},{9,8},{10,11... | collective-permute-start | bytes 49160 | tf_op jit(solution)/shard_map/ppermute | solution.py:19
  21.7 5.2 %copy-start.1 = (bf16[2048,1024]{1,0:T(8,128)(2,1)S(1)}, bf16[2048,1024]{1,0:T(8,128)(2,1)}, u32[]{:S(2)}) copy-start(bf16[2048,1024]{1,0:T(8,128)(2,1)} %refs_3_.3) | copy-start | bytes 12582916
  21.7 5.2 %copy-start.2 = (bf16[1024,2048]{1,0:T(8,128)(2,1)S(1)}, bf16[1024,2048]{1,0:T(8,128)(2,1)}, u32[]{:S(2)}) copy-start(bf16[1024,2048]{1,0:T(8,128)(2,1)} %refs_4_.3) | copy-start | bytes 12582916
  21.7 5.2 %copy-start.6 = (f32[2048]{0:T(1024)S(1)}, f32[2048]{0:T(1024)}, u32[]{:S(2)}) copy-start(f32[2048]{0:T(1024)} %param.25) | copy-start | bytes 24580
  21.7 5.1 %collective-permute-start.9 = (bf16[16,512]{1,0:T(8,128)(2,1)S(1)}, bf16[16,512]{1,0:T(8,128)(2,1)S(1)}, u32[]{:S(2)}, u32[]{:S(2)}) collective-permute-start(bf16[16,512]{1,0:T(8,128)(2,1)S(1)} %shard_map.151.refs_0_.stream_ref), channel_id=1, source_target_pairs={{0,7},{1,6},{2,5},{3,4},{4,3},{5,2},{6,1},{7,0},{8,15},{9,14},{10,... | collective-permute-start | bytes 49160 | tf_op jit(solution)/shard_map/ppermute | solution.py:26
  24.1 4.2 %collective-permute-start.11 = (bf16[16,512]{1,0:T(8,128)(2,1)S(1)}, bf16[16,512]{1,0:T(8,128)(2,1)S(1)}, u32[]{:S(2)}, u32[]{:S(2)}) collective-permute-start(bf16[16,512]{1,0:T(8,128)(2,1)S(1)} %shard_map.151.refs_0_.stream_ref), channel_id=1, source_target_pairs={{0,5},{1,4},{2,7},{3,6},{4,1},{5,0},{6,3},{7,2},{8,13},{9,12},{10,... | collective-permute-start | bytes 49160 | tf_op jit(solution)/shard_map/ppermute | solution.py:26
  25.0 3.4 %collective-permute-start.10 = (bf16[16,512]{1,0:T(8,128)(2,1)S(1)}, bf16[16,512]{1,0:T(8,128)(2,1)S(1)}, u32[]{:S(2)}, u32[]{:S(2)}) collective-permute-start(bf16[16,512]{1,0:T(8,128)(2,1)S(1)} %shard_map.151.refs_0_.stream_ref), channel_id=1, source_target_pairs={{0,3},{1,2},{2,1},{3,0},{4,7},{5,6},{6,5},{7,4},{8,11},{9,10},{10,... | collective-permute-start | bytes 49160 | tf_op jit(solution)/shard_map/ppermute | solution.py:26
  29.3 1.3 %collective-permute-start.12 = (bf16[4,16,256]{2,1,0:T(8,128)(2,1)S(1)}, bf16[4,16,256]{2,1,0:T(8,128)(2,1)S(1)}, u32[]{:S(2)}, u32[]{:S(2)}) collective-permute-start(bf16[4,16,256]{2,1,0:T(8,128)(2,1)S(1)} %get-tuple-element.29), channel_id=1, source_target_pairs={{0,1},{1,0},{2,3},{3,2},{4,5},{5,4},{6,7},{7,6},{8,9},{9,8},{10,11... | collective-permute-start | bytes 98312 | tf_op jit(solution)/shard_map/ppermute | solution.py:19
  30.6 8.2 %collective-permute-start.13 = (bf16[16,256]{1,0:T(8,128)(2,1)S(1)}, bf16[16,256]{1,0:T(8,128)(2,1)S(1)}, u32[]{:S(2)}, u32[]{:S(2)}) collective-permute-start(bf16[16,256]{1,0:T(8,128)(2,1)S(1)} %get-tuple-element.31), channel_id=1, source_target_pairs={{0,3},{1,2},{2,1},{3,0},{4,7},{5,6},{6,5},{7,4},{8,11},{9,10},{10,... | collective-permute-start | bytes 24584 | tf_op jit(solution)/shard_map/ppermute | solution.py:26
  31.3 7.4 %collective-permute-start.14 = (bf16[16,256]{1,0:T(8,128)(2,1)S(1)}, bf16[16,256]{1,0:T(8,128)(2,1)S(1)}, u32[]{:S(2)}, u32[]{:S(2)}) collective-permute-start(bf16[16,256]{1,0:T(8,128)(2,1)S(1)} %get-tuple-element.32), channel_id=1, source_target_pairs={{0,5},{1,4},{2,7},{3,6},{4,1},{5,0},{6,3},{7,2},{8,13},{9,12},{10,... | collective-permute-start | bytes 24584 | tf_op jit(solution)/shard_map/ppermute | solution.py:26
  32.9 5.9 %collective-permute-start.15 = (bf16[16,256]{1,0:T(8,128)(2,1)S(1)}, bf16[16,256]{1,0:T(8,128)(2,1)S(1)}, u32[]{:S(2)}, u32[]{:S(2)}) collective-permute-start(bf16[16,256]{1,0:T(8,128)(2,1)S(1)} %get-tuple-element.33), channel_id=1, source_target_pairs={{0,7},{1,6},{2,5},{3,4},{4,3},{5,2},{6,1},{7,0},{8,15},{9,14},{10,... | collective-permute-start | bytes 24584 | tf_op jit(solution)/shard_map/ppermute | solution.py:26
  (6 other events, 10.7 us)

commit v6 on v5

--- a/solution.py
+++ b/solution.py
@@ -190,14 +190,13 @@
     columns = jnp.concatenate(rows, axis=0).T
     copies = []
     for n in range(count):
-        b = first + n
-        for h in range(heads):
-            at = slice(h * keys, (h + 1) * keys)
-            keep, key = columns[at, b: b + 1], columns[at, seqs + b: seqs + b + 1]
-            value = values_ref[b: b + 1, h * vals: (h + 1) * vals]
-            tiles[n, h] = keep * state_ref[b, h] + key * value
-            copies.append(pltpu.make_async_copy(tiles.at[n, h], out_hbm.at[b, h], sems.at[n, h]))
-            copies[-1].start()
+        b, h = divmod(first + n, heads)
+        at = slice(h * keys, (h + 1) * keys)
+        keep, key = columns[at, b: b + 1], columns[at, seqs + b: seqs + b + 1]
+        value = values_ref[b: b + 1, h * vals: (h + 1) * vals]
+        tiles[n] = keep * state_ref[b, h] + key * value
+        copies.append(pltpu.make_async_copy(tiles.at[n], out_hbm.at[b, h], sems.at[n]))
+        copies[-1].start()
     for copy in copies:
         copy.wait()
 
@@ -208,7 +207,7 @@
         out_shape=jax.ShapeDtypeStruct(state.shape, f32),
         in_specs=[VMEM, VMEM, VMEM] + [pl.BlockSpec(memory_space=pl.ANY)] * len(written),
         out_specs=pl.BlockSpec(memory_space=pl.ANY),
-        scratch_shapes=[pltpu.VMEM((count, *state.shape[1:]), f32), pltpu.SemaphoreType.DMA((count, state.shape[1]))],
+        scratch_shapes=[pltpu.VMEM((count, *state.shape[2:]), f32), pltpu.SemaphoreType.DMA((count,))],
         input_output_aliases={3: 0} if written else {},
         compiler_params=pltpu.CompilerParams(vmem_limit_bytes=8 * 2**20),
         cost_estimate=LIGHT,
@@ -368,8 +367,8 @@
     gated, factors, values = readout(parts, state, narrowed, decay_offset, head_gain, depth)
     arrived = spread([gated] * kv_size, kv_size, 1)
     new_state = update(factors, values, state, 0, 1)
-    new_state = update(factors, values, state, 1, 1, new_state)
-    new_state = update(factors, values, state, 2, 2, new_state)
+    new_state = update(factors, values, state, 1, 3, new_state)
+    new_state = update(factors, values, state, 4, 4, new_state)
     w_other = swap_cores(w_out)
     branch, branch_sent = branch_of(arrived, w_out, w_other)
     stream = small(stream_kernel, like((rows, 2 * half), bf16), branch, swap_cores(branch_sent), tokens, other)

time: 39.6 us -> 39.5 us (level)
  no operation moved by 1% of the time
where the time goes in v6:
time: 39.5 us; the launch traced here: 39.4 us
  starting transfers between devices  17.3 us (44%)
  waiting for transfers between devices  12.9 us (33%)
  Pallas kernels  8.16 us (21%)
  between operations  0.88 us (2%)
    ppermute x12, starting transfers between devices, spread(): came.append(lax.ppermute(pieces[k], ('kv', 'tp'), pairs))  15.8 us
    ppermute x12, waiting for transfers between devices, spread(): came.append(lax.ppermute(pieces[k], ('kv', 'tp'), pairs))  10 us
    pallas_call x3, Pallas kernels, update(): pl.pallas_call(functools.partial(update_kernel, first, count), out_shape=...  4.21 us
    ppermute x4, waiting for transfers between devices, swap_cores(): return lax.ppermute(value, 'tp', [(0, 1), (1, 0)])  2.92 us
    ppermute x4, starting transfers between devices, swap_cores(): return lax.ppermute(value, 'tp', [(0, 1), (1, 0)])  1.52 us
    pallas_call x1, Pallas kernels, mixer(): pl.pallas_call(functools.partial(mixer_kernel, late), out_shape=outs, in_...  0.96 us
    pallas_call x5, Pallas kernels, small(): pl.pallas_call(body, out_shape=outs, in_specs=[VMEM] * len(args), out_spe...  0.87 us
  transfers between devices with their start and end apart: 16, of which 8 were waited for; matrix products, arithmetic and copies ran while one was open for 0% of the time, Pallas kernels for 14%

profile of v6, /device:TPU:0, one launch (start us, length us, event | category | flops | bytes accessed | tf_op | source)
XLA Modules:
  0.0 39.4 jit_solution(13973013264486682461)
XLA Ops:
  0.7 0.6 %collective-permute-start = (bf16[16,256]{1,0:T(8,128)(2,1)}, bf16[16,256]{1,0:T(8,128)(2,1)S(1)}, u32[]{:S(2)}, u32[]{:S(2)}) collective-permute-start(bf16[16,256]{1,0:T(8,128)(2,1)} %own_ref.5), channel_id=1, source_target_pairs={{0,1},{1,0},{2,3},{3,2},{4,5},{5,4},{6,7},{7,6},{8,9},{9,8},{10,11... | collective-permute-start | bytes 24584 | tf_op jit(solution)/shard_map/ppermute | solution.py:19
  1.3 1.0 %collective-permute-done.other_ref = bf16[16,256]{1,0:T(8,128)(2,1)S(1)} collective-permute-done((bf16[16,256]{1,0:T(8,128)(2,1)}, bf16[16,256]{1,0:T(8,128)(2,1)S(1)}, u32[]{:S(2)}, u32[]{:S(2)}) %collective-permute-start) | collective-permute-done | bytes 8224 | tf_op jit(solution)/shard_map/ppermute | solution.py:19
  3.1 3.0 %collective-permute-start.1 = (bf16[4,3840]{1,0:T(4,128)(2,1)S(1)}, bf16[4,3840]{1,0:T(4,128)(2,1)S(1)}, u32[]{:S(2)}, u32[]{:S(2)}) collective-permute-start(bf16[4,3840]{1,0:T(4,128)(2,1)S(1)} %get-tuple-element.20), channel_id=1, source_target_pairs={{0,2},{1,3},{2,0},{3,1},{4,6},{5,7},{6,4},{7,5},{8,10},{9,11},{10,... | collective-permute-start | bytes 92168 | tf_op jit(solution)/shard_map/ppermute | solution.py:26
  6.1 2.6 %collective-permute-start.2 = (bf16[4,3840]{1,0:T(4,128)(2,1)S(1)}, bf16[4,3840]{1,0:T(4,128)(2,1)S(1)}, u32[]{:S(2)}, u32[]{:S(2)}) collective-permute-start(bf16[4,3840]{1,0:T(4,128)(2,1)S(1)} %get-tuple-element.21), channel_id=1, source_target_pairs={{0,4},{1,5},{2,6},{3,7},{4,0},{5,1},{6,2},{7,3},{8,12},{9,13},{10,... | collective-permute-start | bytes 92168 | tf_op jit(solution)/shard_map/ppermute | solution.py:26
  9.0 2.5 %collective-permute-done.2.refs_2_ = bf16[4,3840]{1,0:T(4,128)(2,1)S(1)} collective-permute-done((bf16[4,3840]{1,0:T(4,128)(2,1)S(1)}, bf16[4,3840]{1,0:T(4,128)(2,1)S(1)}, u32[]{:S(2)}, u32[]{:S(2)}) %collective-permute-start.2) | collective-permute-done | bytes 30752 | tf_op jit(solution)/shard_map/ppermute | solution.py:26
  11.5 3.0 %collective-permute-done.3.refs_3_ = bf16[4,3840]{1,0:T(4,128)(2,1)S(1)} collective-permute-done((bf16[4,3840]{1,0:T(4,128)(2,1)S(1)}, bf16[4,3840]{1,0:T(4,128)(2,1)S(1)}, u32[]{:S(2)}, u32[]{:S(2)}) %collective-permute-start.3) | collective-permute-done | bytes 30752 | tf_op jit(solution)/shard_map/ppermute | solution.py:26
  15.1 2.0 %collective-permute-start.4 = (bf16[4,1024]{1,0:T(4,128)(2,1)S(1)}, bf16[4,1024]{1,0:T(4,128)(2,1)S(1)}, u32[]{:S(2)}, u32[]{:S(2)}) collective-permute-start(bf16[4,1024]{1,0:T(4,128)(2,1)S(1)} %get-tuple-element.23.gated_ref), channel_id=1, source_target_pairs={{0,3},{1,2},{2,1},{3,0},{4,7},{5,6},{6,5},{7,4},{8,11},{9,10},{10,... | collective-permute-start | bytes 24584 | tf_op jit(solution)/shard_map/ppermute | solution.py:26
  17.3 2.5 %collective-permute-done.6.refs_2_ = bf16[4,1024]{1,0:T(4,128)(2,1)S(1)} collective-permute-done((bf16[4,1024]{1,0:T(4,128)(2,1)S(1)}, bf16[4,1024]{1,0:T(4,128)(2,1)S(1)}, u32[]{:S(2)}, u32[]{:S(2)}) %collective-permute-start.6) | collective-permute-done | bytes 8224 | tf_op jit(solution)/shard_map/ppermute | solution.py:26
  20.1 0.7 %collective-permute-start.8 = (bf16[16,512]{1,0:T(8,128)(2,1)S(1)}, bf16[16,512]{1,0:T(8,128)(2,1)S(1)}, u32[]{:S(2)}, u32[]{:S(2)}) collective-permute-start(bf16[16,512]{1,0:T(8,128)(2,1)S(1)} %get-tuple-element.25), channel_id=1, source_target_pairs={{0,1},{1,0},{2,3},{3,2},{4,5},{5,4},{6,7},{7,6},{8,9},{9,8},{10,11... | collective-permute-start | bytes 49160 | tf_op jit(solution)/shard_map/ppermute | solution.py:19
  20.9 0.8 %collective-permute-done.8.came_ref = bf16[16,512]{1,0:T(8,128)(2,1)S(1)} collective-permute-done((bf16[16,512]{1,0:T(8,128)(2,1)S(1)}, bf16[16,512]{1,0:T(8,128)(2,1)S(1)}, u32[]{:S(2)}, u32[]{:S(2)}) %collective-permute-start.8) | collective-permute-done | bytes 16416 | tf_op jit(solution)/shard_map/ppermute | solution.py:19
  21.7 2.4 %collective-permute-start.9 = (bf16[16,512]{1,0:T(8,128)(2,1)S(1)}, bf16[16,512]{1,0:T(8,128)(2,1)S(1)}, u32[]{:S(2)}, u32[]{:S(2)}) collective-permute-start(bf16[16,512]{1,0:T(8,128)(2,1)S(1)} %shard_map.151.refs_0_.stream_ref), channel_id=1, source_target_pairs={{0,7},{1,6},{2,5},{3,4},{4,3},{5,2},{6,1},{7,0},{8,15},{9,14},{10,... | collective-permute-start | bytes 49160 | tf_op jit(solution)/shard_map/ppermute | solution.py:26
  24.1 0.8 %collective-permute-start.11 = (bf16[16,512]{1,0:T(8,128)(2,1)S(1)}, bf16[16,512]{1,0:T(8,128)(2,1)S(1)}, u32[]{:S(2)}, u32[]{:S(2)}) collective-permute-start(bf16[16,512]{1,0:T(8,128)(2,1)S(1)} %shard_map.151.refs_0_.stream_ref), channel_id=1, source_target_pairs={{0,5},{1,4},{2,7},{3,6},{4,1},{5,0},{6,3},{7,2},{8,13},{9,12},{10,... | collective-permute-start | bytes 49160 | tf_op jit(solution)/shard_map/ppermute | solution.py:26
  25.0 0.9 %collective-permute-start.10 = (bf16[16,512]{1,0:T(8,128)(2,1)S(1)}, bf16[16,512]{1,0:T(8,128)(2,1)S(1)}, u32[]{:S(2)}, u32[]{:S(2)}) collective-permute-start(bf16[16,512]{1,0:T(8,128)(2,1)S(1)} %shard_map.151.refs_0_.stream_ref), channel_id=1, source_target_pairs={{0,3},{1,2},{2,1},{3,0},{4,7},{5,6},{6,5},{7,4},{8,11},{9,10},{10,... | collective-permute-start | bytes 49160 | tf_op jit(solution)/shard_map/ppermute | solution.py:26
  25.9 1.0 %collective-permute-done.9.refs_1_ = bf16[16,512]{1,0:T(8,128)(2,1)S(1)} collective-permute-done((bf16[16,512]{1,0:T(8,128)(2,1)S(1)}, bf16[16,512]{1,0:T(8,128)(2,1)S(1)}, u32[]{:S(2)}, u32[]{:S(2)}) %collective-permute-start.9) | collective-permute-done | bytes 16416 | tf_op jit(solution)/shard_map/ppermute | solution.py:26
  27.3 1.0 %collective-permute-done.11.refs_1_ = bf16[16,512]{1,0:T(8,128)(2,1)S(1)} collective-permute-done((bf16[16,512]{1,0:T(8,128)(2,1)S(1)}, bf16[16,512]{1,0:T(8,128)(2,1)S(1)}, u32[]{:S(2)}, u32[]{:S(2)}) %collective-permute-start.11) | collective-permute-done | bytes 16416 | tf_op jit(solution)/shard_map/ppermute | solution.py:26
  28.3 1.0 %mixer.1 = (f32[4,16,256]{2,1,0:T(8,128)S(1)}, bf16[4,16,256]{2,1,0:T(8,128)(2,1)S(1)}) custom-call(f32[16,128]{1,0:T(8,128)S(1)} %get-tuple-element.26.squares_ref, f32[16,1024]{1,0:T(8,128)S(1)} %get-tuple-element.27.hidden_ref, bf16[16,512]{1,0:T(8,128)(2,1)S(1)} %collective-permute-done.10.refs_0_, bf16[16,512]{1,0:T(8,128)(2,1)S(1)} %collective-permute-done.11.refs_1_, ...), custom_call_target="tpu_custom_call" | custom-call | flops 131072 | bytes 131072 | tf_op jit(solution)/shard_map/mixer/pallas_call | solution.py:315
  29.5 1.0 %collective-permute-done.12.came_ref = bf16[4,16,256]{2,1,0:T(8,128)(2,1)S(1)} collective-permute-done((bf16[4,16,256]{2,1,0:T(8,128)(2,1)S(1)}, bf16[4,16,256]{2,1,0:T(8,128)(2,1)S(1)}, u32[]{:S(2)}, u32[]{:S(2)}) %collective-permute-start.12) | collective-permute-done | bytes 32800 | tf_op jit(solution)/shard_map/ppermute | solution.py:19
  30.6 0.8 %collective-permute-start.13 = (bf16[16,256]{1,0:T(8,128)(2,1)S(1)}, bf16[16,256]{1,0:T(8,128)(2,1)S(1)}, u32[]{:S(2)}, u32[]{:S(2)}) collective-permute-start(bf16[16,256]{1,0:T(8,128)(2,1)S(1)} %get-tuple-element.31), channel_id=1, source_target_pairs={{0,3},{1,2},{2,1},{3,0},{4,7},{5,6},{6,5},{7,4},{8,11},{9,10},{10,... | collective-permute-start | bytes 24584 | tf_op jit(solution)/shard_map/ppermute | solution.py:26
  31.3 1.6 %collective-permute-start.14 = (bf16[16,256]{1,0:T(8,128)(2,1)S(1)}, bf16[16,256]{1,0:T(8,128)(2,1)S(1)}, u32[]{:S(2)}, u32[]{:S(2)}) collective-permute-start(bf16[16,256]{1,0:T(8,128)(2,1)S(1)} %get-tuple-element.32), channel_id=1, source_target_pairs={{0,5},{1,4},{2,7},{3,6},{4,1},{5,0},{6,3},{7,2},{8,13},{9,12},{10,... | collective-permute-start | bytes 24584 | tf_op jit(solution)/shard_map/ppermute | solution.py:26
  32.9 1.6 %collective-permute-start.15 = (bf16[16,256]{1,0:T(8,128)(2,1)S(1)}, bf16[16,256]{1,0:T(8,128)(2,1)S(1)}, u32[]{:S(2)}, u32[]{:S(2)}) collective-permute-start(bf16[16,256]{1,0:T(8,128)(2,1)S(1)} %get-tuple-element.33), channel_id=1, source_target_pairs={{0,7},{1,6},{2,5},{3,4},{4,3},{5,2},{6,1},{7,0},{8,15},{9,14},{10,... | collective-permute-start | bytes 24584 | tf_op jit(solution)/shard_map/ppermute | solution.py:26
  34.5 1.1 %update.3.refs_0_ = f32[4,2,256,512]{3,2,1,0:T(8,128)} custom-call(f32[2,4,512]{2,1,0:T(4,128)S(1)} %get-tuple-element.34.factors_ref, f32[4,1024]{1,0:T(4,128)S(1)} %get-tuple-element.35.values_ref, f32[4,2,256,512]{3,2,1,0:T(8,128)S(1)} %copy-done), custom_call_target="tpu_custom_call" | custom-call | flops 131072 | bytes 131072 | tf_op jit(solution)/shard_map/update/pallas_call | solution.py:205
  35.6 1.4 %update.4.refs_0_ = f32[4,2,256,512]{3,2,1,0:T(8,128)} custom-call(f32[2,4,512]{2,1,0:T(4,128)S(1)} %get-tuple-element.34.factors_ref, f32[4,1024]{1,0:T(4,128)S(1)} %get-tuple-element.35.values_ref, f32[4,2,256,512]{3,2,1,0:T(8,128)S(1)} %copy-done, f32[4,2,256,512]{3,2,1,0:T(8,128)} %update.3.refs_0_), custom_call_target="tpu_custom_call", output_to_operand_aliasing={{}: (3, {})} | custom-call | flops 131072 | bytes 131072 | tf_op jit(solution)/shard_map/update/pallas_call | solution.py:205
  37.1 1.7 %update.5 = f32[4,2,256,512]{3,2,1,0:T(8,128)} custom-call(f32[2,4,512]{2,1,0:T(4,128)S(1)} %get-tuple-element.34.factors_ref, f32[4,1024]{1,0:T(4,128)S(1)} %get-tuple-element.35.values_ref, f32[4,2,256,512]{3,2,1,0:T(8,128)S(1)} %copy-done, f32[4,2,256,512]{3,2,1,0:T(8,128)} %update.4.refs_0_), custom_call_target="tpu_custom_call", output_to_operand_aliasing={{}: (3, {})} | custom-call | flops 131072 | bytes 131072 | tf_op jit(solution)/shard_map/update/pallas_call | solution.py:205
  38.8 0.6 %shard_map.153 = bf16[16,256]{1,0:T(8,128)(2,1)} custom-call(bf16[16,512]{1,0:T(8,128)(2,1)S(1)} %shard_map.151.refs_0_.stream_ref, f32[16,256]{1,0:T(8,128)S(1)} %get-tuple-element.30.refs_0_, bf16[16,256]{1,0:T(8,128)(2,1)S(1)} %collective-permute-done.13.refs_1_, bf16[16,256]{1,0:T(8,128)(2,1)S(1)} %collective-permute-done.14.refs_2_, ...), custom_call_target="tpu_custom_call" | custom-call | flops 20000000000 | bytes 1048576 | tf_op jit(solution)/shard_map/pallas_call | solution.py:349
  (51 shorter events, 2.8 us)
Async XLA Ops:
  0.7 2.0 %copy-start.11 = (bf16[512,512]{1,0:T(8,128)(2,1)S(1)}, bf16[512,512]{1,0:T(8,128)(2,1)}, u32[]{:S(2)}) copy-start(bf16[512,512]{1,0:T(8,128)(2,1)} %refs_2_.1) | copy-start | bytes 1572868
  0.7 1.6 %collective-permute-start = (bf16[16,256]{1,0:T(8,128)(2,1)}, bf16[16,256]{1,0:T(8,128)(2,1)S(1)}, u32[]{:S(2)}, u32[]{:S(2)}) collective-permute-start(bf16[16,256]{1,0:T(8,128)(2,1)} %own_ref.5), channel_id=1, source_target_pairs={{0,1},{1,0},{2,3},{3,2},{4,5},{5,4},{6,7},{7,6},{8,9},{9,8},{10,11... | collective-permute-start | bytes 24584 | tf_op jit(solution)/shard_map/ppermute | solution.py:19
  2.7 6.0 %copy-start.5 = (bf16[1024,512]{1,0:T(8,128)(2,1)S(1)}, bf16[1024,512]{1,0:T(8,128)(2,1)}, u32[]{:S(2)}) copy-start(bf16[1024,512]{1,0:T(8,128)(2,1)} %w_ref.1) | copy-start | bytes 3145732
  2.7 6.0 %copy-start = (f32[4,2,256,512]{3,2,1,0:T(8,128)S(1)}, f32[4,2,256,512]{3,2,1,0:T(8,128)}, u32[]{:S(2)}) copy-start(f32[4,2,256,512]{3,2,1,0:T(8,128)} %state_ref.7) | copy-start | bytes 12582916
  3.1 11.3 %copy-start.12 = (f32[512]{0:T(512)S(1)}, f32[512]{0:T(512)}, u32[]{:S(2)}) copy-start(f32[512]{0:T(512)} %param.22) | copy-start | bytes 6148
  3.1 11.3 %copy-start.13 = (f32[512]{0:T(512)S(1)}, f32[512]{0:T(512)}, u32[]{:S(2)}) copy-start(f32[512]{0:T(512)} %param.23) | copy-start | bytes 6148
  3.1 5.8 %collective-permute-start.1 = (bf16[4,3840]{1,0:T(4,128)(2,1)S(1)}, bf16[4,3840]{1,0:T(4,128)(2,1)S(1)}, u32[]{:S(2)}, u32[]{:S(2)}) collective-permute-start(bf16[4,3840]{1,0:T(4,128)(2,1)S(1)} %get-tuple-element.20), channel_id=1, source_target_pairs={{0,2},{1,3},{2,0},{3,1},{4,6},{5,7},{6,4},{7,5},{8,10},{9,11},{10,... | collective-permute-start | bytes 92168 | tf_op jit(solution)/shard_map/ppermute | solution.py:26
  6.1 5.3 %collective-permute-start.2 = (bf16[4,3840]{1,0:T(4,128)(2,1)S(1)}, bf16[4,3840]{1,0:T(4,128)(2,1)S(1)}, u32[]{:S(2)}, u32[]{:S(2)}) collective-permute-start(bf16[4,3840]{1,0:T(4,128)(2,1)S(1)} %get-tuple-element.21), channel_id=1, source_target_pairs={{0,4},{1,5},{2,6},{3,7},{4,0},{5,1},{6,2},{7,3},{8,12},{9,13},{10,... | collective-permute-start | bytes 92168 | tf_op jit(solution)/shard_map/ppermute | solution.py:26
  8.7 5.7 %collective-permute-start.3 = (bf16[4,3840]{1,0:T(4,128)(2,1)S(1)}, bf16[4,3840]{1,0:T(4,128)(2,1)S(1)}, u32[]{:S(2)}, u32[]{:S(2)}) collective-permute-start(bf16[4,3840]{1,0:T(4,128)(2,1)S(1)} %get-tuple-element.22), channel_id=1, source_target_pairs={{0,6},{1,7},{2,4},{3,5},{4,2},{5,3},{6,0},{7,1},{8,14},{9,15},{10,... | collective-permute-start | bytes 92168 | tf_op jit(solution)/shard_map/ppermute | solution.py:26
  8.7 11.1 %collective-permute-start.7 = (bf16[1024,512]{1,0:T(8,128)(2,1)S(1)}, bf16[1024,512]{1,0:T(8,128)(2,1)S(1)}, u32[]{:S(2)}, u32[]{:S(2)}) collective-permute-start(bf16[1024,512]{1,0:T(8,128)(2,1)S(1)} %copy-done.5), channel_id=1, source_target_pairs={{0,1},{1,0},{2,3},{3,2},{4,5},{5,4},{6,7},{7,6},{8,9},{9,8},{10,11... | collective-permute-start | bytes 3145736 | tf_op jit(solution)/shard_map/ppermute | solution.py:19
  15.0 4.9 %collective-permute-start.6 = (bf16[4,1024]{1,0:T(4,128)(2,1)S(1)}, bf16[4,1024]{1,0:T(4,128)(2,1)S(1)}, u32[]{:S(2)}, u32[]{:S(2)}) collective-permute-start(bf16[4,1024]{1,0:T(4,128)(2,1)S(1)} %get-tuple-element.23.gated_ref), channel_id=1, source_target_pairs={{0,7},{1,6},{2,5},{3,4},{4,3},{5,2},{6,1},{7,0},{8,15},{9,14},{10,... | collective-permute-start | bytes 24584 | tf_op jit(solution)/shard_map/ppermute | solution.py:26
  15.0 4.9 %collective-permute-start.5 = (bf16[4,1024]{1,0:T(4,128)(2,1)S(1)}, bf16[4,1024]{1,0:T(4,128)(2,1)S(1)}, u32[]{:S(2)}, u32[]{:S(2)}) collective-permute-start(bf16[4,1024]{1,0:T(4,128)(2,1)S(1)} %get-tuple-element.23.gated_ref), channel_id=1, source_target_pairs={{0,5},{1,4},{2,7},{3,6},{4,1},{5,0},{6,3},{7,2},{8,13},{9,12},{10,... | collective-permute-start | bytes 24584 | tf_op jit(solution)/shard_map/ppermute | solution.py:26
  15.1 4.8 %collective-permute-start.4 = (bf16[4,1024]{1,0:T(4,128)(2,1)S(1)}, bf16[4,1024]{1,0:T(4,128)(2,1)S(1)}, u32[]{:S(2)}, u32[]{:S(2)}) collective-permute-start(bf16[4,1024]{1,0:T(4,128)(2,1)S(1)} %get-tuple-element.23.gated_ref), channel_id=1, source_target_pairs={{0,3},{1,2},{2,1},{3,0},{4,7},{5,6},{6,5},{7,4},{8,11},{9,10},{10,... | collective-permute-start | bytes 24584 | tf_op jit(solution)/shard_map/ppermute | solution.py:26
  20.1 1.6 %collective-permute-start.8 = (bf16[16,512]{1,0:T(8,128)(2,1)S(1)}, bf16[16,512]{1,0:T(8,128)(2,1)S(1)}, u32[]{:S(2)}, u32[]{:S(2)}) collective-permute-start(bf16[16,512]{1,0:T(8,128)(2,1)S(1)} %get-tuple-element.25), channel_id=1, source_target_pairs={{0,1},{1,0},{2,3},{3,2},{4,5},{5,4},{6,7},{7,6},{8,9},{9,8},{10,11... | collective-permute-start | bytes 49160 | tf_op jit(solution)/shard_map/ppermute | solution.py:19
  21.7 5.2 %copy-start.1 = (bf16[2048,1024]{1,0:T(8,128)(2,1)S(1)}, bf16[2048,1024]{1,0:T(8,128)(2,1)}, u32[]{:S(2)}) copy-start(bf16[2048,1024]{1,0:T(8,128)(2,1)} %refs_3_.3) | copy-start | bytes 12582916
  21.7 5.2 %copy-start.2 = (bf16[1024,2048]{1,0:T(8,128)(2,1)S(1)}, bf16[1024,2048]{1,0:T(8,128)(2,1)}, u32[]{:S(2)}) copy-start(bf16[1024,2048]{1,0:T(8,128)(2,1)} %refs_4_.3) | copy-start | bytes 12582916
  21.7 5.2 %copy-start.6 = (f32[2048]{0:T(1024)S(1)}, f32[2048]{0:T(1024)}, u32[]{:S(2)}) copy-start(f32[2048]{0:T(1024)} %param.25) | copy-start | bytes 24580
  21.7 5.1 %collective-permute-start.9 = (bf16[16,512]{1,0:T(8,128)(2,1)S(1)}, bf16[16,512]{1,0:T(8,128)(2,1)S(1)}, u32[]{:S(2)}, u32[]{:S(2)}) collective-permute-start(bf16[16,512]{1,0:T(8,128)(2,1)S(1)} %shard_map.151.refs_0_.stream_ref), channel_id=1, source_target_pairs={{0,7},{1,6},{2,5},{3,4},{4,3},{5,2},{6,1},{7,0},{8,15},{9,14},{10,... | collective-permute-start | bytes 49160 | tf_op jit(solution)/shard_map/ppermute | solution.py:26
  24.1 4.2 %collective-permute-start.11 = (bf16[16,512]{1,0:T(8,128)(2,1)S(1)}, bf16[16,512]{1,0:T(8,128)(2,1)S(1)}, u32[]{:S(2)}, u32[]{:S(2)}) collective-permute-start(bf16[16,512]{1,0:T(8,128)(2,1)S(1)} %shard_map.151.refs_0_.stream_ref), channel_id=1, source_target_pairs={{0,5},{1,4},{2,7},{3,6},{4,1},{5,0},{6,3},{7,2},{8,13},{9,12},{10,... | collective-permute-start | bytes 49160 | tf_op jit(solution)/shard_map/ppermute | solution.py:26
  25.0 3.4 %collective-permute-start.10 = (bf16[16,512]{1,0:T(8,128)(2,1)S(1)}, bf16[16,512]{1,0:T(8,128)(2,1)S(1)}, u32[]{:S(2)}, u32[]{:S(2)}) collective-permute-start(bf16[16,512]{1,0:T(8,128)(2,1)S(1)} %shard_map.151.refs_0_.stream_ref), channel_id=1, source_target_pairs={{0,3},{1,2},{2,1},{3,0},{4,7},{5,6},{6,5},{7,4},{8,11},{9,10},{10,... | collective-permute-start | bytes 49160 | tf_op jit(solution)/shard_map/ppermute | solution.py:26
  29.3 1.3 %collective-permute-start.12 = (bf16[4,16,256]{2,1,0:T(8,128)(2,1)S(1)}, bf16[4,16,256]{2,1,0:T(8,128)(2,1)S(1)}, u32[]{:S(2)}, u32[]{:S(2)}) collective-permute-start(bf16[4,16,256]{2,1,0:T(8,128)(2,1)S(1)} %get-tuple-element.29), channel_id=1, source_target_pairs={{0,1},{1,0},{2,3},{3,2},{4,5},{5,4},{6,7},{7,6},{8,9},{9,8},{10,11... | collective-permute-start | bytes 98312 | tf_op jit(solution)/shard_map/ppermute | solution.py:19
  30.6 8.2 %collective-permute-start.13 = (bf16[16,256]{1,0:T(8,128)(2,1)S(1)}, bf16[16,256]{1,0:T(8,128)(2,1)S(1)}, u32[]{:S(2)}, u32[]{:S(2)}) collective-permute-start(bf16[16,256]{1,0:T(8,128)(2,1)S(1)} %get-tuple-element.31), channel_id=1, source_target_pairs={{0,3},{1,2},{2,1},{3,0},{4,7},{5,6},{6,5},{7,4},{8,11},{9,10},{10,... | collective-permute-start | bytes 24584 | tf_op jit(solution)/shard_map/ppermute | solution.py:26
  31.3 7.4 %collective-permute-start.14 = (bf16[16,256]{1,0:T(8,128)(2,1)S(1)}, bf16[16,256]{1,0:T(8,128)(2,1)S(1)}, u32[]{:S(2)}, u32[]{:S(2)}) collective-permute-start(bf16[16,256]{1,0:T(8,128)(2,1)S(1)} %get-tuple-element.32), channel_id=1, source_target_pairs={{0,5},{1,4},{2,7},{3,6},{4,1},{5,0},{6,3},{7,2},{8,13},{9,12},{10,... | collective-permute-start | bytes 24584 | tf_op jit(solution)/shard_map/ppermute | solution.py:26
  32.9 5.8 %collective-permute-start.15 = (bf16[16,256]{1,0:T(8,128)(2,1)S(1)}, bf16[16,256]{1,0:T(8,128)(2,1)S(1)}, u32[]{:S(2)}, u32[]{:S(2)}) collective-permute-start(bf16[16,256]{1,0:T(8,128)(2,1)S(1)} %get-tuple-element.33), channel_id=1, source_target_pairs={{0,7},{1,6},{2,5},{3,4},{4,3},{5,2},{6,1},{7,0},{8,15},{9,14},{10,... | collective-permute-start | bytes 24584 | tf_op jit(solution)/shard_map/ppermute | solution.py:26
  (6 other events, 10.7 us)
